TPU v7x, 512 devices: a whole 4x8x8 slice. The times are simulated.
512 devices in a mesh: sp: 32 (over z, x), dp: 16 (over y, core).
Axes of the slice: x: 4, y: 8, z: 8, core: 2. Of those that a mesh axis runs over, the one named last changes fastest.
Arguments:
- hidden_in: bfloat16 [16384, 2048], P('sp'), may hold values from -6 to 6
- content_weight: bfloat16 [2048, 2048], P('sp', 'dp'), may hold values from -0.125 to 0.125
- gating_weight: bfloat16 [2048, 2048], P('sp', 'dp'), may hold values from -2 to 2
- norm_gain: float32 [2048], P('dp'), may hold values from 0.1 to 1.9
- mixing_weight: bfloat16 [16, 128, 128], P('dp'), may hold values from -0.5 to 0.5
- mixing_bias: float32 [16, 128], P('dp'), may hold values from 0.1 to 1.9
- out_grad: bfloat16 [16384, 2048], P('sp', 'dp'), may hold values from -13 to 13
Outputs:
- input_grad: bfloat16 [16384, 2048], P('sp', 'dp')
- content_grad: float32 [2048, 2048], P('sp', 'dp')
- gating_grad: float32 [2048, 2048], P('sp', 'dp')
- mixing_grad: float32 [16, 128, 128], P('dp')
All inputs are finite; a program needn't handle non-finite values.
Results may differ from a plain program's by a relative error of at most 0.019.
Values may be sent and summed in bfloat16 or wider, within the bound.
No kernel may reach another device: no remote copies, remote signals or barrier semaphores. Data moves between devices by JAX's collectives and lax.ppermute only.
A program may use at most 64 MiB of HBM per device.

v0:
```python
import functools
import math

import jax
import jax.numpy as jnp
from jax import lax
from jax.experimental import pallas as pl
from jax.experimental.pallas import tpu as pltpu
from jax.sharding import Mesh
from jax.sharding import PartitionSpec as P


BLOCK = 128
SP = ("sp_0", "sp_1")
DP = ("dp_0", "dp_1")


norm_eps = 1e-05
f32, bf16 = jnp.float32, jnp.bfloat16


def exchange(array, axis):
    return lax.all_to_all(array, axis, split_axis=0, concat_axis=0, tiled=True)


def swapped(array):
    return lax.ppermute(array, "dp_1", [(0, 1), (1, 0)])


def sent_apart(array, step):
    ring = lax.axis_size("dp_0")
    moves = []
    for y in range(ring):
        moves.append((2 * y, 2 * ((y + step) % ring)))
        moves.append((2 * y + 1, 2 * ((y - step) % ring) + 1))
    return lax.ppermute(array, DP, moves)


def normal_below(values):
    return 0.5 * (1.0 + lax.erf(values * (1.0 / math.sqrt(2.0))))


def gelu_slope(values):
    density = jnp.exp(-0.5 * values * values) * (1.0 / math.sqrt(2.0 * math.pi))
    return normal_below(values) + values * density


def causal(weights):
    rows = lax.broadcasted_iota(jnp.int32, (BLOCK, BLOCK), 0)
    cols = lax.broadcasted_iota(jnp.int32, (BLOCK, BLOCK), 1)
    return jnp.where(cols <= rows, weights, jnp.zeros_like(weights))


def nt(a, b, **kw):
    return lax.dot_general(a, b, (((1,), (1,)), ((), ())), preferred_element_type=f32, **kw)


def nn(a, b):
    return jnp.dot(a, b, preferred_element_type=f32)


def call(body, outs, scalars=False):
    def run(*args):
        inside = [pltpu.VMEM] * len(args)
        if scalars:
            inside[0] = pltpu.SMEM
        args = [
            a if m is pltpu.SMEM else pltpu.with_memory_space_constraint(a, m)
            for a, m in zip(args, inside)
        ]
        specs = [pl.BlockSpec(memory_space=m) for m in inside]
        limit = pltpu.CompilerParams(vmem_limit_bytes=20 * 1024 * 1024)
        made = pl.pallas_call(body, out_shape=outs, in_specs=specs, compiler_params=limit)
        return made(*args)

    return run


def like(shape, dtype):
    return pltpu.VMEM(shape, dtype)


def outside(shape, dtype):
    return jax.ShapeDtypeStruct(shape, dtype)


def project_body(hidden, weight, mixing, gain, grad, pre_out, gating_out, mixed_out, back_out, sums_out):
    n_x, n_z, rows, both = weight.shape
    slab = n_x * rows
    width = both // 2
    pre = None
    for z in range(n_z):
        term = nn(hidden[:, z * slab : (z + 1) * slab], weight[:, z].reshape(slab, both))
        pre = term if pre is None else pre + term
    pre = pre.astype(bf16)
    pre_out[...] = pre
    pre_content = pre[:, :width].astype(f32)
    pre_gating = pre[:, width:].astype(f32)
    gating = pre_gating * normal_below(pre_gating)
    gating_out[...] = gating
    mixed_grad = (grad[...].astype(f32) * (pre_content * normal_below(pre_content))).astype(bf16)
    mixed_out[...] = mixed_grad
    table = causal(mixing[0].astype(f32)).T.astype(bf16)
    pieces = []
    for at in range(0, mixed_grad.shape[0], BLOCK):
        pieces.append(nn(table, mixed_grad[at : at + BLOCK]) * gain[...])
    back = jnp.concatenate(pieces, axis=0)
    back_out[...] = back
    row = lax.broadcasted_iota(jnp.int32, (8, width), 0)
    sums = None
    for at, values in enumerate((gating, gating * gating, back, back * gating)):
        pick = jnp.where(row == at, 1.0, 0.0).astype(f32)
        term = nt(pick, values, precision=lax.Precision.HIGHEST)
        sums = term if sums is None else sums + term
    for peer in range(sums_out.shape[0]):
        sums_out[peer] = sums[:4]


def join_body(content, gating, out):
    both = jnp.concatenate([content[...], gating[...]], axis=1)
    for peer in range(out.shape[0]):
        out[peer] = both


def spread_body(arrived, out):
    for peer in range(out.shape[0]):
        out[peer] = arrived[...]


def flip_body(array, out):
    step = 256
    for at in range(0, array.shape[1], step):
        out[at : at + step] = array[:, at : at + step].T


def slopes_body(pre, grad, content_out, gating_out):
    width = grad.shape[1]
    content_out[...] = grad[...].astype(f32) * gelu_slope(pre[:, :width].astype(f32))
    gating_out[...] = gelu_slope(pre[:, width:].astype(f32))


def norm_body(full_width, sums, gating, mixed_grad, back, content_slope, gating_slope, mixing, bias, gain, joined_out, mixing_out):
    total = jnp.sum(sums[...], axis=0) * (1.0 / full_width)
    row_mean = total[0:1]
    row_var = total[1:2] - row_mean * row_mean
    inv_std = lax.rsqrt(row_var + norm_eps)
    first = total[2:3]
    second = inv_std * (total[3:4] - row_mean * first)
    columns = jnp.concatenate([row_mean, inv_std, first, second] * 2, axis=0).T
    row_mean, inv_std, first, second = [columns[:, i : i + 1] for i in range(4)]
    centred = (gating[...] - row_mean) * inv_std
    normed = (centred * gain[...]).astype(bf16)
    table = causal(mixing[0].astype(f32)).astype(bf16)
    shift = jnp.broadcast_to(bias[...], (8, BLOCK)).T[:, 0:1]
    width = normed.shape[1]
    mixing_grad = None
    for at in range(0, normed.shape[0], BLOCK):
        rows = slice(at, at + BLOCK)
        mixed = nn(table, normed[rows]) + shift
        joined_out[rows, :width] = (mixed * content_slope[rows]).astype(bf16)
        term = nt(mixed_grad[rows], normed[rows])
        mixing_grad = term if mixing_grad is None else mixing_grad + term
    gating_back = inv_std * (back[...] - first - centred * second)
    joined_out[:, width:] = (gating_back * gating_slope[...]).astype(bf16)
    mixing_grad = causal(mixing_grad).astype(bf16)
    half = BLOCK // 2
    mixing_out[...] = jnp.concatenate([mixing_grad[:half], mixing_grad[half:]], axis=1)


def weight_terms_body(hidden_t, joined, mixing_term, out):
    n_x, n_all, rows, _ = out.shape
    n_z = n_all - 1
    slab = n_x * rows
    for z in range(n_z):
        term = nn(hidden_t[z * slab : (z + 1) * slab], joined[...]).astype(bf16)
        for x in range(n_x):
            out[x, z] = term[x * rows : (x + 1) * rows]
    for x in range(n_x):
        out[x, n_z] = mixing_term[...]


def input_terms_body(where, joined, joined_far, weight, weight_far, one, two, three, four, own):
    n_x, _, rows, both = weight.shape

    def term(x_from, n, z):
        near = weight[pl.ds(x_from, n), pl.ds(z, 1)].reshape(n * rows, both)
        far = weight_far[pl.ds(x_from, n), pl.ds(z, 1)].reshape(n * rows, both)
        return nt(joined[...], near) + nt(joined_far[...], far)

    three[...] = term(0, n_x, where[3]).astype(bf16)
    two[...] = term(0, n_x, where[2]).astype(bf16)
    one[...] = term(0, n_x, where[1]).astype(bf16)
    half = n_x // 2
    four[...] = term(where[5] * half, half, where[4]).astype(bf16)
    own[...] = term(where[5] * half, half, where[0])


def regroup_body(arrived, out):
    n_z = out.shape[0]
    total = arrived[0].astype(f32)
    for x in range(1, arrived.shape[0]):
        total = total + arrived[x].astype(f32)
    total = total.astype(bf16)
    for z in range(n_z):
        out[z, 0] = total[z]
        out[z, 1] = total[n_z]


def finish_body(scale, arrived, content_out, gating_out, mixing_out):
    total = arrived[0].astype(f32)
    for z in range(1, arrived.shape[0]):
        total = total + arrived[z].astype(f32)
    total = total * scale
    half = content_out.shape[1]
    content_out[...] = total[0][:, :half]
    gating_out[...] = total[0][:, half:]
    mixing_out[0, : BLOCK // 2] = total[1][:, :half]
    mixing_out[0, BLOCK // 2 :] = total[1][:, half:]


def gather_body(where, one, two, three, four, own, keep_out, send_out):
    half = own.shape[1]
    total = one[...].astype(f32) + two[...].astype(f32) + three[...].astype(f32)
    first = where[5] == 0
    left, right = total[:, :half], total[:, half:]
    keep_out[...] = own[...] + four[...].astype(f32) + jnp.where(first, left, right)
    send_out[...] = jnp.where(first, right, left).astype(bf16)


def step(
    hidden_in, content_weight, gating_weight, norm_gain, mixing_weight, mixing_bias, out_grad
):
    tok_rows, width = hidden_in.shape
    shard_rows, local_width = content_weight.shape
    both = 2 * local_width
    n_z, n_x = lax.axis_size("sp_0"), lax.axis_size("sp_1")
    n_sp, n_dp = n_z * n_x, lax.axis_size(DP)
    ring = lax.axis_size("dp_0")
    full_width = local_width * n_dp
    out_cols = width // n_dp
    grad_scale = 1.0 / math.sqrt(tok_rows * n_sp)
    here, core = lax.axis_index("dp_0"), lax.axis_index("dp_1")
    side = 1 - 2 * core
    where = jnp.stack([(here + side * k + ring) % ring for k in range(5)] + [core]).astype(jnp.int32)
    gain = norm_gain[None, :]

    hidden_t = call(flip_body, like((width, tok_rows), bf16))(hidden_in)
    shards = call(join_body, like((n_z, shard_rows, both), bf16))(content_weight, gating_weight)
    along_z = exchange(shards, "sp_0")
    spread = call(spread_body, like((n_x, n_z, shard_rows, both), bf16))(along_z)
    weight = exchange(spread, "sp_1")
    weight_far = swapped(weight)

    tile, wide = (tok_rows, local_width), (tok_rows, both)
    pre, gating, mixed_grad, back, sums = call(
        project_body,
        (like(wide, bf16), like(tile, f32), like(tile, bf16), like(tile, f32), like((n_dp, 4, tok_rows), f32)),
    )(hidden_in, weight, mixing_weight, gain, out_grad)
    sums = exchange(sums, DP)
    content_slope, gating_slope = call(
        slopes_body, (like(tile, f32), like(tile, f32))
    )(pre, out_grad)
    joined, mixing_term = call(
        functools.partial(norm_body, full_width), (like(wide, bf16), like((BLOCK // 2, both), bf16))
    )(sums, gating, mixed_grad, back, content_slope, gating_slope, mixing_weight, mixing_bias, gain)

    joined_far = swapped(joined)
    terms = call(
        weight_terms_body, like((n_x, n_z + 1, shard_rows, both), bf16)
    )(hidden_t, joined, mixing_term)
    along_x = exchange(terms, "sp_1")

    pair, single = (tok_rows, 2 * out_cols), (tok_rows, out_cols)
    one, two, three, four, own = call(
        input_terms_body,
        (like(pair, bf16), like(pair, bf16), like(pair, bf16), like(single, bf16), like(single, f32)),
        scalars=True,
    )(where, joined, joined_far, weight, weight_far)
    three = sent_apart(three, 3)
    four = sent_apart(four, 4)
    two = sent_apart(two, 2)
    one = sent_apart(one, 1)

    regrouped = call(regroup_body, like((n_z, 2, shard_rows, both), bf16))(along_x)
    arrived = exchange(regrouped, "sp_0")

    keep, send = call(
        gather_body, (like(single, f32), like(single, bf16)), scalars=True
    )(where, one, two, three, four, own)
    input_grad = (keep + swapped(send).astype(f32)).astype(bf16)

    content_grad, gating_grad, mixing_grad = call(
        functools.partial(finish_body, grad_scale),
        (
            outside((shard_rows, local_width), f32),
            outside((shard_rows, local_width), f32),
            outside(mixing_weight.shape, f32),
        ),
    )(arrived)
    return (input_grad, content_grad, gating_grad, mixing_grad)


def solution(mesh):
    split = Mesh(mesh.devices.reshape(8, 4, 8, 2), (*SP, *DP))
    in_specs = (
        P(SP, None),
        P(SP, DP),
        P(SP, DP),
        P(DP),
        P(DP, None, None),
        P(DP, None),
        P(SP, DP),
    )
    out_specs = (P(SP, DP), P(SP, DP), P(SP, DP), P(DP, None, None))
    return jax.shard_map(step, mesh=split, in_specs=in_specs, out_specs=out_specs, check_vma=False)
```

profile of v0, /device:TPU:17, one launch (start us, length us, event | category | flops | bytes accessed | tf_op | source)
XLA Modules:
  0.0 139.0 jit_solution(4265777015620229917)
XLA Ops:
  0.7 0.9 copy-done.20
  1.5 0.7 copy-done.21
  2.3 20.3 %all_to_all.25.arrived = bf16[8,64,256]{2,1,0:T(8,128)(2,1)S(1)} all-to-all(bf16[8,64,256]{2,1,0:T(8,128)(2,1)S(1)} %shard_map.102), channel_id=1, replica_groups=mesh['sp_0'=8,'sp_1'=4,'dp_0'=8,'dp_1'=2] {'sp_0'}, dimensions={0} | all-to-all | bytes 524288 | tf_op jit(solution)/shard_map/all_to_all | solution.py:23
  22.7 16.4 %all_to_all.26.weight = bf16[4,8,64,256]{3,2,1,0:T(8,128)(2,1)S(1)} all-to-all(bf16[4,8,64,256]{3,2,1,0:T(8,128)(2,1)S(1)} %shard_map.103), channel_id=1, replica_groups=mesh['sp_0'=8,'sp_1'=4,'dp_0'=8,'dp_1'=2] {'sp_1'}, dimensions={0} | all-to-all | bytes 2097152 | tf_op jit(solution)/shard_map/all_to_all | solution.py:23
  39.1 3.4 %shard_map.104 = (bf16[512,256]{1,0:T(8,128)(2,1)S(1)}, f32[512,128]{1,0:T(8,128)S(1)}, bf16[512,128]{1,0:T(8,128)(2,1)S(1)}, f32[512,128]{1,0:T(8,128)S(1)}, f32[16,4,512]{2,1,0:T(4,128)}) custom-call(bf16[512,2048]{1,0:T(8,128)(2,1)S(1)} %copy-done, bf16[4,8,64,256]{3,2,1,0:T(8,128)(2,1)S(1)} %all_to_all.26.weight, bf16[1,128,128]{2,1,0:T(8,128)(2,1)S(1)} %copy-done.16, ...), custom_call_target="tpu_custom_call" | custom-call | tf_op jit(solution)/shard_map/pallas_call | solution.py:74
  42.5 0.7 copy-done.6
  43.2 0.7 copy-done.8
  43.9 0.7 copy-done.10
  44.6 0.6 copy-done.18
  45.3 10.5 %all-to-all-start.2 = ((f32[16,4,512]{2,1,0:T(4,128)}), f32[16,4,512]{2,1,0:T(4,128)S(1)}, u32[]{:S(2)}, u32[]{:S(2)}) async-start(f32[16,4,512]{2,1,0:T(4,128)} %get-tuple-element.23), calls=%async_computation.2 | async-start | bytes 262144 | tf_op jit(solution)/shard_map/all_to_all | solution.py:23
  55.8 1.6 %copy-done.1 = bf16[512,2048]{1,0:T(8,128)(2,1)S(1)} copy-done((bf16[512,2048]{1,0:T(8,128)(2,1)S(1)}, bf16[512,2048]{1,0:T(8,128)(2,1)}, u32[]{:S(2)}) %copy-start.1) | copy-done | bytes 2097176
  57.4 0.6 shard_map.109.hidden_t
  58.0 0.3 copy-done.7
  58.3 0.2 shard_map.105
  58.6 0.7 copy-done.12
  59.3 0.7 copy-done.14
  60.0 2.9 %all-to-all-done.2.sums = f32[16,4,512]{2,1,0:T(4,128)S(1)} async-done(((f32[16,4,512]{2,1,0:T(4,128)}), f32[16,4,512]{2,1,0:T(4,128)S(1)}, u32[]{:S(2)}, u32[]{:S(2)}) %all-to-all-start.2) | async-done | bytes 131104 | tf_op jit(solution)/shard_map/all_to_all | solution.py:23
  62.9 0.7 copy-done.4
  63.5 0.9 copy-done.5
  64.4 0.9 copy-done.9
  65.4 0.9 copy-done.11
  66.3 0.9 copy-done.13
  67.3 0.9 copy-done.15
  68.2 0.8 copy-done.17
  69.0 0.9 copy-done.19
  69.9 0.7 shard_map.106
  70.6 0.7 shard_map.110
  71.3 1.0 copy-done.2
  72.4 3.5 %all-to-all-start.3 = ((bf16[4,9,64,256]{3,2,1,0:T(8,128)(2,1)}), bf16[4,9,64,256]{3,2,1,0:T(8,128)(2,1)S(1)}, u32[]{:S(2)}, u32[]{:S(2)}) async-start(bf16[4,9,64,256]{3,2,1,0:T(8,128)(2,1)} %copy-done.2), calls=%async_computation.3 | async-start | bytes 2359296 | tf_op jit(solution)/shard_map/all_to_all | solution.py:23
  75.9 1.9 %collective-permute-start.1 = (bf16[4,8,64,256]{3,2,1,0:T(8,128)(2,1)S(1)}, bf16[4,8,64,256]{3,2,1,0:T(8,128)(2,1)S(1)}, u32[]{:S(2)}, u32[]{:S(2)}) collective-permute-start(bf16[4,8,64,256]{3,2,1,0:T(8,128)(2,1)S(1)} %all_to_all.26.weight), channel_id=1, source_target_pairs={{0,1},{1,0},{2,3},{3,2},{4,5},{5,4},{6,7},{7,6},{8,9},{9,8},{10,11... | collective-permute-start | bytes 3145736 | tf_op jit(solution)/shard_map/ppermute | solution.py:27
  77.8 14.6 %all-to-all-done.3.arrived = bf16[4,9,64,256]{3,2,1,0:T(8,128)(2,1)S(1)} async-done(((bf16[4,9,64,256]{3,2,1,0:T(8,128)(2,1)}), bf16[4,9,64,256]{3,2,1,0:T(8,128)(2,1)S(1)}, u32[]{:S(2)}, u32[]{:S(2)}) %all-to-all-start.3) | async-done | bytes 1179680 | tf_op jit(solution)/shard_map/all_to_all | solution.py:23
  92.4 0.9 shard_map.111
  93.4 3.5 %all-to-all-start.4 = ((bf16[8,2,64,256]{3,2,1,0:T(8,128)(2,1)}), bf16[8,2,64,256]{3,2,1,0:T(8,128)(2,1)S(1)}, u32[]{:S(2)}, u32[]{:S(2)}) async-start(bf16[8,2,64,256]{3,2,1,0:T(8,128)(2,1)} %shard_map.111), calls=%async_computation.4 | async-start | bytes 1048576 | tf_op jit(solution)/shard_map/all_to_all | solution.py:23
  96.9 2.8 %collective-permute-start = (bf16[512,256]{1,0:T(8,128)(2,1)S(1)}, bf16[512,256]{1,0:T(8,128)(2,1)S(1)}, u32[]{:S(2)}, u32[]{:S(2)}) collective-permute-start(bf16[512,256]{1,0:T(8,128)(2,1)S(1)} %get-tuple-element.30.joined), channel_id=1, source_target_pairs={{0,1},{1,0},{2,3},{3,2},{4,5},{5,4},{6,7},{7,6},{8,9},{9,8},{10,11... | collective-permute-start | bytes 786440 | tf_op jit(solution)/shard_map/ppermute | solution.py:27
  99.7 0.1 stack.27.where
  99.8 1.0 collective-permute-done.joined_far
  100.8 1.4 %shard_map.107 = (bf16[512,256]{1,0:T(8,128)(2,1)S(1)}, bf16[512,256]{1,0:T(8,128)(2,1)S(1)}, bf16[512,256]{1,0:T(8,128)(2,1)S(1)}, bf16[512,128]{1,0:T(8,128)(2,1)S(1)}, f32[512,128]{1,0:T(8,128)S(1)}) custom-call(s32[6]{0:T(128)S(1)} %stack.27.where, bf16[512,256]{1,0:T(8,128)(2,1)S(1)} %get-tuple-element.30.joined, ...), custom_call_target="tpu_custom_call" | custom-call | tf_op jit(solution)/shard_map/pallas_call | solution.py:74
  102.2 2.9 %collective-permute-start.2 = (bf16[512,256]{1,0:T(8,128)(2,1)S(1)}, bf16[512,256]{1,0:T(8,128)(2,1)S(1)}, u32[]{:S(2)}, u32[]{:S(2)}) collective-permute-start(bf16[512,256]{1,0:T(8,128)(2,1)S(1)} %get-tuple-element.31), channel_id=1, source_target_pairs={{0,2},{1,15},{2,4},{3,1},{4,6},{5,3},{6,8},{7,5},{8,10},{9,7},{10,... | collective-permute-start | bytes 786440 | tf_op jit(solution)/shard_map/ppermute | solution.py:36
  105.1 2.9 %collective-permute-start.3 = (bf16[512,256]{1,0:T(8,128)(2,1)S(1)}, bf16[512,256]{1,0:T(8,128)(2,1)S(1)}, u32[]{:S(2)}, u32[]{:S(2)}) collective-permute-start(bf16[512,256]{1,0:T(8,128)(2,1)S(1)} %get-tuple-element.32), channel_id=1, source_target_pairs={{0,4},{1,13},{2,6},{3,15},{4,8},{5,1},{6,10},{7,3},{8,12},{9,5},{1... | collective-permute-start | bytes 786440 | tf_op jit(solution)/shard_map/ppermute | solution.py:36
  108.0 3.1 %collective-permute-start.4 = (bf16[512,256]{1,0:T(8,128)(2,1)S(1)}, bf16[512,256]{1,0:T(8,128)(2,1)S(1)}, u32[]{:S(2)}, u32[]{:S(2)}) collective-permute-start(bf16[512,256]{1,0:T(8,128)(2,1)S(1)} %get-tuple-element.33), channel_id=1, source_target_pairs={{0,6},{1,11},{2,8},{3,13},{4,10},{5,15},{6,12},{7,1},{8,14},{9,3},... | collective-permute-start | bytes 786440 | tf_op jit(solution)/shard_map/ppermute | solution.py:36
  111.1 6.4 %collective-permute-start.5 = (bf16[512,128]{1,0:T(8,128)(2,1)S(1)}, bf16[512,128]{1,0:T(8,128)(2,1)S(1)}, u32[]{:S(2)}, u32[]{:S(2)}) collective-permute-start(bf16[512,128]{1,0:T(8,128)(2,1)S(1)} %get-tuple-element.34), channel_id=1, source_target_pairs={{0,8},{1,9},{2,10},{3,11},{4,12},{5,13},{6,14},{7,15},{8,0},{9,1},... | collective-permute-start | bytes 393224 | tf_op jit(solution)/shard_map/ppermute | solution.py:36
  117.5 8.9 %collective-permute-done.5.four = bf16[512,128]{1,0:T(8,128)(2,1)S(1)} collective-permute-done((bf16[512,128]{1,0:T(8,128)(2,1)S(1)}, bf16[512,128]{1,0:T(8,128)(2,1)S(1)}, u32[]{:S(2)}, u32[]{:S(2)}) %collective-permute-start.5) | collective-permute-done | bytes 131104 | tf_op jit(solution)/shard_map/ppermute | solution.py:36
  126.3 3.7 %collective-permute-done.4.three = bf16[512,256]{1,0:T(8,128)(2,1)S(1)} collective-permute-done((bf16[512,256]{1,0:T(8,128)(2,1)S(1)}, bf16[512,256]{1,0:T(8,128)(2,1)S(1)}, u32[]{:S(2)}, u32[]{:S(2)}) %collective-permute-start.4) | collective-permute-done | bytes 262176 | tf_op jit(solution)/shard_map/ppermute | solution.py:36
  130.0 0.7 shard_map.108
  130.7 5.9 %collective-permute-start.6 = (bf16[512,128]{1,0:T(8,128)(2,1)S(1)}, bf16[512,128]{1,0:T(8,128)(2,1)S(1)}, u32[]{:S(2)}, u32[]{:S(2)}) collective-permute-start(bf16[512,128]{1,0:T(8,128)(2,1)S(1)} %get-tuple-element.37), channel_id=1, source_target_pairs={{0,1},{1,0},{2,3},{3,2},{4,5},{5,4},{6,7},{7,6},{8,9},{9,8},{10,11... | collective-permute-start | bytes 393224 | tf_op jit(solution)/shard_map/ppermute | solution.py:27
  136.6 1.0 collective-permute-done.6
  137.6 0.7 add_convert_fusion
  138.3 0.7 shard_map.112
  (35 shorter events, 0.2 us)
Async XLA Ops:
  0.6 38.4 %copy-start.3 = (bf16[512,128]{1,0:T(8,128)(2,1)S(1)}, bf16[512,128]{1,0:T(8,128)(2,1)}, u32[]{:S(2)}) copy-start(bf16[512,128]{1,0:T(8,128)(2,1)} %grad.3) | copy-start | bytes 393220
  0.6 38.4 %copy-start.16 = (bf16[1,128,128]{2,1,0:T(8,128)(2,1)S(1)}, bf16[1,128,128]{2,1,0:T(8,128)(2,1)}, u32[]{:S(2)}) copy-start(bf16[1,128,128]{2,1,0:T(8,128)(2,1)} %mixing.3) | copy-start | bytes 98308
  0.7 38.4 %copy-start = (bf16[512,2048]{1,0:T(8,128)(2,1)S(1)}, bf16[512,2048]{1,0:T(8,128)(2,1)}, u32[]{:S(2)}) copy-start(bf16[512,2048]{1,0:T(8,128)(2,1)} %array.1) | copy-start | bytes 6291460
  0.7 0.9 copy-start.20
  1.5 0.7 copy-start.21
  2.3 36.8 %copy-start.22 = (f32[128]{0:T(128)S(1)}, f32[128]{0:T(128)}, u32[]{:S(2)}) copy-start(f32[128]{0:T(128)} %param.10) | copy-start | bytes 1540
  42.5 0.7 copy-start.6
  43.2 0.7 copy-start.8
  43.9 0.7 copy-start.10
  44.6 0.7 copy-start.18
  45.3 17.6 %all-to-all-start.2 = ((f32[16,4,512]{2,1,0:T(4,128)}), f32[16,4,512]{2,1,0:T(4,128)S(1)}, u32[]{:S(2)}, u32[]{:S(2)}) async-start(f32[16,4,512]{2,1,0:T(4,128)} %get-tuple-element.23), calls=%async_computation.2 | async-start | bytes 262144 | tf_op jit(solution)/shard_map/all_to_all | solution.py:23
  55.8 1.6 %copy-start.1 = (bf16[512,2048]{1,0:T(8,128)(2,1)S(1)}, bf16[512,2048]{1,0:T(8,128)(2,1)}, u32[]{:S(2)}) copy-start(bf16[512,2048]{1,0:T(8,128)(2,1)} %array.1) | copy-start | bytes 6291460
  57.4 0.9 copy-start.7
  57.4 6.2 %copy-start.23 = (f32[1,128]{1,0:T(1,128)S(1)}, f32[1,128]{1,0:T(1,128)}, u32[]{:S(2)}) copy-start(f32[1,128]{1,0:T(1,128)} %bias.1) | copy-start | bytes 1540
  58.6 0.7 copy-start.12
  59.3 0.7 copy-start.14
  62.9 0.7 copy-start.4
  63.5 0.9 copy-start.5
  64.4 0.9 copy-start.9
  65.4 0.9 copy-start.11
  66.3 0.9 copy-start.13
  67.3 0.9 copy-start.15
  68.2 0.8 copy-start.17
  69.0 0.9 copy-start.19
  71.3 1.0 copy-start.2
  72.4 20.1 %all-to-all-start.3 = ((bf16[4,9,64,256]{3,2,1,0:T(8,128)(2,1)}), bf16[4,9,64,256]{3,2,1,0:T(8,128)(2,1)S(1)}, u32[]{:S(2)}, u32[]{:S(2)}) async-start(bf16[4,9,64,256]{3,2,1,0:T(8,128)(2,1)} %copy-done.2), calls=%async_computation.3 | async-start | bytes 2359296 | tf_op jit(solution)/shard_map/all_to_all | solution.py:23
  75.9 24.9 %collective-permute-start.1 = (bf16[4,8,64,256]{3,2,1,0:T(8,128)(2,1)S(1)}, bf16[4,8,64,256]{3,2,1,0:T(8,128)(2,1)S(1)}, u32[]{:S(2)}, u32[]{:S(2)}) collective-permute-start(bf16[4,8,64,256]{3,2,1,0:T(8,128)(2,1)S(1)} %all_to_all.26.weight), channel_id=1, source_target_pairs={{0,1},{1,0},{2,3},{3,2},{4,5},{5,4},{6,7},{7,6},{8,9},{9,8},{10,11... | collective-permute-start | bytes 3145736 | tf_op jit(solution)/shard_map/ppermute | solution.py:27
  93.4 44.9 %all-to-all-start.4 = ((bf16[8,2,64,256]{3,2,1,0:T(8,128)(2,1)}), bf16[8,2,64,256]{3,2,1,0:T(8,128)(2,1)S(1)}, u32[]{:S(2)}, u32[]{:S(2)}) async-start(bf16[8,2,64,256]{3,2,1,0:T(8,128)(2,1)} %shard_map.111), calls=%async_computation.4 | async-start | bytes 1048576 | tf_op jit(solution)/shard_map/all_to_all | solution.py:23
  96.9 3.9 %collective-permute-start = (bf16[512,256]{1,0:T(8,128)(2,1)S(1)}, bf16[512,256]{1,0:T(8,128)(2,1)S(1)}, u32[]{:S(2)}, u32[]{:S(2)}) collective-permute-start(bf16[512,256]{1,0:T(8,128)(2,1)S(1)} %get-tuple-element.30.joined), channel_id=1, source_target_pairs={{0,1},{1,0},{2,3},{3,2},{4,5},{5,4},{6,7},{7,6},{8,9},{9,8},{10,11... | collective-permute-start | bytes 786440 | tf_op jit(solution)/shard_map/ppermute | solution.py:27
  102.2 24.1 %collective-permute-start.2 = (bf16[512,256]{1,0:T(8,128)(2,1)S(1)}, bf16[512,256]{1,0:T(8,128)(2,1)S(1)}, u32[]{:S(2)}, u32[]{:S(2)}) collective-permute-start(bf16[512,256]{1,0:T(8,128)(2,1)S(1)} %get-tuple-element.31), channel_id=1, source_target_pairs={{0,2},{1,15},{2,4},{3,1},{4,6},{5,3},{6,8},{7,5},{8,10},{9,7},{10,... | collective-permute-start | bytes 786440 | tf_op jit(solution)/shard_map/ppermute | solution.py:36
  105.1 21.2 %collective-permute-start.3 = (bf16[512,256]{1,0:T(8,128)(2,1)S(1)}, bf16[512,256]{1,0:T(8,128)(2,1)S(1)}, u32[]{:S(2)}, u32[]{:S(2)}) collective-permute-start(bf16[512,256]{1,0:T(8,128)(2,1)S(1)} %get-tuple-element.32), channel_id=1, source_target_pairs={{0,4},{1,13},{2,6},{3,15},{4,8},{5,1},{6,10},{7,3},{8,12},{9,5},{1... | collective-permute-start | bytes 786440 | tf_op jit(solution)/shard_map/ppermute | solution.py:36
  108.0 22.0 %collective-permute-start.4 = (bf16[512,256]{1,0:T(8,128)(2,1)S(1)}, bf16[512,256]{1,0:T(8,128)(2,1)S(1)}, u32[]{:S(2)}, u32[]{:S(2)}) collective-permute-start(bf16[512,256]{1,0:T(8,128)(2,1)S(1)} %get-tuple-element.33), channel_id=1, source_target_pairs={{0,6},{1,11},{2,8},{3,13},{4,10},{5,15},{6,12},{7,1},{8,14},{9,3},... | collective-permute-start | bytes 786440 | tf_op jit(solution)/shard_map/ppermute | solution.py:36
  111.1 15.2 %collective-permute-start.5 = (bf16[512,128]{1,0:T(8,128)(2,1)S(1)}, bf16[512,128]{1,0:T(8,128)(2,1)S(1)}, u32[]{:S(2)}, u32[]{:S(2)}) collective-permute-start(bf16[512,128]{1,0:T(8,128)(2,1)S(1)} %get-tuple-element.34), channel_id=1, source_target_pairs={{0,8},{1,9},{2,10},{3,11},{4,12},{5,13},{6,14},{7,15},{8,0},{9,1},... | collective-permute-start | bytes 393224 | tf_op jit(solution)/shard_map/ppermute | solution.py:36
  130.7 6.9 %collective-permute-start.6 = (bf16[512,128]{1,0:T(8,128)(2,1)S(1)}, bf16[512,128]{1,0:T(8,128)(2,1)S(1)}, u32[]{:S(2)}, u32[]{:S(2)}) collective-permute-start(bf16[512,128]{1,0:T(8,128)(2,1)S(1)} %get-tuple-element.37), channel_id=1, source_target_pairs={{0,1},{1,0},{2,3},{3,2},{4,5},{5,4},{6,7},{7,6},{8,9},{9,8},{10,11... | collective-permute-start | bytes 393224 | tf_op jit(solution)/shard_map/ppermute | solution.py:27
where the time goes:
time: 140 us; the launch traced here: 139 us
  starting transfers between devices  43.4 us (31%)
  blocking collectives  36.7 us (26%)
  waiting for transfers between devices  32.1 us (23%)
  local copies, waits for them, and re-layouts  15.8 us (11%)
  Pallas kernels  9.46 us (7%)
    all_to_all x2, blocking collectives, exchange(): return lax.all_to_all(array, axis, split_axis=0, concat_axis=0, tiled=True)  36.7 us
    all_to_all x3, starting transfers between devices, exchange(): return lax.all_to_all(array, axis, split_axis=0, concat_axis=0, tiled=True)  17.5 us
    all_to_all x3, waiting for transfers between devices, exchange(): return lax.all_to_all(array, axis, split_axis=0, concat_axis=0, tiled=True)  17.5 us
    unnamed x48, local copies, waits for them, and re-layouts  15.7 us
    ppermute x4, starting transfers between devices, sent_apart(): return lax.ppermute(array, DP, moves)  15.2 us
    ppermute x4, waiting for transfers between devices, sent_apart(): return lax.ppermute(array, DP, moves)  12.6 us
    ppermute x3, starting transfers between devices, swapped(): return lax.ppermute(array, 'dp_1', [(0, 1), (1, 0)])  10.6 us
    pallas_call x11, Pallas kernels, run(): return made(*args)  9.46 us
  transfers between devices with their start and end apart: 10, of which 6 were waited for; matrix products, arithmetic and copies ran while one was open for 1% of the time, Pallas kernels for 3%

commit v1 on v0

--- a/solution.py
+++ b/solution.py
@@ -59,19 +59,24 @@
     return jnp.dot(a, b, preferred_element_type=f32)
 
 
-def call(body, outs, scalars=False):
+def call(body, outs, scalars=False, cold=(), free=()):
     def run(*args):
-        inside = [pltpu.VMEM] * len(args)
-        if scalars:
-            inside[0] = pltpu.SMEM
-        args = [
-            a if m is pltpu.SMEM else pltpu.with_memory_space_constraint(a, m)
-            for a, m in zip(args, inside)
-        ]
-        specs = [pl.BlockSpec(memory_space=m) for m in inside]
+        specs, operands = [], []
+        for at, array in enumerate(args):
+            if scalars and at == 0:
+                specs.append(pl.BlockSpec(memory_space=pltpu.SMEM))
+            elif at in free:
+                specs.append(pl.BlockSpec())
+            elif at in cold:
+                specs.append(pl.BlockSpec())
+                array = pltpu.with_memory_space_constraint(array, pltpu.HBM)
+            else:
+                specs.append(pl.BlockSpec(memory_space=pltpu.VMEM))
+                array = pltpu.with_memory_space_constraint(array, pltpu.VMEM)
+            operands.append(array)
         limit = pltpu.CompilerParams(vmem_limit_bytes=20 * 1024 * 1024)
         made = pl.pallas_call(body, out_shape=outs, in_specs=specs, compiler_params=limit)
-        return made(*args)
+        return made(*operands)
 
     return run
 
@@ -80,11 +85,15 @@
     return pltpu.VMEM(shape, dtype)
 
 
+def stored(shape, dtype):
+    return pltpu.HBM(shape, dtype)
+
+
 def outside(shape, dtype):
     return jax.ShapeDtypeStruct(shape, dtype)
 
 
-def project_body(hidden, weight, mixing, gain, grad, pre_out, gating_out, mixed_out, back_out, sums_out):
+def project_body(hidden, weight, mixing, gain, grad, pre_out, sums_out):
     n_x, n_z, rows, both = weight.shape
     slab = n_x * rows
     width = both // 2
@@ -94,18 +103,7 @@
         pre = term if pre is None else pre + term
     pre = pre.astype(bf16)
     pre_out[...] = pre
-    pre_content = pre[:, :width].astype(f32)
-    pre_gating = pre[:, width:].astype(f32)
-    gating = pre_gating * normal_below(pre_gating)
-    gating_out[...] = gating
-    mixed_grad = (grad[...].astype(f32) * (pre_content * normal_below(pre_content))).astype(bf16)
-    mixed_out[...] = mixed_grad
-    table = causal(mixing[0].astype(f32)).T.astype(bf16)
-    pieces = []
-    for at in range(0, mixed_grad.shape[0], BLOCK):
-        pieces.append(nn(table, mixed_grad[at : at + BLOCK]) * gain[...])
-    back = jnp.concatenate(pieces, axis=0)
-    back_out[...] = back
+    gating, _, back, _ = branches(pre, grad[...], mixing[0], gain[...])
     row = lax.broadcasted_iota(jnp.int32, (8, width), 0)
     sums = None
     for at, values in enumerate((gating, gating * gating, back, back * gating)):
@@ -116,6 +114,20 @@
         sums_out[peer] = sums[:4]
 
 
+def branches(pre, grad, mixing, gain):
+    width = grad.shape[1]
+    pre_content = pre[:, :width].astype(f32)
+    pre_gating = pre[:, width:].astype(f32)
+    gating = pre_gating * normal_below(pre_gating)
+    content = pre_content * normal_below(pre_content)
+    mixed_grad = (grad.astype(f32) * content).astype(bf16)
+    table = causal(mixing.astype(f32)).T.astype(bf16)
+    pieces = []
+    for at in range(0, mixed_grad.shape[0], BLOCK):
+        pieces.append(nn(table, mixed_grad[at : at + BLOCK]) * gain)
+    return gating, mixed_grad, jnp.concatenate(pieces, axis=0), (pre_content, pre_gating)
+
+
 def join_body(content, gating, out):
     both = jnp.concatenate([content[...], gating[...]], axis=1)
     for peer in range(out.shape[0]):
@@ -133,13 +145,11 @@
         out[at : at + step] = array[:, at : at + step].T
 
 
-def slopes_body(pre, grad, content_out, gating_out):
-    width = grad.shape[1]
-    content_out[...] = grad[...].astype(f32) * gelu_slope(pre[:, :width].astype(f32))
-    gating_out[...] = gelu_slope(pre[:, width:].astype(f32))
-
-
-def norm_body(full_width, sums, gating, mixed_grad, back, content_slope, gating_slope, mixing, bias, gain, joined_out, mixing_out):
+def norm_body(full_width, sums, pre, grad, mixing, bias, gain, joined_out, mixing_out):
+    gating, mixed_grad, back, (pre_content, pre_gating) = branches(
+        pre[...], grad[...], mixing[0], gain[...]
+    )
+    content_slope = grad[...].astype(f32) * gelu_slope(pre_content)
     total = jnp.sum(sums[...], axis=0) * (1.0 / full_width)
     row_mean = total[0:1]
     row_var = total[1:2] - row_mean * row_mean
@@ -148,7 +158,7 @@
     second = inv_std * (total[3:4] - row_mean * first)
     columns = jnp.concatenate([row_mean, inv_std, first, second] * 2, axis=0).T
     row_mean, inv_std, first, second = [columns[:, i : i + 1] for i in range(4)]
-    centred = (gating[...] - row_mean) * inv_std
+    centred = (gating - row_mean) * inv_std
     normed = (centred * gain[...]).astype(bf16)
     table = causal(mixing[0].astype(f32)).astype(bf16)
     shift = jnp.broadcast_to(bias[...], (8, BLOCK)).T[:, 0:1]
@@ -160,8 +170,8 @@
         joined_out[rows, :width] = (mixed * content_slope[rows]).astype(bf16)
         term = nt(mixed_grad[rows], normed[rows])
         mixing_grad = term if mixing_grad is None else mixing_grad + term
-    gating_back = inv_std * (back[...] - first - centred * second)
-    joined_out[:, width:] = (gating_back * gating_slope[...]).astype(bf16)
+    gating_back = inv_std * (back - first - centred * second)
+    joined_out[:, width:] = (gating_back * gelu_slope(pre_gating)).astype(bf16)
     mixing_grad = causal(mixing_grad).astype(bf16)
     half = BLOCK // 2
     mixing_out[...] = jnp.concatenate([mixing_grad[:half], mixing_grad[half:]], axis=1)
@@ -179,20 +189,39 @@
         out[x, n_z] = mixing_term[...]
 
 
-def input_terms_body(where, joined, joined_far, weight, weight_far, one, two, three, four, own):
-    n_x, _, rows, both = weight.shape
-
-    def term(x_from, n, z):
-        near = weight[pl.ds(x_from, n), pl.ds(z, 1)].reshape(n * rows, both)
-        far = weight_far[pl.ds(x_from, n), pl.ds(z, 1)].reshape(n * rows, both)
-        return nt(joined[...], near) + nt(joined_far[...], far)
-
-    three[...] = term(0, n_x, where[3]).astype(bf16)
-    two[...] = term(0, n_x, where[2]).astype(bf16)
-    one[...] = term(0, n_x, where[1]).astype(bf16)
+def term_for(joined, joined_far, weight, weight_far, x_from, n, z):
+    _, _, rows, both = weight.shape
+    near = weight[pl.ds(x_from, n), pl.ds(z, 1)].reshape(n * rows, both)
+    far = weight_far[pl.ds(x_from, n), pl.ds(z, 1)].reshape(n * rows, both)
+    return nt(joined[...], near) + nt(joined_far[...], far)
+
+
+def far_terms_body(where, joined, joined_far, weight, weight_far, three, four):
+    n_x = weight.shape[0]
     half = n_x // 2
-    four[...] = term(where[5] * half, half, where[4]).astype(bf16)
-    own[...] = term(where[5] * half, half, where[0])
+    sources = (joined, joined_far, weight, weight_far)
+    four[...] = term_for(*sources, where[5] * half, half, where[4]).astype(bf16)
+    three[...] = term_for(*sources, 0, n_x, where[3]).astype(bf16)
+
+
+def near_terms_body(where, joined, joined_far, weight, weight_far, one, two, own):
+    n_x = weight.shape[0]
+    half = n_x // 2
+    sources = (joined, joined_far, weight, weight_far)
+    one[...] = term_for(*sources, 0, n_x, where[1]).astype(bf16)
+    two[...] = term_for(*sources, 0, n_x, where[2])
+    own[...] = term_for(*sources, where[5] * half, half, where[0])
+
+
+def merge_body(where, two, three, four, out):
+    half = four.shape[1]
+    first = where[5] == 0
+    extra = four[...].astype(f32)
+    none = jnp.zeros_like(extra)
+    left = two[:, :half] + three[:, :half].astype(f32) + jnp.where(first, extra, none)
+    right = two[:, half:] + three[:, half:].astype(f32) + jnp.where(first, none, extra)
+    out[:, :half] = left.astype(bf16)
+    out[:, half:] = right.astype(bf16)
 
 
 def regroup_body(arrived, out):
@@ -218,12 +247,12 @@
     mixing_out[0, BLOCK // 2 :] = total[1][:, half:]
 
 
-def gather_body(where, one, two, three, four, own, keep_out, send_out):
+def gather_body(where, one, two, own, keep_out, send_out):
     half = own.shape[1]
-    total = one[...].astype(f32) + two[...].astype(f32) + three[...].astype(f32)
+    total = one[...].astype(f32) + two[...].astype(f32)
     first = where[5] == 0
     left, right = total[:, :half], total[:, half:]
-    keep_out[...] = own[...] + four[...].astype(f32) + jnp.where(first, left, right)
+    keep_out[...] = own[...] + jnp.where(first, left, right)
     send_out[...] = jnp.where(first, right, left).astype(bf16)
 
 
@@ -245,48 +274,51 @@
     gain = norm_gain[None, :]
 
     hidden_t = call(flip_body, like((width, tok_rows), bf16))(hidden_in)
-    shards = call(join_body, like((n_z, shard_rows, both), bf16))(content_weight, gating_weight)
+    shards = call(join_body, stored((n_z, shard_rows, both), bf16), cold=(0, 1))(
+        content_weight, gating_weight
+    )
     along_z = exchange(shards, "sp_0")
     spread = call(spread_body, like((n_x, n_z, shard_rows, both), bf16))(along_z)
     weight = exchange(spread, "sp_1")
     weight_far = swapped(weight)
 
-    tile, wide = (tok_rows, local_width), (tok_rows, both)
-    pre, gating, mixed_grad, back, sums = call(
-        project_body,
-        (like(wide, bf16), like(tile, f32), like(tile, bf16), like(tile, f32), like((n_dp, 4, tok_rows), f32)),
+    wide = (tok_rows, both)
+    pre, sums = call(
+        project_body, (stored(wide, bf16), stored((n_dp, 4, tok_rows), f32)), cold=(2,)
     )(hidden_in, weight, mixing_weight, gain, out_grad)
     sums = exchange(sums, DP)
-    content_slope, gating_slope = call(
-        slopes_body, (like(tile, f32), like(tile, f32))
-    )(pre, out_grad)
     joined, mixing_term = call(
-        functools.partial(norm_body, full_width), (like(wide, bf16), like((BLOCK // 2, both), bf16))
-    )(sums, gating, mixed_grad, back, content_slope, gating_slope, mixing_weight, mixing_bias, gain)
+        functools.partial(norm_body, full_width),
+        (like(wide, bf16), like((BLOCK // 2, both), bf16)),
+        cold=(0, 1, 3, 4, 5),
+    )(sums, pre, out_grad, mixing_weight, mixing_bias, gain)
 
     joined_far = swapped(joined)
     terms = call(
-        weight_terms_body, like((n_x, n_z + 1, shard_rows, both), bf16)
+        weight_terms_body, stored((n_x, n_z + 1, shard_rows, both), bf16)
     )(hidden_t, joined, mixing_term)
     along_x = exchange(terms, "sp_1")
 
     pair, single = (tok_rows, 2 * out_cols), (tok_rows, out_cols)
-    one, two, three, four, own = call(
-        input_terms_body,
-        (like(pair, bf16), like(pair, bf16), like(pair, bf16), like(single, bf16), like(single, f32)),
-        scalars=True,
-    )(where, joined, joined_far, weight, weight_far)
-    three = sent_apart(three, 3)
-    four = sent_apart(four, 4)
+    sources = (where, joined, joined_far, weight, weight_far)
+    three, four = call(
+        far_terms_body, (like(pair, bf16), like(single, bf16)), scalars=True
+    )(*sources)
+    four = sent_apart(four, 2)
+    three = sent_apart(three, 1)
+    one, two, own = call(
+        near_terms_body, (like(pair, bf16), like(pair, f32), like(single, f32)), scalars=True
+    )(*sources)
+    one = sent_apart(one, 1)
+    two = call(merge_body, like(pair, bf16), scalars=True)(where, two, three, four)
     two = sent_apart(two, 2)
-    one = sent_apart(one, 1)
-
-    regrouped = call(regroup_body, like((n_z, 2, shard_rows, both), bf16))(along_x)
+
+    regrouped = call(regroup_body, stored((n_z, 2, shard_rows, both), bf16))(along_x)
     arrived = exchange(regrouped, "sp_0")
 
     keep, send = call(
         gather_body, (like(single, f32), like(single, bf16)), scalars=True
-    )(where, one, two, three, four, own)
+    )(where, one, two, own)
     input_grad = (keep + swapped(send).astype(f32)).astype(bf16)
 
     content_grad, gating_grad, mixing_grad = call(

time: 140 us -> 127 us (0.907)
  the two profiles are of different devices: /device:TPU:17 before, /device:TPU:1 now
where the time goes in v1:
time: 127 us
  starting transfers between devices  38.6 us (30%)
  blocking collectives  37.7 us (30%)
  waiting for transfers between devices  30 us (24%)
  Pallas kernels  16.3 us (13%)
  local copies, waits for them, and re-layouts  2.34 us (2%)
    all_to_all x2, blocking collectives, exchange(): return lax.all_to_all(array, axis, split_axis=0, concat_axis=0, tiled=True)  37.7 us
    all_to_all x3, waiting for transfers between devices, exchange(): return lax.all_to_all(array, axis, split_axis=0, concat_axis=0, tiled=True)  19.4 us
    all_to_all x3, starting transfers between devices, exchange(): return lax.all_to_all(array, axis, split_axis=0, concat_axis=0, tiled=True)  17.6 us
    pallas_call x12, Pallas kernels, run(): return made(*operands)  16.3 us
    ppermute x3, starting transfers between devices, swapped(): return lax.ppermute(array, 'dp_1', [(0, 1), (1, 0)])  11.1 us
    ppermute x4, starting transfers between devices, sent_apart(): return lax.ppermute(array, DP, moves)  9.9 us
    ppermute x4, waiting for transfers between devices, sent_apart(): return lax.ppermute(array, DP, moves)  9.62 us
  transfers between devices with their start and end apart: 10, of which 5 were waited for; matrix products, arithmetic and copies ran while one was open for 1% of the time, Pallas kernels for 8%

profile of v1, /device:TPU:1, one launch (start us, length us, event | category | flops | bytes accessed | tf_op | source)
XLA Modules:
  0.0 126.6 jit_solution(7399741571601916488)
XLA Ops:
  0.6 0.0 copy-start.2
  0.6 0.0 copy-start
  0.7 0.0 copy-start.3
  0.7 1.6 %shard_map.102 = bf16[8,64,256]{2,1,0:T(8,128)(2,1)} custom-call(bf16[64,128]{1,0:T(8,128)(2,1)} %content.1, bf16[64,128]{1,0:T(8,128)(2,1)} %gating.1), custom_call_target="tpu_custom_call" | custom-call | tf_op jit(solution)/shard_map/pallas_call | solution.py:79
  2.3 21.3 %all_to_all.25.arrived = bf16[8,64,256]{2,1,0:T(8,128)(2,1)S(1)} all-to-all(bf16[8,64,256]{2,1,0:T(8,128)(2,1)} %shard_map.102), channel_id=1, replica_groups=mesh['sp_0'=8,'sp_1'=4,'dp_0'=8,'dp_1'=2] {'sp_0'}, dimensions={0} | all-to-all | bytes 524288 | tf_op jit(solution)/shard_map/all_to_all | solution.py:23
  23.6 0.1 shard_map.103
  23.7 16.4 %all_to_all.26.weight = bf16[4,8,64,256]{3,2,1,0:T(8,128)(2,1)S(1)} all-to-all(bf16[4,8,64,256]{3,2,1,0:T(8,128)(2,1)S(1)} %shard_map.103), channel_id=1, replica_groups=mesh['sp_0'=8,'sp_1'=4,'dp_0'=8,'dp_1'=2] {'sp_1'}, dimensions={0} | all-to-all | bytes 2097152 | tf_op jit(solution)/shard_map/all_to_all | solution.py:23
  40.1 0.0 copy-done.2
  40.1 0.0 copy-done
  40.1 0.0 copy-done.3
  40.1 4.2 %shard_map.104 = (bf16[512,256]{1,0:T(8,128)(2,1)}, f32[16,4,512]{2,1,0:T(4,128)}) custom-call(bf16[512,2048]{1,0:T(8,128)(2,1)S(1)} %copy-done, bf16[4,8,64,256]{3,2,1,0:T(8,128)(2,1)S(1)} %all_to_all.26.weight, bf16[1,128,128]{2,1,0:T(8,128)(2,1)} %mixing.3, f32[1,128]{1,0:T(1,128)S(1)} %bitcast.8, bf16[512,128]{1,0:T(8,128)(2,1)S(1)} %copy-done.2), custom_call_target="tpu_custom_call" | custom-call | tf_op jit(solution)/shard_map/pallas_call | solution.py:79
  44.3 10.6 %all-to-all-start.2 = ((f32[16,4,512]{2,1,0:T(4,128)}), f32[16,4,512]{2,1,0:T(4,128)S(1)}, u32[]{:S(2)}, u32[]{:S(2)}) async-start(f32[16,4,512]{2,1,0:T(4,128)} %get-tuple-element.18), calls=%async_computation.2 | async-start | bytes 262144 | tf_op jit(solution)/shard_map/all_to_all | solution.py:23
  54.8 2.0 %collective-permute-start.1 = (bf16[4,8,64,256]{3,2,1,0:T(8,128)(2,1)S(1)}, bf16[4,8,64,256]{3,2,1,0:T(8,128)(2,1)}, u32[]{:S(2)}, u32[]{:S(2)}) collective-permute-start(bf16[4,8,64,256]{3,2,1,0:T(8,128)(2,1)S(1)} %all_to_all.26.weight), channel_id=1, source_target_pairs={{0,1},{1,0},{2,3},{3,2},{4,5},{5,4},{6,7},{7,6},{8,9},{9,8},{10,11... | collective-permute-start | bytes 3145736 | tf_op jit(solution)/shard_map/ppermute | solution.py:27
  56.9 0.0 copy-start.1
  56.9 1.6 %copy-done.1 = bf16[512,2048]{1,0:T(8,128)(2,1)S(1)} copy-done((bf16[512,2048]{1,0:T(8,128)(2,1)S(1)}, bf16[512,2048]{1,0:T(8,128)(2,1)}, u32[]{:S(2)}) %copy-start.1) | copy-done | bytes 2097176
  58.4 0.6 shard_map.110.hidden_t
  59.1 4.7 %all-to-all-done.2.sums = f32[16,4,512]{2,1,0:T(4,128)S(1)} async-done(((f32[16,4,512]{2,1,0:T(4,128)}), f32[16,4,512]{2,1,0:T(4,128)S(1)}, u32[]{:S(2)}, u32[]{:S(2)}) %all-to-all-start.2) | async-done | bytes 131104 | tf_op jit(solution)/shard_map/all_to_all | solution.py:23
  63.7 0.0 copy-start.4
  63.7 0.7 copy-done.4
  64.4 1.7 %shard_map.105 = (bf16[512,256]{1,0:T(8,128)(2,1)S(1)}, bf16[64,256]{1,0:T(8,128)(2,1)S(1)}) custom-call(f32[16,4,512]{2,1,0:T(4,128)} %copy-done.4, bf16[512,256]{1,0:T(8,128)(2,1)} %get-tuple-element.19.pre, bf16[512,128]{1,0:T(8,128)(2,1)S(1)} %copy-done.2, bf16[1,128,128]{2,1,0:T(8,128)(2,1)} %mixing.3, f32[1,128]{1,0:T(1,128)} %bias.1, f32[1,128]{1,0:T(1,128)} %bitcast.7), custom_call_target="tpu_custom_call" | custom-call | tf_op jit(solution)/shard_map/pallas_call | solution.py:79
  66.1 1.7 %shard_map.111 = bf16[4,9,64,256]{3,2,1,0:T(8,128)(2,1)} custom-call(bf16[2048,512]{1,0:T(8,128)(2,1)S(1)} %shard_map.110.hidden_t, bf16[512,256]{1,0:T(8,128)(2,1)S(1)} %get-tuple-element.20.joined, bf16[64,256]{1,0:T(8,128)(2,1)S(1)} %get-tuple-element.28.mixing_term), custom_call_target="tpu_custom_call" | custom-call | tf_op jit(solution)/shard_map/pallas_call | solution.py:79
  67.8 3.5 %all-to-all-start.3 = ((bf16[4,9,64,256]{3,2,1,0:T(8,128)(2,1)}), bf16[4,9,64,256]{3,2,1,0:T(8,128)(2,1)S(1)}, u32[]{:S(2)}, u32[]{:S(2)}) async-start(bf16[4,9,64,256]{3,2,1,0:T(8,128)(2,1)} %shard_map.111), calls=%async_computation.3 | async-start | bytes 2359296 | tf_op jit(solution)/shard_map/all_to_all | solution.py:23
  71.4 1.9 %collective-permute-start = (bf16[512,256]{1,0:T(8,128)(2,1)S(1)}, bf16[512,256]{1,0:T(8,128)(2,1)S(1)}, u32[]{:S(2)}, u32[]{:S(2)}) collective-permute-start(bf16[512,256]{1,0:T(8,128)(2,1)S(1)} %get-tuple-element.20.joined), channel_id=1, source_target_pairs={{0,1},{1,0},{2,3},{3,2},{4,5},{5,4},{6,7},{7,6},{8,9},{9,8},{10,11... | collective-permute-start | bytes 786440 | tf_op jit(solution)/shard_map/ppermute | solution.py:27
  73.3 14.8 %all-to-all-done.3.arrived = bf16[4,9,64,256]{3,2,1,0:T(8,128)(2,1)S(1)} async-done(((bf16[4,9,64,256]{3,2,1,0:T(8,128)(2,1)}), bf16[4,9,64,256]{3,2,1,0:T(8,128)(2,1)S(1)}, u32[]{:S(2)}, u32[]{:S(2)}) %all-to-all-start.3) | async-done | bytes 1179680 | tf_op jit(solution)/shard_map/all_to_all | solution.py:23
  88.1 0.9 shard_map.112
  89.0 3.5 %all-to-all-start.4 = ((bf16[8,2,64,256]{3,2,1,0:T(8,128)(2,1)}), bf16[8,2,64,256]{3,2,1,0:T(8,128)(2,1)S(1)}, u32[]{:S(2)}, u32[]{:S(2)}) async-start(bf16[8,2,64,256]{3,2,1,0:T(8,128)(2,1)} %shard_map.112), calls=%async_computation.4 | async-start | bytes 1048576 | tf_op jit(solution)/shard_map/all_to_all | solution.py:23
  92.6 0.1 stack.27.where
  92.6 0.0 collective-permute-done.joined_far
  92.7 0.0 collective-permute-done.1.weight_far
  92.7 1.7 %shard_map.107 = (bf16[512,256]{1,0:T(8,128)(2,1)S(1)}, bf16[512,128]{1,0:T(8,128)(2,1)S(1)}) custom-call(s32[6]{0:T(128)S(1)} %stack.27.where, bf16[512,256]{1,0:T(8,128)(2,1)S(1)} %get-tuple-element.20.joined, bf16[512,256]{1,0:T(8,128)(2,1)S(1)} %collective-permute-done.joined_far, bf16[4,8,64,256]{3,2,1,0:T(8,128)(2,1)S(1)} %all_to_all.26.weight, ...), custom_call_target="tpu_custom_call" | custom-call | tf_op jit(solution)/shard_map/pallas_call | solution.py:79
  94.3 2.1 %collective-permute-start.3 = (bf16[512,256]{1,0:T(8,128)(2,1)S(1)}, bf16[512,256]{1,0:T(8,128)(2,1)S(1)}, u32[]{:S(2)}, u32[]{:S(2)}) collective-permute-start(bf16[512,256]{1,0:T(8,128)(2,1)S(1)} %get-tuple-element.23), channel_id=1, source_target_pairs={{0,2},{1,15},{2,4},{3,1},{4,6},{5,3},{6,8},{7,5},{8,10},{9,7},{10,... | collective-permute-start | bytes 786440 | tf_op jit(solution)/shard_map/ppermute | solution.py:36
  96.5 1.9 %collective-permute-start.4 = (bf16[512,128]{1,0:T(8,128)(2,1)S(1)}, bf16[512,128]{1,0:T(8,128)(2,1)S(1)}, u32[]{:S(2)}, u32[]{:S(2)}) collective-permute-start(bf16[512,128]{1,0:T(8,128)(2,1)S(1)} %get-tuple-element.24), channel_id=1, source_target_pairs={{0,4},{1,13},{2,6},{3,15},{4,8},{5,1},{6,10},{7,3},{8,12},{9,5},{1... | collective-permute-start | bytes 393224 | tf_op jit(solution)/shard_map/ppermute | solution.py:36
  98.4 1.8 %shard_map.106 = (bf16[512,256]{1,0:T(8,128)(2,1)S(1)}, f32[512,256]{1,0:T(8,128)S(1)}, f32[512,128]{1,0:T(8,128)S(1)}) custom-call(s32[6]{0:T(128)S(1)} %stack.27.where, bf16[512,256]{1,0:T(8,128)(2,1)S(1)} %get-tuple-element.20.joined, bf16[512,256]{1,0:T(8,128)(2,1)S(1)} %collective-permute-done.joined_far, ...), custom_call_target="tpu_custom_call" | custom-call | tf_op jit(solution)/shard_map/pallas_call | solution.py:79
  100.3 2.6 %collective-permute-start.2 = (bf16[512,256]{1,0:T(8,128)(2,1)S(1)}, bf16[512,256]{1,0:T(8,128)(2,1)S(1)}, u32[]{:S(2)}, u32[]{:S(2)}) collective-permute-start(bf16[512,256]{1,0:T(8,128)(2,1)S(1)} %get-tuple-element.21), channel_id=1, source_target_pairs={{0,2},{1,15},{2,4},{3,1},{4,6},{5,3},{6,8},{7,5},{8,10},{9,7},{10,... | collective-permute-start | bytes 786440 | tf_op jit(solution)/shard_map/ppermute | solution.py:36
  102.9 1.9 %collective-permute-done.4.four = bf16[512,128]{1,0:T(8,128)(2,1)S(1)} collective-permute-done((bf16[512,128]{1,0:T(8,128)(2,1)S(1)}, bf16[512,128]{1,0:T(8,128)(2,1)S(1)}, u32[]{:S(2)}, u32[]{:S(2)}) %collective-permute-start.4) | collective-permute-done | bytes 131104 | tf_op jit(solution)/shard_map/ppermute | solution.py:36
  104.8 0.0 collective-permute-done.3.three
  104.8 0.7 shard_map.108
  105.5 3.2 %collective-permute-start.5 = (bf16[512,256]{1,0:T(8,128)(2,1)S(1)}, bf16[512,256]{1,0:T(8,128)(2,1)S(1)}, u32[]{:S(2)}, u32[]{:S(2)}) collective-permute-start(bf16[512,256]{1,0:T(8,128)(2,1)S(1)} %shard_map.108), channel_id=1, source_target_pairs={{0,4},{1,13},{2,6},{3,15},{4,8},{5,1},{6,10},{7,3},{8,12},{9,5},{1... | collective-permute-start | bytes 786440 | tf_op jit(solution)/shard_map/ppermute | solution.py:36
  108.7 0.0 collective-permute-done.2.one
  108.7 7.7 %collective-permute-done.5.two = bf16[512,256]{1,0:T(8,128)(2,1)S(1)} collective-permute-done((bf16[512,256]{1,0:T(8,128)(2,1)S(1)}, bf16[512,256]{1,0:T(8,128)(2,1)S(1)}, u32[]{:S(2)}, u32[]{:S(2)}) %collective-permute-start.5) | collective-permute-done | bytes 262176 | tf_op jit(solution)/shard_map/ppermute | solution.py:36
  116.4 0.6 shard_map.109
  117.0 7.2 %collective-permute-start.6 = (bf16[512,128]{1,0:T(8,128)(2,1)S(1)}, bf16[512,128]{1,0:T(8,128)(2,1)S(1)}, u32[]{:S(2)}, u32[]{:S(2)}) collective-permute-start(bf16[512,128]{1,0:T(8,128)(2,1)S(1)} %get-tuple-element.27), channel_id=1, source_target_pairs={{0,1},{1,0},{2,3},{3,2},{4,5},{5,4},{6,7},{7,6},{8,9},{9,8},{10,11... | collective-permute-start | bytes 393224 | tf_op jit(solution)/shard_map/ppermute | solution.py:27
  124.2 1.0 collective-permute-done.6
  125.2 0.7 add_convert_fusion
  125.9 0.0 all-to-all-done.4.arrived
  125.9 0.7 shard_map.113
Async XLA Ops:
  0.6 39.4 %copy-start.2 = (bf16[512,128]{1,0:T(8,128)(2,1)S(1)}, bf16[512,128]{1,0:T(8,128)(2,1)}, u32[]{:S(2)}) copy-start(bf16[512,128]{1,0:T(8,128)(2,1)} %grad.3) | copy-start | bytes 393220
  0.6 39.4 %copy-start = (bf16[512,2048]{1,0:T(8,128)(2,1)S(1)}, bf16[512,2048]{1,0:T(8,128)(2,1)}, u32[]{:S(2)}) copy-start(bf16[512,2048]{1,0:T(8,128)(2,1)} %array.1) | copy-start | bytes 6291460
  0.7 39.4 %copy-start.3 = (f32[128]{0:T(128)S(1)}, f32[128]{0:T(128)}, u32[]{:S(2)}) copy-start(f32[128]{0:T(128)} %param.10) | copy-start | bytes 1540
  44.3 19.5 %all-to-all-start.2 = ((f32[16,4,512]{2,1,0:T(4,128)}), f32[16,4,512]{2,1,0:T(4,128)S(1)}, u32[]{:S(2)}, u32[]{:S(2)}) async-start(f32[16,4,512]{2,1,0:T(4,128)} %get-tuple-element.18), calls=%async_computation.2 | async-start | bytes 262144 | tf_op jit(solution)/shard_map/all_to_all | solution.py:23
  54.8 37.8 %collective-permute-start.1 = (bf16[4,8,64,256]{3,2,1,0:T(8,128)(2,1)S(1)}, bf16[4,8,64,256]{3,2,1,0:T(8,128)(2,1)}, u32[]{:S(2)}, u32[]{:S(2)}) collective-permute-start(bf16[4,8,64,256]{3,2,1,0:T(8,128)(2,1)S(1)} %all_to_all.26.weight), channel_id=1, source_target_pairs={{0,1},{1,0},{2,3},{3,2},{4,5},{5,4},{6,7},{7,6},{8,9},{9,8},{10,11... | collective-permute-start | bytes 3145736 | tf_op jit(solution)/shard_map/ppermute | solution.py:27
  56.9 1.6 %copy-start.1 = (bf16[512,2048]{1,0:T(8,128)(2,1)S(1)}, bf16[512,2048]{1,0:T(8,128)(2,1)}, u32[]{:S(2)}) copy-start(bf16[512,2048]{1,0:T(8,128)(2,1)} %array.1) | copy-start | bytes 6291460
  63.7 0.7 copy-start.4
  67.8 20.2 %all-to-all-start.3 = ((bf16[4,9,64,256]{3,2,1,0:T(8,128)(2,1)}), bf16[4,9,64,256]{3,2,1,0:T(8,128)(2,1)S(1)}, u32[]{:S(2)}, u32[]{:S(2)}) async-start(bf16[4,9,64,256]{3,2,1,0:T(8,128)(2,1)} %shard_map.111), calls=%async_computation.3 | async-start | bytes 2359296 | tf_op jit(solution)/shard_map/all_to_all | solution.py:23
  71.4 21.3 %collective-permute-start = (bf16[512,256]{1,0:T(8,128)(2,1)S(1)}, bf16[512,256]{1,0:T(8,128)(2,1)S(1)}, u32[]{:S(2)}, u32[]{:S(2)}) collective-permute-start(bf16[512,256]{1,0:T(8,128)(2,1)S(1)} %get-tuple-element.20.joined), channel_id=1, source_target_pairs={{0,1},{1,0},{2,3},{3,2},{4,5},{5,4},{6,7},{7,6},{8,9},{9,8},{10,11... | collective-permute-start | bytes 786440 | tf_op jit(solution)/shard_map/ppermute | solution.py:27
  89.0 36.9 %all-to-all-start.4 = ((bf16[8,2,64,256]{3,2,1,0:T(8,128)(2,1)}), bf16[8,2,64,256]{3,2,1,0:T(8,128)(2,1)S(1)}, u32[]{:S(2)}, u32[]{:S(2)}) async-start(bf16[8,2,64,256]{3,2,1,0:T(8,128)(2,1)} %shard_map.112), calls=%async_computation.4 | async-start | bytes 1048576 | tf_op jit(solution)/shard_map/all_to_all | solution.py:23
  94.3 10.5 %collective-permute-start.3 = (bf16[512,256]{1,0:T(8,128)(2,1)S(1)}, bf16[512,256]{1,0:T(8,128)(2,1)S(1)}, u32[]{:S(2)}, u32[]{:S(2)}) collective-permute-start(bf16[512,256]{1,0:T(8,128)(2,1)S(1)} %get-tuple-element.23), channel_id=1, source_target_pairs={{0,2},{1,15},{2,4},{3,1},{4,6},{5,3},{6,8},{7,5},{8,10},{9,7},{10,... | collective-permute-start | bytes 786440 | tf_op jit(solution)/shard_map/ppermute | solution.py:36
  96.5 8.3 %collective-permute-start.4 = (bf16[512,128]{1,0:T(8,128)(2,1)S(1)}, bf16[512,128]{1,0:T(8,128)(2,1)S(1)}, u32[]{:S(2)}, u32[]{:S(2)}) collective-permute-start(bf16[512,128]{1,0:T(8,128)(2,1)S(1)} %get-tuple-element.24), channel_id=1, source_target_pairs={{0,4},{1,13},{2,6},{3,15},{4,8},{5,1},{6,10},{7,3},{8,12},{9,5},{1... | collective-permute-start | bytes 393224 | tf_op jit(solution)/shard_map/ppermute | solution.py:36
  100.3 8.4 %collective-permute-start.2 = (bf16[512,256]{1,0:T(8,128)(2,1)S(1)}, bf16[512,256]{1,0:T(8,128)(2,1)S(1)}, u32[]{:S(2)}, u32[]{:S(2)}) collective-permute-start(bf16[512,256]{1,0:T(8,128)(2,1)S(1)} %get-tuple-element.21), channel_id=1, source_target_pairs={{0,2},{1,15},{2,4},{3,1},{4,6},{5,3},{6,8},{7,5},{8,10},{9,7},{10,... | collective-permute-start | bytes 786440 | tf_op jit(solution)/shard_map/ppermute | solution.py:36
  105.5 10.9 %collective-permute-start.5 = (bf16[512,256]{1,0:T(8,128)(2,1)S(1)}, bf16[512,256]{1,0:T(8,128)(2,1)S(1)}, u32[]{:S(2)}, u32[]{:S(2)}) collective-permute-start(bf16[512,256]{1,0:T(8,128)(2,1)S(1)} %shard_map.108), channel_id=1, source_target_pairs={{0,4},{1,13},{2,6},{3,15},{4,8},{5,1},{6,10},{7,3},{8,12},{9,5},{1... | collective-permute-start | bytes 786440 | tf_op jit(solution)/shard_map/ppermute | solution.py:36
  117.0 8.1 %collective-permute-start.6 = (bf16[512,128]{1,0:T(8,128)(2,1)S(1)}, bf16[512,128]{1,0:T(8,128)(2,1)S(1)}, u32[]{:S(2)}, u32[]{:S(2)}) collective-permute-start(bf16[512,128]{1,0:T(8,128)(2,1)S(1)} %get-tuple-element.27), channel_id=1, source_target_pairs={{0,1},{1,0},{2,3},{3,2},{4,5},{5,4},{6,7},{7,6},{8,9},{9,8},{10,11... | collective-permute-start | bytes 393224 | tf_op jit(solution)/shard_map/ppermute | solution.py:27

commit v2 on v1

--- a/solution.py
+++ b/solution.py
@@ -196,30 +196,25 @@
     return nt(joined[...], near) + nt(joined_far[...], far)
 
 
-def far_terms_body(where, joined, joined_far, weight, weight_far, three, four):
+def input_terms_body(where, joined, joined_far, weight, weight_far, four, odd, two, own):
     n_x = weight.shape[0]
     half = n_x // 2
+    width = two.shape[1]
     sources = (joined, joined_far, weight, weight_far)
     four[...] = term_for(*sources, where[5] * half, half, where[4]).astype(bf16)
-    three[...] = term_for(*sources, 0, n_x, where[3]).astype(bf16)
-
-
-def near_terms_body(where, joined, joined_far, weight, weight_far, one, two, own):
-    n_x = weight.shape[0]
-    half = n_x // 2
-    sources = (joined, joined_far, weight, weight_far)
-    one[...] = term_for(*sources, 0, n_x, where[1]).astype(bf16)
+    odd[:, :width] = term_for(*sources, 0, n_x, where[3]).astype(bf16)
+    odd[:, width:] = term_for(*sources, 0, n_x, where[1]).astype(bf16)
     two[...] = term_for(*sources, 0, n_x, where[2])
     own[...] = term_for(*sources, where[5] * half, half, where[0])
 
 
-def merge_body(where, two, three, four, out):
+def merge_body(where, two, odd, four, out):
     half = four.shape[1]
     first = where[5] == 0
     extra = four[...].astype(f32)
     none = jnp.zeros_like(extra)
-    left = two[:, :half] + three[:, :half].astype(f32) + jnp.where(first, extra, none)
-    right = two[:, half:] + three[:, half:].astype(f32) + jnp.where(first, none, extra)
+    left = two[:, :half] + odd[:, :half].astype(f32) + jnp.where(first, extra, none)
+    right = two[:, half:] + odd[:, half : 2 * half].astype(f32) + jnp.where(first, none, extra)
     out[:, :half] = left.astype(bf16)
     out[:, half:] = right.astype(bf16)
 
@@ -247,9 +242,9 @@
     mixing_out[0, BLOCK // 2 :] = total[1][:, half:]
 
 
-def gather_body(where, one, two, own, keep_out, send_out):
+def gather_body(where, odd, two, own, keep_out, send_out):
     half = own.shape[1]
-    total = one[...].astype(f32) + two[...].astype(f32)
+    total = odd[:, 2 * half :].astype(f32) + two[...].astype(f32)
     first = where[5] == 0
     left, right = total[:, :half], total[:, half:]
     keep_out[...] = own[...] + jnp.where(first, left, right)
@@ -299,18 +294,17 @@
     )(hidden_t, joined, mixing_term)
     along_x = exchange(terms, "sp_1")
 
-    pair, single = (tok_rows, 2 * out_cols), (tok_rows, out_cols)
+    single, pair = (tok_rows, out_cols), (tok_rows, 2 * out_cols)
+    wide_pair = (tok_rows, 4 * out_cols)
     sources = (where, joined, joined_far, weight, weight_far)
-    three, four = call(
-        far_terms_body, (like(pair, bf16), like(single, bf16)), scalars=True
+    four, odd, two, own = call(
+        input_terms_body,
+        (like(single, bf16), like(wide_pair, bf16), like(pair, f32), like(single, f32)),
+        scalars=True,
     )(*sources)
     four = sent_apart(four, 2)
-    three = sent_apart(three, 1)
-    one, two, own = call(
-        near_terms_body, (like(pair, bf16), like(pair, f32), like(single, f32)), scalars=True
-    )(*sources)
-    one = sent_apart(one, 1)
-    two = call(merge_body, like(pair, bf16), scalars=True)(where, two, three, four)
+    odd = sent_apart(odd, 1)
+    two = call(merge_body, like(pair, bf16), scalars=True)(where, two, odd, four)
     two = sent_apart(two, 2)
 
     regrouped = call(regroup_body, stored((n_z, 2, shard_rows, both), bf16))(along_x)
@@ -318,7 +312,7 @@
 
     keep, send = call(
         gather_body, (like(single, f32), like(single, bf16)), scalars=True
-    )(where, one, two, own)
+    )(where, odd, two, own)
     input_grad = (keep + swapped(send).astype(f32)).astype(bf16)
 
     content_grad, gating_grad, mixing_grad = call(

time: 127 us -> 125 us (0.984)
  starting transfers between devices: 38.6 us -> 36.3 us
  local copies, waits for them, and re-layouts: 2.34 us -> 3.99 us
  waiting for transfers between devices: 30 us -> 28.7 us
    all_to_all x3, waiting for transfers between devices: 19.4 us -> 13.7 us  [exchange(): return lax.all_to_all(array, axis, split_axis=0, concat_axis=0, tiled=True)]
    ppermute x3, starting transfers between devices: 11.1 us -> 14.9 us  [swapped(): return lax.ppermute(array, 'dp_1', [(0, 1), (1, 0)])]
    all_to_all x3, starting transfers between devices: 17.6 us -> 14.2 us  [exchange(): return lax.all_to_all(array, axis, split_axis=0, concat_axis=0, tiled=True)]
    ppermute x4 -> x3, waiting for transfers between devices: 9.62 us -> 12.7 us  [sent_apart(): return lax.ppermute(array, DP, moves)]
    ppermute x4 -> x3, starting transfers between devices: 9.9 us -> 7.19 us  [sent_apart(): return lax.ppermute(array, DP, moves)]
    unnamed x10 -> x14, local copies, waits for them, and re-layouts: 2.26 us -> 3.91 us
    ppermute x3, waiting for transfers between devices: 0.97 us -> 2.33 us  [swapped(): return lax.ppermute(array, 'dp_1', [(0, 1), (1, 0)])]
    pallas_call x12 -> x11, Pallas kernels: 16.3 us -> 15.5 us  [run(): return made(*operands)]
  transfers between devices with their start and end apart: 10 -> 9, of which waited for: 5 -> 6; matrix products, arithmetic and copies ran while one was open for 1% -> 1% of each run, Pallas kernels for 8% -> 11%
where the time goes in v2:
time: 125 us; the launch traced here: 124 us
  blocking collectives  37.7 us (30%)
  starting transfers between devices  36.3 us (29%)
  waiting for transfers between devices  28.7 us (23%)
  Pallas kernels  15.5 us (12%)
  local copies, waits for them, and re-layouts  3.99 us (3%)
    all_to_all x2, blocking collectives, exchange(): return lax.all_to_all(array, axis, split_axis=0, concat_axis=0, tiled=True)  37.7 us
    pallas_call x11, Pallas kernels, run(): return made(*operands)  15.5 us
    ppermute x3, starting transfers between devices, swapped(): return lax.ppermute(array, 'dp_1', [(0, 1), (1, 0)])  14.9 us
    all_to_all x3, starting transfers between devices, exchange(): return lax.all_to_all(array, axis, split_axis=0, concat_axis=0, tiled=True)  14.2 us
    all_to_all x3, waiting for transfers between devices, exchange(): return lax.all_to_all(array, axis, split_axis=0, concat_axis=0, tiled=True)  13.7 us
    ppermute x3, waiting for transfers between devices, sent_apart(): return lax.ppermute(array, DP, moves)  12.7 us
    ppermute x3, starting transfers between devices, sent_apart(): return lax.ppermute(array, DP, moves)  7.19 us
    unnamed x14, local copies, waits for them, and re-layouts  3.91 us
  transfers between devices with their start and end apart: 9, of which 6 were waited for; matrix products, arithmetic and copies ran while one was open for 1% of the time, Pallas kernels for 11%

profile of v2, /device:TPU:1, one launch (start us, length us, event | category | flops | bytes accessed | tf_op | source)
XLA Modules:
  0.0 123.7 jit_solution(14691402281765908563)
XLA Ops:
  0.6 0.0 copy-start.2
  0.6 0.0 copy-start
  0.7 0.0 copy-start.5
  0.7 1.6 %shard_map.102 = bf16[8,64,256]{2,1,0:T(8,128)(2,1)} custom-call(bf16[64,128]{1,0:T(8,128)(2,1)} %content.1, bf16[64,128]{1,0:T(8,128)(2,1)} %gating.1), custom_call_target="tpu_custom_call" | custom-call | tf_op jit(solution)/shard_map/pallas_call | solution.py:79
  2.3 21.3 %all_to_all.25.arrived = bf16[8,64,256]{2,1,0:T(8,128)(2,1)S(1)} all-to-all(bf16[8,64,256]{2,1,0:T(8,128)(2,1)} %shard_map.102), channel_id=1, replica_groups=mesh['sp_0'=8,'sp_1'=4,'dp_0'=8,'dp_1'=2] {'sp_0'}, dimensions={0} | all-to-all | bytes 524288 | tf_op jit(solution)/shard_map/all_to_all | solution.py:23
  23.6 0.1 shard_map.103
  23.7 16.4 %all_to_all.26.weight = bf16[4,8,64,256]{3,2,1,0:T(8,128)(2,1)S(1)} all-to-all(bf16[4,8,64,256]{3,2,1,0:T(8,128)(2,1)S(1)} %shard_map.103), channel_id=1, replica_groups=mesh['sp_0'=8,'sp_1'=4,'dp_0'=8,'dp_1'=2] {'sp_1'}, dimensions={0} | all-to-all | bytes 2097152 | tf_op jit(solution)/shard_map/all_to_all | solution.py:23
  40.1 5.4 %collective-permute-start.1 = (bf16[4,8,64,256]{3,2,1,0:T(8,128)(2,1)S(1)}, bf16[4,8,64,256]{3,2,1,0:T(8,128)(2,1)}, u32[]{:S(2)}, u32[]{:S(2)}) collective-permute-start(bf16[4,8,64,256]{3,2,1,0:T(8,128)(2,1)S(1)} %all_to_all.26.weight), channel_id=1, source_target_pairs={{0,1},{1,0},{2,3},{3,2},{4,5},{5,4},{6,7},{7,6},{8,9},{9,8},{10,11... | collective-permute-start | bytes 3145736 | tf_op jit(solution)/shard_map/ppermute | solution.py:27
  45.5 0.0 copy-done.2
  45.5 0.0 copy-done
  45.5 0.0 copy-done.5
  45.5 4.2 %shard_map.104 = (bf16[512,256]{1,0:T(8,128)(2,1)}, f32[16,4,512]{2,1,0:T(4,128)}) custom-call(bf16[512,2048]{1,0:T(8,128)(2,1)S(1)} %copy-done, bf16[4,8,64,256]{3,2,1,0:T(8,128)(2,1)S(1)} %all_to_all.26.weight, bf16[1,128,128]{2,1,0:T(8,128)(2,1)} %mixing.3, f32[1,128]{1,0:T(1,128)S(1)} %bitcast.8, bf16[512,128]{1,0:T(8,128)(2,1)S(1)} %copy-done.2), custom_call_target="tpu_custom_call" | custom-call | tf_op jit(solution)/shard_map/pallas_call | solution.py:79
  49.6 7.2 %all-to-all-start.2 = ((f32[16,4,512]{2,1,0:T(4,128)}), f32[16,4,512]{2,1,0:T(4,128)S(1)}, u32[]{:S(2)}, u32[]{:S(2)}) async-start(f32[16,4,512]{2,1,0:T(4,128)} %get-tuple-element.17), calls=%async_computation.2 | async-start | bytes 262144 | tf_op jit(solution)/shard_map/all_to_all | solution.py:23
  56.9 0.0 copy-start.1
  56.9 1.6 %copy-done.1 = bf16[512,2048]{1,0:T(8,128)(2,1)S(1)} copy-done((bf16[512,2048]{1,0:T(8,128)(2,1)S(1)}, bf16[512,2048]{1,0:T(8,128)(2,1)}, u32[]{:S(2)}) %copy-start.1) | copy-done | bytes 2097176
  58.5 0.6 shard_map.109.hidden_t
  59.1 6.7 %all-to-all-done.2.sums = f32[16,4,512]{2,1,0:T(4,128)S(1)} async-done(((f32[16,4,512]{2,1,0:T(4,128)}), f32[16,4,512]{2,1,0:T(4,128)S(1)}, u32[]{:S(2)}, u32[]{:S(2)}) %all-to-all-start.2) | async-done | bytes 131104 | tf_op jit(solution)/shard_map/all_to_all | solution.py:23
  65.8 0.0 copy-start.6
  65.8 0.7 copy-done.6
  66.4 1.7 %shard_map.105 = (bf16[512,256]{1,0:T(8,128)(2,1)S(1)}, bf16[64,256]{1,0:T(8,128)(2,1)S(1)}) custom-call(f32[16,4,512]{2,1,0:T(4,128)} %copy-done.6, bf16[512,256]{1,0:T(8,128)(2,1)} %get-tuple-element.18.pre, bf16[512,128]{1,0:T(8,128)(2,1)S(1)} %copy-done.2, bf16[1,128,128]{2,1,0:T(8,128)(2,1)} %mixing.3, f32[1,128]{1,0:T(1,128)} %bias.1, f32[1,128]{1,0:T(1,128)} %bitcast.7), custom_call_target="tpu_custom_call" | custom-call | tf_op jit(solution)/shard_map/pallas_call | solution.py:79
  68.1 1.7 %shard_map.110 = bf16[4,9,64,256]{3,2,1,0:T(8,128)(2,1)} custom-call(bf16[2048,512]{1,0:T(8,128)(2,1)S(1)} %shard_map.109.hidden_t, bf16[512,256]{1,0:T(8,128)(2,1)S(1)} %get-tuple-element.19.joined, bf16[64,256]{1,0:T(8,128)(2,1)S(1)} %get-tuple-element.26.mixing_term), custom_call_target="tpu_custom_call" | custom-call | tf_op jit(solution)/shard_map/pallas_call | solution.py:79
  69.9 3.5 %all-to-all-start.3 = ((bf16[4,9,64,256]{3,2,1,0:T(8,128)(2,1)}), bf16[4,9,64,256]{3,2,1,0:T(8,128)(2,1)S(1)}, u32[]{:S(2)}, u32[]{:S(2)}) async-start(bf16[4,9,64,256]{3,2,1,0:T(8,128)(2,1)} %shard_map.110), calls=%async_computation.3 | async-start | bytes 2359296 | tf_op jit(solution)/shard_map/all_to_all | solution.py:23
  73.4 1.9 %collective-permute-start = (bf16[512,256]{1,0:T(8,128)(2,1)S(1)}, bf16[512,256]{1,0:T(8,128)(2,1)S(1)}, u32[]{:S(2)}, u32[]{:S(2)}) collective-permute-start(bf16[512,256]{1,0:T(8,128)(2,1)S(1)} %get-tuple-element.19.joined), channel_id=1, source_target_pairs={{0,1},{1,0},{2,3},{3,2},{4,5},{5,4},{6,7},{7,6},{8,9},{9,8},{10,11... | collective-permute-start | bytes 786440 | tf_op jit(solution)/shard_map/ppermute | solution.py:27
  75.4 0.1 stack.27.where
  75.5 1.4 %collective-permute-done.joined_far = bf16[512,256]{1,0:T(8,128)(2,1)S(1)} collective-permute-done((bf16[512,256]{1,0:T(8,128)(2,1)S(1)}, bf16[512,256]{1,0:T(8,128)(2,1)S(1)}, u32[]{:S(2)}, u32[]{:S(2)}) %collective-permute-start) | collective-permute-done | bytes 262176 | tf_op jit(solution)/shard_map/ppermute | solution.py:27
  76.8 0.0 copy-start.3
  76.8 0.7 copy-done.3
  77.5 0.0 collective-permute-done.1.weight_far
  77.5 0.0 copy-start.4
  77.5 0.9 copy-done.4
  78.5 2.6 %shard_map.106 = (bf16[512,128]{1,0:T(8,128)(2,1)S(1)}, bf16[512,512]{1,0:T(8,128)(2,1)}, f32[512,256]{1,0:T(8,128)S(1)}, f32[512,128]{1,0:T(8,128)S(1)}) custom-call(s32[6]{0:T(128)S(1)} %stack.27.where, bf16[512,256]{1,0:T(8,128)(2,1)S(1)} %get-tuple-element.19.joined, bf16[512,256]{1,0:T(8,128)(2,1)S(1)} %copy-done.4, ...), custom_call_target="tpu_custom_call" | custom-call | tf_op jit(solution)/shard_map/pallas_call | solution.py:79
  81.1 2.0 %collective-permute-start.2 = (bf16[512,512]{1,0:T(8,128)(2,1)}, bf16[512,512]{1,0:T(8,128)(2,1)S(1)}, u32[]{:S(2)}, u32[]{:S(2)}) collective-permute-start(bf16[512,512]{1,0:T(8,128)(2,1)} %get-tuple-element.20), channel_id=1, source_target_pairs={{0,2},{1,15},{2,4},{3,1},{4,6},{5,3},{6,8},{7,5},{8,10},{9,7},{10,... | collective-permute-start | bytes 1572872 | tf_op jit(solution)/shard_map/ppermute | solution.py:36
  83.1 7.0 %all-to-all-done.3.arrived = bf16[4,9,64,256]{3,2,1,0:T(8,128)(2,1)S(1)} async-done(((bf16[4,9,64,256]{3,2,1,0:T(8,128)(2,1)}), bf16[4,9,64,256]{3,2,1,0:T(8,128)(2,1)S(1)}, u32[]{:S(2)}, u32[]{:S(2)}) %all-to-all-start.3) | async-done | bytes 1179680 | tf_op jit(solution)/shard_map/all_to_all | solution.py:23
  90.1 0.9 shard_map.111
  91.0 3.5 %all-to-all-start.4 = ((bf16[8,2,64,256]{3,2,1,0:T(8,128)(2,1)}), bf16[8,2,64,256]{3,2,1,0:T(8,128)(2,1)S(1)}, u32[]{:S(2)}, u32[]{:S(2)}) async-start(bf16[8,2,64,256]{3,2,1,0:T(8,128)(2,1)} %shard_map.111), calls=%async_computation.4 | async-start | bytes 1048576 | tf_op jit(solution)/shard_map/all_to_all | solution.py:23
  94.5 2.0 %collective-permute-start.3 = (bf16[512,128]{1,0:T(8,128)(2,1)S(1)}, bf16[512,128]{1,0:T(8,128)(2,1)S(1)}, u32[]{:S(2)}, u32[]{:S(2)}) collective-permute-start(bf16[512,128]{1,0:T(8,128)(2,1)S(1)} %get-tuple-element.22), channel_id=1, source_target_pairs={{0,4},{1,13},{2,6},{3,15},{4,8},{5,1},{6,10},{7,3},{8,12},{9,5},{1... | collective-permute-start | bytes 393224 | tf_op jit(solution)/shard_map/ppermute | solution.py:36
  96.5 6.2 %collective-permute-done.3.four = bf16[512,128]{1,0:T(8,128)(2,1)S(1)} collective-permute-done((bf16[512,128]{1,0:T(8,128)(2,1)S(1)}, bf16[512,128]{1,0:T(8,128)(2,1)S(1)}, u32[]{:S(2)}, u32[]{:S(2)}) %collective-permute-start.3) | collective-permute-done | bytes 131104 | tf_op jit(solution)/shard_map/ppermute | solution.py:36
  102.7 0.0 collective-permute-done.2.odd
  102.8 0.7 shard_map.107
  103.4 3.3 %collective-permute-start.4 = (bf16[512,256]{1,0:T(8,128)(2,1)S(1)}, bf16[512,256]{1,0:T(8,128)(2,1)S(1)}, u32[]{:S(2)}, u32[]{:S(2)}) collective-permute-start(bf16[512,256]{1,0:T(8,128)(2,1)S(1)} %shard_map.107), channel_id=1, source_target_pairs={{0,4},{1,13},{2,6},{3,15},{4,8},{5,1},{6,10},{7,3},{8,12},{9,5},{1... | collective-permute-start | bytes 786440 | tf_op jit(solution)/shard_map/ppermute | solution.py:36
  106.7 6.4 %collective-permute-done.4.two = bf16[512,256]{1,0:T(8,128)(2,1)S(1)} collective-permute-done((bf16[512,256]{1,0:T(8,128)(2,1)S(1)}, bf16[512,256]{1,0:T(8,128)(2,1)S(1)}, u32[]{:S(2)}, u32[]{:S(2)}) %collective-permute-start.4) | collective-permute-done | bytes 262176 | tf_op jit(solution)/shard_map/ppermute | solution.py:36
  113.1 0.7 shard_map.108
  113.8 7.6 %collective-permute-start.5 = (bf16[512,128]{1,0:T(8,128)(2,1)S(1)}, bf16[512,128]{1,0:T(8,128)(2,1)S(1)}, u32[]{:S(2)}, u32[]{:S(2)}) collective-permute-start(bf16[512,128]{1,0:T(8,128)(2,1)S(1)} %get-tuple-element.25), channel_id=1, source_target_pairs={{0,1},{1,0},{2,3},{3,2},{4,5},{5,4},{6,7},{7,6},{8,9},{9,8},{10,11... | collective-permute-start | bytes 393224 | tf_op jit(solution)/shard_map/ppermute | solution.py:27
  121.4 1.0 collective-permute-done.5
  122.4 0.7 add_convert_fusion
  123.0 0.0 all-to-all-done.4.arrived
  123.0 0.7 shard_map.112
Async XLA Ops:
  0.6 44.8 %copy-start.2 = (bf16[512,128]{1,0:T(8,128)(2,1)S(1)}, bf16[512,128]{1,0:T(8,128)(2,1)}, u32[]{:S(2)}) copy-start(bf16[512,128]{1,0:T(8,128)(2,1)} %grad.3) | copy-start | bytes 393220
  0.6 44.8 %copy-start = (bf16[512,2048]{1,0:T(8,128)(2,1)S(1)}, bf16[512,2048]{1,0:T(8,128)(2,1)}, u32[]{:S(2)}) copy-start(bf16[512,2048]{1,0:T(8,128)(2,1)} %array.1) | copy-start | bytes 6291460
  0.7 44.8 %copy-start.5 = (f32[128]{0:T(128)S(1)}, f32[128]{0:T(128)}, u32[]{:S(2)}) copy-start(f32[128]{0:T(128)} %param.10) | copy-start | bytes 1540
  40.1 37.5 %collective-permute-start.1 = (bf16[4,8,64,256]{3,2,1,0:T(8,128)(2,1)S(1)}, bf16[4,8,64,256]{3,2,1,0:T(8,128)(2,1)}, u32[]{:S(2)}, u32[]{:S(2)}) collective-permute-start(bf16[4,8,64,256]{3,2,1,0:T(8,128)(2,1)S(1)} %all_to_all.26.weight), channel_id=1, source_target_pairs={{0,1},{1,0},{2,3},{3,2},{4,5},{5,4},{6,7},{7,6},{8,9},{9,8},{10,11... | collective-permute-start | bytes 3145736 | tf_op jit(solution)/shard_map/ppermute | solution.py:27
  49.6 16.1 %all-to-all-start.2 = ((f32[16,4,512]{2,1,0:T(4,128)}), f32[16,4,512]{2,1,0:T(4,128)S(1)}, u32[]{:S(2)}, u32[]{:S(2)}) async-start(f32[16,4,512]{2,1,0:T(4,128)} %get-tuple-element.17), calls=%async_computation.2 | async-start | bytes 262144 | tf_op jit(solution)/shard_map/all_to_all | solution.py:23
  56.9 1.6 %copy-start.1 = (bf16[512,2048]{1,0:T(8,128)(2,1)S(1)}, bf16[512,2048]{1,0:T(8,128)(2,1)}, u32[]{:S(2)}) copy-start(bf16[512,2048]{1,0:T(8,128)(2,1)} %array.1) | copy-start | bytes 6291460
  65.8 0.7 copy-start.6
  69.9 20.2 %all-to-all-start.3 = ((bf16[4,9,64,256]{3,2,1,0:T(8,128)(2,1)}), bf16[4,9,64,256]{3,2,1,0:T(8,128)(2,1)S(1)}, u32[]{:S(2)}, u32[]{:S(2)}) async-start(bf16[4,9,64,256]{3,2,1,0:T(8,128)(2,1)} %shard_map.110), calls=%async_computation.3 | async-start | bytes 2359296 | tf_op jit(solution)/shard_map/all_to_all | solution.py:23
  73.4 3.4 %collective-permute-start = (bf16[512,256]{1,0:T(8,128)(2,1)S(1)}, bf16[512,256]{1,0:T(8,128)(2,1)S(1)}, u32[]{:S(2)}, u32[]{:S(2)}) collective-permute-start(bf16[512,256]{1,0:T(8,128)(2,1)S(1)} %get-tuple-element.19.joined), channel_id=1, source_target_pairs={{0,1},{1,0},{2,3},{3,2},{4,5},{5,4},{6,7},{7,6},{8,9},{9,8},{10,11... | collective-permute-start | bytes 786440 | tf_op jit(solution)/shard_map/ppermute | solution.py:27
  76.8 0.7 copy-start.3
  77.5 1.0 copy-start.4
  81.1 21.6 %collective-permute-start.2 = (bf16[512,512]{1,0:T(8,128)(2,1)}, bf16[512,512]{1,0:T(8,128)(2,1)S(1)}, u32[]{:S(2)}, u32[]{:S(2)}) collective-permute-start(bf16[512,512]{1,0:T(8,128)(2,1)} %get-tuple-element.20), channel_id=1, source_target_pairs={{0,2},{1,15},{2,4},{3,1},{4,6},{5,3},{6,8},{7,5},{8,10},{9,7},{10,... | collective-permute-start | bytes 1572872 | tf_op jit(solution)/shard_map/ppermute | solution.py:36
  91.0 32.0 %all-to-all-start.4 = ((bf16[8,2,64,256]{3,2,1,0:T(8,128)(2,1)}), bf16[8,2,64,256]{3,2,1,0:T(8,128)(2,1)S(1)}, u32[]{:S(2)}, u32[]{:S(2)}) async-start(bf16[8,2,64,256]{3,2,1,0:T(8,128)(2,1)} %shard_map.111), calls=%async_computation.4 | async-start | bytes 1048576 | tf_op jit(solution)/shard_map/all_to_all | solution.py:23
  94.5 8.2 %collective-permute-start.3 = (bf16[512,128]{1,0:T(8,128)(2,1)S(1)}, bf16[512,128]{1,0:T(8,128)(2,1)S(1)}, u32[]{:S(2)}, u32[]{:S(2)}) collective-permute-start(bf16[512,128]{1,0:T(8,128)(2,1)S(1)} %get-tuple-element.22), channel_id=1, source_target_pairs={{0,4},{1,13},{2,6},{3,15},{4,8},{5,1},{6,10},{7,3},{8,12},{9,5},{1... | collective-permute-start | bytes 393224 | tf_op jit(solution)/shard_map/ppermute | solution.py:36
  103.4 9.7 %collective-permute-start.4 = (bf16[512,256]{1,0:T(8,128)(2,1)S(1)}, bf16[512,256]{1,0:T(8,128)(2,1)S(1)}, u32[]{:S(2)}, u32[]{:S(2)}) collective-permute-start(bf16[512,256]{1,0:T(8,128)(2,1)S(1)} %shard_map.107), channel_id=1, source_target_pairs={{0,4},{1,13},{2,6},{3,15},{4,8},{5,1},{6,10},{7,3},{8,12},{9,5},{1... | collective-permute-start | bytes 786440 | tf_op jit(solution)/shard_map/ppermute | solution.py:36
  113.8 8.6 %collective-permute-start.5 = (bf16[512,128]{1,0:T(8,128)(2,1)S(1)}, bf16[512,128]{1,0:T(8,128)(2,1)S(1)}, u32[]{:S(2)}, u32[]{:S(2)}) collective-permute-start(bf16[512,128]{1,0:T(8,128)(2,1)S(1)} %get-tuple-element.25), channel_id=1, source_target_pairs={{0,1},{1,0},{2,3},{3,2},{4,5},{5,4},{6,7},{7,6},{8,9},{9,8},{10,11... | collective-permute-start | bytes 393224 | tf_op jit(solution)/shard_map/ppermute | solution.py:27

commit v3 on v2

--- a/solution.py
+++ b/solution.py
@@ -96,35 +96,33 @@
 def project_body(hidden, weight, mixing, gain, grad, pre_out, sums_out):
     n_x, n_z, rows, both = weight.shape
     slab = n_x * rows
-    width = both // 2
     pre = None
     for z in range(n_z):
         term = nn(hidden[:, z * slab : (z + 1) * slab], weight[:, z].reshape(slab, both))
         pre = term if pre is None else pre + term
     pre = pre.astype(bf16)
     pre_out[...] = pre
-    gating, _, back, _ = branches(pre, grad[...], mixing[0], gain[...])
-    row = lax.broadcasted_iota(jnp.int32, (8, width), 0)
-    sums = None
+    flipped = causal(mixing[0].astype(f32)).T.astype(bf16)
+    gating, _, back, _ = branches(pre, grad[...], flipped, gain[...])
+    lane = lax.broadcasted_iota(jnp.int32, gating.shape, 1)
+    sums = jnp.zeros_like(gating)
     for at, values in enumerate((gating, gating * gating, back, back * gating)):
-        pick = jnp.where(row == at, 1.0, 0.0).astype(f32)
-        term = nt(pick, values, precision=lax.Precision.HIGHEST)
-        sums = term if sums is None else sums + term
+        sums = jnp.where(lane == at, jnp.sum(values, axis=1, keepdims=True), sums)
+    sums = sums.T
     for peer in range(sums_out.shape[0]):
         sums_out[peer] = sums[:4]
 
 
-def branches(pre, grad, mixing, gain):
+def branches(pre, grad, flipped, gain):
     width = grad.shape[1]
     pre_content = pre[:, :width].astype(f32)
     pre_gating = pre[:, width:].astype(f32)
     gating = pre_gating * normal_below(pre_gating)
     content = pre_content * normal_below(pre_content)
     mixed_grad = (grad.astype(f32) * content).astype(bf16)
-    table = causal(mixing.astype(f32)).T.astype(bf16)
     pieces = []
     for at in range(0, mixed_grad.shape[0], BLOCK):
-        pieces.append(nn(table, mixed_grad[at : at + BLOCK]) * gain)
+        pieces.append(nn(flipped, mixed_grad[at : at + BLOCK]) * gain)
     return gating, mixed_grad, jnp.concatenate(pieces, axis=0), (pre_content, pre_gating)
 
 
@@ -145,9 +143,9 @@
         out[at : at + step] = array[:, at : at + step].T
 
 
-def norm_body(full_width, sums, pre, grad, mixing, bias, gain, joined_out, mixing_out):
+def norm_body(full_width, sums, pre, grad, table, flipped, bias, gain, joined_out, mixing_out):
     gating, mixed_grad, back, (pre_content, pre_gating) = branches(
-        pre[...], grad[...], mixing[0], gain[...]
+        pre[...], grad[...], flipped[...], gain[...]
     )
     content_slope = grad[...].astype(f32) * gelu_slope(pre_content)
     total = jnp.sum(sums[...], axis=0) * (1.0 / full_width)
@@ -160,13 +158,12 @@
     row_mean, inv_std, first, second = [columns[:, i : i + 1] for i in range(4)]
     centred = (gating - row_mean) * inv_std
     normed = (centred * gain[...]).astype(bf16)
-    table = causal(mixing[0].astype(f32)).astype(bf16)
     shift = jnp.broadcast_to(bias[...], (8, BLOCK)).T[:, 0:1]
     width = normed.shape[1]
     mixing_grad = None
     for at in range(0, normed.shape[0], BLOCK):
         rows = slice(at, at + BLOCK)
-        mixed = nn(table, normed[rows]) + shift
+        mixed = nn(table[...], normed[rows]) + shift
         joined_out[rows, :width] = (mixed * content_slope[rows]).astype(bf16)
         term = nt(mixed_grad[rows], normed[rows])
         mixing_grad = term if mixing_grad is None else mixing_grad + term
@@ -178,39 +175,77 @@
 
 
 def weight_terms_body(hidden_t, joined, mixing_term, out):
-    n_x, n_all, rows, _ = out.shape
-    n_z = n_all - 1
-    slab = n_x * rows
-    for z in range(n_z):
-        term = nn(hidden_t[z * slab : (z + 1) * slab], joined[...]).astype(bf16)
+    n_x, _, rows, _ = out.shape
+    step, last = pl.program_id(0), pl.num_programs(0) - 1
+
+    @pl.when(step < last)
+    def _():
+        term = nn(hidden_t[...], joined[...]).astype(bf16)
         for x in range(n_x):
-            out[x, z] = term[x * rows : (x + 1) * rows]
-    for x in range(n_x):
-        out[x, n_z] = mixing_term[...]
-
-
-def term_for(joined, joined_far, weight, weight_far, x_from, n, z):
-    _, _, rows, both = weight.shape
-    near = weight[pl.ds(x_from, n), pl.ds(z, 1)].reshape(n * rows, both)
-    far = weight_far[pl.ds(x_from, n), pl.ds(z, 1)].reshape(n * rows, both)
-    return nt(joined[...], near) + nt(joined_far[...], far)
-
-
-def input_terms_body(where, joined, joined_far, weight, weight_far, four, odd, two, own):
-    n_x = weight.shape[0]
+            out[x, 0] = term[x * rows : (x + 1) * rows]
+
+    @pl.when(step == last)
+    def _():
+        for x in range(n_x):
+            out[x, 0] = mixing_term[...]
+
+
+def weight_terms(hidden_t, joined, mixing_term, n_x, n_z):
+    tokens, both = joined.shape
+    slab = hidden_t.shape[0] // n_z
+    inside = pl.BlockSpec(memory_space=pltpu.VMEM)
+    return pl.pallas_call(
+        weight_terms_body,
+        grid=(n_z + 1,),
+        out_shape=stored((n_x, n_z + 1, slab // n_x, both), bf16),
+        in_specs=[
+            pl.BlockSpec((slab, tokens), lambda z: (jnp.minimum(z, n_z - 1), 0)),
+            inside,
+            inside,
+        ],
+        out_specs=pl.BlockSpec((n_x, 1, slab // n_x, both), lambda z: (0, z, 0, 0)),
+        compiler_params=pltpu.CompilerParams(vmem_limit_bytes=20 * 1024 * 1024),
+        name="weight_terms",
+    )(
+        pltpu.with_memory_space_constraint(hidden_t, pltpu.HBM),
+        pltpu.with_memory_space_constraint(joined, pltpu.VMEM),
+        pltpu.with_memory_space_constraint(mixing_term, pltpu.VMEM),
+    )
+
+
+def pick_body(where, weight, mixing, mine_out, theirs_out, table_out, flipped_out):
+    table = causal(mixing[0].astype(f32))
+    table_out[...] = table.astype(bf16)
+    flipped_out[...] = table.T.astype(bf16)
+    n_x, _, rows, both = weight.shape
     half = n_x // 2
-    width = two.shape[1]
-    sources = (joined, joined_far, weight, weight_far)
-    four[...] = term_for(*sources, where[5] * half, half, where[4]).astype(bf16)
-    odd[:, :width] = term_for(*sources, 0, n_x, where[3]).astype(bf16)
-    odd[:, width:] = term_for(*sources, 0, n_x, where[1]).astype(bf16)
-    two[...] = term_for(*sources, 0, n_x, where[2])
-    own[...] = term_for(*sources, where[5] * half, half, where[0])
+    for out, base, core in ((mine_out, 0, where[10]), (theirs_out, 5, 1 - where[10])):
+        at = 0
+        for step in (3, 1, 2):
+            block = weight[:, pl.ds(where[base + step], 1)].reshape(n_x * rows, both)
+            out[at : at + n_x * rows] = block
+            at += n_x * rows
+        for step in (4, 0):
+            block = weight[pl.ds(core * half, half), pl.ds(where[base + step], 1)]
+            out[at : at + half * rows] = block.reshape(half * rows, both)
+            at += half * rows
+
+
+def input_terms_body(joined, joined_far, mine, far, odd, two, four, own):
+    def term(at, n):
+        rows = slice(at, at + n)
+        return nt(joined[...], mine[rows]) + nt(joined_far[...], far[rows])
+
+    single, pair = own.shape[1], two.shape[1]
+    odd[...] = term(0, 2 * pair).astype(bf16)
+    four[...] = term(3 * pair, single).astype(bf16)
+    two[...] = term(2 * pair, pair)
+    own[...] = term(3 * pair + single, single)
 
 
 def merge_body(where, two, odd, four, out):
     half = four.shape[1]
-    first = where[5] == 0
+    first = where[10] == 0
     extra = four[...].astype(f32)
     none = jnp.zeros_like(extra)
     left = two[:, :half] + odd[:, :half].astype(f32) + jnp.where(first, extra, none)
@@ -245,7 +280,7 @@
 def gather_body(where, odd, two, own, keep_out, send_out):
     half = own.shape[1]
     total = odd[:, 2 * half :].astype(f32) + two[...].astype(f32)
-    first = where[5] == 0
+    first = where[10] == 0
     left, right = total[:, :half], total[:, half:]
     keep_out[...] = own[...] + jnp.where(first, left, right)
     send_out[...] = jnp.where(first, right, left).astype(bf16)
@@ -265,43 +300,43 @@
     grad_scale = 1.0 / math.sqrt(tok_rows * n_sp)
     here, core = lax.axis_index("dp_0"), lax.axis_index("dp_1")
     side = 1 - 2 * core
-    where = jnp.stack([(here + side * k + ring) % ring for k in range(5)] + [core]).astype(jnp.int32)
+    ahead = [(here + side * k + ring) % ring for k in range(5)]
+    behind = [(here - side * k + ring) % ring for k in range(5)]
+    where = jnp.stack(ahead + behind + [core]).astype(jnp.int32)
     gain = norm_gain[None, :]
 
-    hidden_t = call(flip_body, like((width, tok_rows), bf16))(hidden_in)
+    hidden_t = call(flip_body, stored((width, tok_rows), bf16))(hidden_in)
     shards = call(join_body, stored((n_z, shard_rows, both), bf16), cold=(0, 1))(
         content_weight, gating_weight
     )
     along_z = exchange(shards, "sp_0")
     spread = call(spread_body, like((n_x, n_z, shard_rows, both), bf16))(along_z)
     weight = exchange(spread, "sp_1")
-    weight_far = swapped(weight)
+    single, pair = (tok_rows, out_cols), (tok_rows, 2 * out_cols)
+    wide_pair, picked = (tok_rows, 4 * out_cols), (width // 2, both)
+    square = like((BLOCK, BLOCK), bf16)
+    mine, theirs, table, flipped = call(
+        pick_body, (like(picked, bf16), like(picked, bf16), square, square), scalars=True, cold=(2,)
+    )(where, weight, mixing_weight)
+    far = swapped(theirs)
 
     wide = (tok_rows, both)
     pre, sums = call(
-        project_body, (stored(wide, bf16), stored((n_dp, 4, tok_rows), f32)), cold=(2,)
+        project_body, (like(wide, bf16), stored((n_dp, 4, tok_rows), f32))
     )(hidden_in, weight, mixing_weight, gain, out_grad)
     sums = exchange(sums, DP)
     joined, mixing_term = call(
-        functools.partial(norm_body, full_width),
-        (like(wide, bf16), like((BLOCK // 2, both), bf16)),
-        cold=(0, 1, 3, 4, 5),
-    )(sums, pre, out_grad, mixing_weight, mixing_bias, gain)
+        functools.partial(norm_body, full_width), (like(wide, bf16), like((BLOCK // 2, both), bf16))
+    )(sums, pre, out_grad, table, flipped, mixing_bias, gain)
 
     joined_far = swapped(joined)
-    terms = call(
-        weight_terms_body, stored((n_x, n_z + 1, shard_rows, both), bf16)
-    )(hidden_t, joined, mixing_term)
+    terms = weight_terms(hidden_t, joined, mixing_term, n_x, n_z)
     along_x = exchange(terms, "sp_1")
 
-    single, pair = (tok_rows, out_cols), (tok_rows, 2 * out_cols)
-    wide_pair = (tok_rows, 4 * out_cols)
-    sources = (where, joined, joined_far, weight, weight_far)
-    four, odd, two, own = call(
+    odd, two, four, own = call(
         input_terms_body,
-        (like(single, bf16), like(wide_pair, bf16), like(pair, f32), like(single, f32)),
-        scalars=True,
-    )(*sources)
+        (like(wide_pair, bf16), like(pair, f32), like(single, bf16), like(single, f32)),
+    )(joined, joined_far, mine, far)
     four = sent_apart(four, 2)
     odd = sent_apart(odd, 1)
     two = call(merge_body, like(pair, bf16), scalars=True)(where, two, odd, four)

time: 125 us -> 125 us (level)
  local copies, waits for them, and re-layouts: 3.99 us -> 1.76 us
  Pallas kernels: 15.5 us -> 17.2 us
    pallas_call x0 -> x1, Pallas kernels: none -> 6.32 us  [weight_terms(): pl.pallas_call(weight_terms_body, grid=(n_z + 1,), out_shape=stored((n_x,...]
    pallas_call x11, Pallas kernels: 15.5 us -> 10.9 us  [run(): return made(*operands)]
    all_to_all x3, starting transfers between devices: 14.2 us -> 17.6 us  [exchange(): return lax.all_to_all(array, axis, split_axis=0, concat_axis=0, tiled=True)]
    ppermute x3, starting transfers between devices: 14.9 us -> 12 us  [swapped(): return lax.ppermute(array, 'dp_1', [(0, 1), (1, 0)])]
    unnamed x14, local copies, waits for them, and re-layouts: 3.91 us -> 1.67 us
  transfers between devices with their start and end apart: 9 -> 9, of which waited for: 6 -> 6; matrix products, arithmetic and copies ran while one was open for 1% -> 1% of each run, Pallas kernels for 11% -> 5%
where the time goes in v3:
time: 125 us; the launch traced here: 124 us
  blocking collectives  37.7 us (30%)
  starting transfers between devices  36.7 us (29%)
  waiting for transfers between devices  29.1 us (23%)
  Pallas kernels  17.2 us (14%)
  local copies, waits for them, and re-layouts  1.76 us (1%)
    all_to_all x2, blocking collectives, exchange(): return lax.all_to_all(array, axis, split_axis=0, concat_axis=0, tiled=True)  37.7 us
    all_to_all x3, starting transfers between devices, exchange(): return lax.all_to_all(array, axis, split_axis=0, concat_axis=0, tiled=True)  17.6 us
    all_to_all x3, waiting for transfers between devices, exchange(): return lax.all_to_all(array, axis, split_axis=0, concat_axis=0, tiled=True)  14.3 us
    ppermute x3, waiting for transfers between devices, sent_apart(): return lax.ppermute(array, DP, moves)  12.6 us
    ppermute x3, starting transfers between devices, swapped(): return lax.ppermute(array, 'dp_1', [(0, 1), (1, 0)])  12 us
    pallas_call x11, Pallas kernels, run(): return made(*operands)  10.9 us
    ppermute x3, starting transfers between devices, sent_apart(): return lax.ppermute(array, DP, moves)  7.19 us
    pallas_call x1, Pallas kernels, weight_terms(): pl.pallas_call(weight_terms_body, grid=(n_z + 1,), out_shape=stored((n_x,...  6.32 us
  transfers between devices with their start and end apart: 9, of which 6 were waited for; matrix products, arithmetic and copies ran while one was open for 1% of the time, Pallas kernels for 5%

profile of v3, /device:TPU:1, one launch (start us, length us, event | category | flops | bytes accessed | tf_op | source)
XLA Modules:
  0.0 124.0 jit_solution(1528157975190597258)
XLA Ops:
  0.6 0.0 copy-start.1
  0.6 0.0 copy-start.4
  0.7 0.0 copy-start
  0.7 0.0 copy-start.5
  0.7 1.6 %shard_map.102 = bf16[8,64,256]{2,1,0:T(8,128)(2,1)} custom-call(bf16[64,128]{1,0:T(8,128)(2,1)} %content.1, bf16[64,128]{1,0:T(8,128)(2,1)} %gating.1), custom_call_target="tpu_custom_call" | custom-call | tf_op jit(solution)/shard_map/pallas_call | solution.py:79
  2.3 21.3 %all_to_all.25.arrived = bf16[8,64,256]{2,1,0:T(8,128)(2,1)S(1)} all-to-all(bf16[8,64,256]{2,1,0:T(8,128)(2,1)} %shard_map.102), channel_id=1, replica_groups=mesh['sp_0'=8,'sp_1'=4,'dp_0'=8,'dp_1'=2] {'sp_0'}, dimensions={0} | all-to-all | bytes 524288 | tf_op jit(solution)/shard_map/all_to_all | solution.py:23
  23.6 0.1 shard_map.103
  23.7 16.4 %all_to_all.26.weight = bf16[4,8,64,256]{3,2,1,0:T(8,128)(2,1)S(1)} all-to-all(bf16[4,8,64,256]{3,2,1,0:T(8,128)(2,1)S(1)} %shard_map.103), channel_id=1, replica_groups=mesh['sp_0'=8,'sp_1'=4,'dp_0'=8,'dp_1'=2] {'sp_1'}, dimensions={0} | all-to-all | bytes 2097152 | tf_op jit(solution)/shard_map/all_to_all | solution.py:23
  40.1 0.0 copy-done.1
  40.1 0.0 copy-done.4
  40.1 0.0 copy-done
  40.1 0.0 copy-done.5
  40.1 1.8 %shard_map.104 = (bf16[512,256]{1,0:T(8,128)(2,1)S(1)}, f32[16,4,512]{2,1,0:T(4,128)}) custom-call(bf16[512,2048]{1,0:T(8,128)(2,1)S(1)} %copy-done, bf16[4,8,64,256]{3,2,1,0:T(8,128)(2,1)S(1)} %all_to_all.26.weight, bf16[1,128,128]{2,1,0:T(8,128)(2,1)S(1)} %copy-done.4, f32[1,128]{1,0:T(1,128)S(1)} %bitcast.11, bf16[512,128]{1,0:T(8,128)(2,1)S(1)} %copy-done.1), custom_call_target="tpu_custom_call" | custom-call | tf_op jit(solution)/shard_map/pallas_call | solution.py:79
  42.0 0.0 copy-start.2
  42.0 0.7 copy-done.2
  42.7 10.6 %all-to-all-start.2 = ((f32[16,4,512]{2,1,0:T(4,128)}), f32[16,4,512]{2,1,0:T(4,128)S(1)}, u32[]{:S(2)}, u32[]{:S(2)}) async-start(f32[16,4,512]{2,1,0:T(4,128)} %get-tuple-element.21), calls=%async_computation.2 | async-start | bytes 262144 | tf_op jit(solution)/shard_map/all_to_all | solution.py:23
  53.2 0.0 copy-start.6
  53.3 1.9 %shard_map.110.hidden_t = bf16[2048,512]{1,0:T(8,128)(2,1)} custom-call(bf16[512,2048]{1,0:T(8,128)(2,1)S(1)} %copy-done), custom_call_target="tpu_custom_call" | custom-call | tf_op jit(solution)/shard_map/pallas_call | solution.py:79
  55.2 0.1 stack.44.where
  55.3 0.9 shard_map.105
  56.2 6.0 %all-to-all-done.2.sums = f32[16,4,512]{2,1,0:T(4,128)S(1)} async-done(((f32[16,4,512]{2,1,0:T(4,128)}), f32[16,4,512]{2,1,0:T(4,128)S(1)}, u32[]{:S(2)}, u32[]{:S(2)}) %all-to-all-start.2) | async-done | bytes 131104 | tf_op jit(solution)/shard_map/all_to_all | solution.py:23
  62.1 0.0 copy-done.6
  62.1 0.0 copy-start.3
  62.1 0.9 copy-done.3
  63.1 0.7 shard_map.106
  63.8 6.3 %weight_terms.1 = bf16[4,9,64,256]{3,2,1,0:T(8,128)(2,1)} custom-call(bf16[2048,512]{1,0:T(8,128)(2,1)} %shard_map.110.hidden_t, bf16[512,256]{1,0:T(8,128)(2,1)S(1)} %get-tuple-element.25.joined, bf16[64,256]{1,0:T(8,128)(2,1)S(1)} %get-tuple-element.34.mixing_term), custom_call_target="tpu_custom_call" | custom-call | tf_op jit(solution)/shard_map/weight_terms/pallas_call | solution.py:197
  70.1 3.5 %all-to-all-start.3 = ((bf16[4,9,64,256]{3,2,1,0:T(8,128)(2,1)}), bf16[4,9,64,256]{3,2,1,0:T(8,128)(2,1)S(1)}, u32[]{:S(2)}, u32[]{:S(2)}) async-start(bf16[4,9,64,256]{3,2,1,0:T(8,128)(2,1)} %weight_terms.1), calls=%async_computation.3 | async-start | bytes 2359296 | tf_op jit(solution)/shard_map/all_to_all | solution.py:23
  73.7 1.9 %collective-permute-start.1 = (bf16[1024,256]{1,0:T(8,128)(2,1)S(1)}, bf16[1024,256]{1,0:T(8,128)(2,1)S(1)}, u32[]{:S(2)}, u32[]{:S(2)}) collective-permute-start(bf16[1024,256]{1,0:T(8,128)(2,1)S(1)} %get-tuple-element.27), channel_id=1, source_target_pairs={{0,1},{1,0},{2,3},{3,2},{4,5},{5,4},{6,7},{7,6},{8,9},{9,8},{10,11... | collective-permute-start | bytes 1572872 | tf_op jit(solution)/shard_map/ppermute | solution.py:27
  75.6 2.4 %collective-permute-start = (bf16[512,256]{1,0:T(8,128)(2,1)S(1)}, bf16[512,256]{1,0:T(8,128)(2,1)S(1)}, u32[]{:S(2)}, u32[]{:S(2)}) collective-permute-start(bf16[512,256]{1,0:T(8,128)(2,1)S(1)} %get-tuple-element.25.joined), channel_id=1, source_target_pairs={{0,1},{1,0},{2,3},{3,2},{4,5},{5,4},{6,7},{7,6},{8,9},{9,8},{10,11... | collective-permute-start | bytes 786440 | tf_op jit(solution)/shard_map/ppermute | solution.py:27
  78.0 1.1 collective-permute-done.joined_far
  79.2 0.0 collective-permute-done.1.far
  79.2 0.9 shard_map.107
  80.0 2.0 %collective-permute-start.2 = (bf16[512,512]{1,0:T(8,128)(2,1)S(1)}, bf16[512,512]{1,0:T(8,128)(2,1)S(1)}, u32[]{:S(2)}, u32[]{:S(2)}) collective-permute-start(bf16[512,512]{1,0:T(8,128)(2,1)S(1)} %get-tuple-element.28), channel_id=1, source_target_pairs={{0,2},{1,15},{2,4},{3,1},{4,6},{5,3},{6,8},{7,5},{8,10},{9,7},{10,... | collective-permute-start | bytes 1572872 | tf_op jit(solution)/shard_map/ppermute | solution.py:36
  82.0 8.4 %all-to-all-done.3.arrived = bf16[4,9,64,256]{3,2,1,0:T(8,128)(2,1)S(1)} async-done(((bf16[4,9,64,256]{3,2,1,0:T(8,128)(2,1)}), bf16[4,9,64,256]{3,2,1,0:T(8,128)(2,1)S(1)}, u32[]{:S(2)}, u32[]{:S(2)}) %all-to-all-start.3) | async-done | bytes 1179680 | tf_op jit(solution)/shard_map/all_to_all | solution.py:23
  90.4 1.0 shard_map.111
  91.3 3.5 %all-to-all-start.4 = ((bf16[8,2,64,256]{3,2,1,0:T(8,128)(2,1)}), bf16[8,2,64,256]{3,2,1,0:T(8,128)(2,1)S(1)}, u32[]{:S(2)}, u32[]{:S(2)}) async-start(bf16[8,2,64,256]{3,2,1,0:T(8,128)(2,1)} %shard_map.111), calls=%async_computation.4 | async-start | bytes 1048576 | tf_op jit(solution)/shard_map/all_to_all | solution.py:23
  94.8 1.9 %collective-permute-start.3 = (bf16[512,128]{1,0:T(8,128)(2,1)S(1)}, bf16[512,128]{1,0:T(8,128)(2,1)S(1)}, u32[]{:S(2)}, u32[]{:S(2)}) collective-permute-start(bf16[512,128]{1,0:T(8,128)(2,1)S(1)} %get-tuple-element.30), channel_id=1, source_target_pairs={{0,4},{1,13},{2,6},{3,15},{4,8},{5,1},{6,10},{7,3},{8,12},{9,5},{1... | collective-permute-start | bytes 393224 | tf_op jit(solution)/shard_map/ppermute | solution.py:36
  96.8 6.2 %collective-permute-done.3.four = bf16[512,128]{1,0:T(8,128)(2,1)S(1)} collective-permute-done((bf16[512,128]{1,0:T(8,128)(2,1)S(1)}, bf16[512,128]{1,0:T(8,128)(2,1)S(1)}, u32[]{:S(2)}, u32[]{:S(2)}) %collective-permute-start.3) | collective-permute-done | bytes 131104 | tf_op jit(solution)/shard_map/ppermute | solution.py:36
  103.0 0.0 collective-permute-done.2.odd
  103.0 0.6 shard_map.108
  103.7 3.3 %collective-permute-start.4 = (bf16[512,256]{1,0:T(8,128)(2,1)S(1)}, bf16[512,256]{1,0:T(8,128)(2,1)S(1)}, u32[]{:S(2)}, u32[]{:S(2)}) collective-permute-start(bf16[512,256]{1,0:T(8,128)(2,1)S(1)} %shard_map.108), channel_id=1, source_target_pairs={{0,4},{1,13},{2,6},{3,15},{4,8},{5,1},{6,10},{7,3},{8,12},{9,5},{1... | collective-permute-start | bytes 786440 | tf_op jit(solution)/shard_map/ppermute | solution.py:36
  107.0 6.4 %collective-permute-done.4.two = bf16[512,256]{1,0:T(8,128)(2,1)S(1)} collective-permute-done((bf16[512,256]{1,0:T(8,128)(2,1)S(1)}, bf16[512,256]{1,0:T(8,128)(2,1)S(1)}, u32[]{:S(2)}, u32[]{:S(2)}) %collective-permute-start.4) | collective-permute-done | bytes 262176 | tf_op jit(solution)/shard_map/ppermute | solution.py:36
  113.4 0.6 shard_map.109
  114.0 7.6 %collective-permute-start.5 = (bf16[512,128]{1,0:T(8,128)(2,1)S(1)}, bf16[512,128]{1,0:T(8,128)(2,1)S(1)}, u32[]{:S(2)}, u32[]{:S(2)}) collective-permute-start(bf16[512,128]{1,0:T(8,128)(2,1)S(1)} %get-tuple-element.33), channel_id=1, source_target_pairs={{0,1},{1,0},{2,3},{3,2},{4,5},{5,4},{6,7},{7,6},{8,9},{9,8},{10,11... | collective-permute-start | bytes 393224 | tf_op jit(solution)/shard_map/ppermute | solution.py:27
  121.6 1.0 collective-permute-done.5
  122.6 0.7 add_convert_fusion
  123.3 0.0 all-to-all-done.4.arrived
  123.3 0.7 shard_map.112
Async XLA Ops:
  0.6 39.5 %copy-start.1 = (bf16[512,128]{1,0:T(8,128)(2,1)S(1)}, bf16[512,128]{1,0:T(8,128)(2,1)}, u32[]{:S(2)}) copy-start(bf16[512,128]{1,0:T(8,128)(2,1)} %grad.3) | copy-start | bytes 393220
  0.6 39.5 %copy-start.4 = (bf16[1,128,128]{2,1,0:T(8,128)(2,1)S(1)}, bf16[1,128,128]{2,1,0:T(8,128)(2,1)}, u32[]{:S(2)}) copy-start(bf16[1,128,128]{2,1,0:T(8,128)(2,1)} %mixing.3) | copy-start | bytes 98308
  0.7 39.5 %copy-start = (bf16[512,2048]{1,0:T(8,128)(2,1)S(1)}, bf16[512,2048]{1,0:T(8,128)(2,1)}, u32[]{:S(2)}) copy-start(bf16[512,2048]{1,0:T(8,128)(2,1)} %array.1) | copy-start | bytes 6291460
  0.7 39.5 %copy-start.5 = (f32[128]{0:T(128)S(1)}, f32[128]{0:T(128)}, u32[]{:S(2)}) copy-start(f32[128]{0:T(128)} %param.10) | copy-start | bytes 1540
  42.0 0.7 copy-start.2
  42.7 19.5 %all-to-all-start.2 = ((f32[16,4,512]{2,1,0:T(4,128)}), f32[16,4,512]{2,1,0:T(4,128)S(1)}, u32[]{:S(2)}, u32[]{:S(2)}) async-start(f32[16,4,512]{2,1,0:T(4,128)} %get-tuple-element.21), calls=%async_computation.2 | async-start | bytes 262144 | tf_op jit(solution)/shard_map/all_to_all | solution.py:23
  53.2 8.9 %copy-start.6 = (f32[1,128]{1,0:T(1,128)S(1)}, f32[1,128]{1,0:T(1,128)}, u32[]{:S(2)}) copy-start(f32[1,128]{1,0:T(1,128)} %bias.1) | copy-start | bytes 1540
  62.1 1.0 copy-start.3
  70.1 20.2 %all-to-all-start.3 = ((bf16[4,9,64,256]{3,2,1,0:T(8,128)(2,1)}), bf16[4,9,64,256]{3,2,1,0:T(8,128)(2,1)S(1)}, u32[]{:S(2)}, u32[]{:S(2)}) async-start(bf16[4,9,64,256]{3,2,1,0:T(8,128)(2,1)} %weight_terms.1), calls=%async_computation.3 | async-start | bytes 2359296 | tf_op jit(solution)/shard_map/all_to_all | solution.py:23
  73.7 5.5 %collective-permute-start.1 = (bf16[1024,256]{1,0:T(8,128)(2,1)S(1)}, bf16[1024,256]{1,0:T(8,128)(2,1)S(1)}, u32[]{:S(2)}, u32[]{:S(2)}) collective-permute-start(bf16[1024,256]{1,0:T(8,128)(2,1)S(1)} %get-tuple-element.27), channel_id=1, source_target_pairs={{0,1},{1,0},{2,3},{3,2},{4,5},{5,4},{6,7},{7,6},{8,9},{9,8},{10,11... | collective-permute-start | bytes 1572872 | tf_op jit(solution)/shard_map/ppermute | solution.py:27
  75.6 3.6 %collective-permute-start = (bf16[512,256]{1,0:T(8,128)(2,1)S(1)}, bf16[512,256]{1,0:T(8,128)(2,1)S(1)}, u32[]{:S(2)}, u32[]{:S(2)}) collective-permute-start(bf16[512,256]{1,0:T(8,128)(2,1)S(1)} %get-tuple-element.25.joined), channel_id=1, source_target_pairs={{0,1},{1,0},{2,3},{3,2},{4,5},{5,4},{6,7},{7,6},{8,9},{9,8},{10,11... | collective-permute-start | bytes 786440 | tf_op jit(solution)/shard_map/ppermute | solution.py:27
  80.0 23.0 %collective-permute-start.2 = (bf16[512,512]{1,0:T(8,128)(2,1)S(1)}, bf16[512,512]{1,0:T(8,128)(2,1)S(1)}, u32[]{:S(2)}, u32[]{:S(2)}) collective-permute-start(bf16[512,512]{1,0:T(8,128)(2,1)S(1)} %get-tuple-element.28), channel_id=1, source_target_pairs={{0,2},{1,15},{2,4},{3,1},{4,6},{5,3},{6,8},{7,5},{8,10},{9,7},{10,... | collective-permute-start | bytes 1572872 | tf_op jit(solution)/shard_map/ppermute | solution.py:36
  91.3 32.0 %all-to-all-start.4 = ((bf16[8,2,64,256]{3,2,1,0:T(8,128)(2,1)}), bf16[8,2,64,256]{3,2,1,0:T(8,128)(2,1)S(1)}, u32[]{:S(2)}, u32[]{:S(2)}) async-start(bf16[8,2,64,256]{3,2,1,0:T(8,128)(2,1)} %shard_map.111), calls=%async_computation.4 | async-start | bytes 1048576 | tf_op jit(solution)/shard_map/all_to_all | solution.py:23
  94.8 8.2 %collective-permute-start.3 = (bf16[512,128]{1,0:T(8,128)(2,1)S(1)}, bf16[512,128]{1,0:T(8,128)(2,1)S(1)}, u32[]{:S(2)}, u32[]{:S(2)}) collective-permute-start(bf16[512,128]{1,0:T(8,128)(2,1)S(1)} %get-tuple-element.30), channel_id=1, source_target_pairs={{0,4},{1,13},{2,6},{3,15},{4,8},{5,1},{6,10},{7,3},{8,12},{9,5},{1... | collective-permute-start | bytes 393224 | tf_op jit(solution)/shard_map/ppermute | solution.py:36
  103.7 9.7 %collective-permute-start.4 = (bf16[512,256]{1,0:T(8,128)(2,1)S(1)}, bf16[512,256]{1,0:T(8,128)(2,1)S(1)}, u32[]{:S(2)}, u32[]{:S(2)}) collective-permute-start(bf16[512,256]{1,0:T(8,128)(2,1)S(1)} %shard_map.108), channel_id=1, source_target_pairs={{0,4},{1,13},{2,6},{3,15},{4,8},{5,1},{6,10},{7,3},{8,12},{9,5},{1... | collective-permute-start | bytes 786440 | tf_op jit(solution)/shard_map/ppermute | solution.py:36
  114.0 8.6 %collective-permute-start.5 = (bf16[512,128]{1,0:T(8,128)(2,1)S(1)}, bf16[512,128]{1,0:T(8,128)(2,1)S(1)}, u32[]{:S(2)}, u32[]{:S(2)}) collective-permute-start(bf16[512,128]{1,0:T(8,128)(2,1)S(1)} %get-tuple-element.33), channel_id=1, source_target_pairs={{0,1},{1,0},{2,3},{3,2},{4,5},{5,4},{6,7},{7,6},{8,9},{9,8},{10,11... | collective-permute-start | bytes 393224 | tf_op jit(solution)/shard_map/ppermute | solution.py:27

commit v4 on v3

--- a/solution.py
+++ b/solution.py
@@ -174,36 +174,46 @@
     mixing_out[...] = jnp.concatenate([mixing_grad[:half], mixing_grad[half:]], axis=1)
 
 
-def weight_terms_body(hidden_t, joined, mixing_term, out):
-    n_x, _, rows, _ = out.shape
-    step, last = pl.program_id(0), pl.num_programs(0) - 1
-
-    @pl.when(step < last)
-    def _():
-        term = nn(hidden_t[...], joined[...]).astype(bf16)
-        for x in range(n_x):
-            out[x, 0] = term[x * rows : (x + 1) * rows]
-
-    @pl.when(step == last)
-    def _():
-        for x in range(n_x):
-            out[x, 0] = mixing_term[...]
+def weight_terms_body(hidden_t, joined, mixing_term, out, held, made, come, gone):
+    n_x, n_all, rows, both = out.shape
+    n_z = n_all - 1
+    slab = n_x * rows
+    loads = [
+        pltpu.make_async_copy(hidden_t.at[pl.ds(z * slab, slab)], held.at[z], come.at[z])
+        for z in range(n_z)
+    ]
+    stores = [
+        pltpu.make_async_copy(made.at[z], out.at[:, z], gone.at[z]) for z in range(n_all)
+    ]
+    for load in loads:
+        load.start()
+    for x in range(n_x):
+        made[n_z, x] = mixing_term[...]
+    stores[n_z].start()
+    for z in range(n_z):
+        loads[z].wait()
+        made[z] = nn(held[z], joined[...]).astype(bf16).reshape(n_x, rows, both)
+        stores[z].start()
+    for store in stores:
+        store.wait()
 
 
 def weight_terms(hidden_t, joined, mixing_term, n_x, n_z):
     tokens, both = joined.shape
     slab = hidden_t.shape[0] // n_z
-    inside = pl.BlockSpec(memory_space=pltpu.VMEM)
+    rows = slab // n_x
+    near, far = pl.BlockSpec(memory_space=pltpu.VMEM), pl.BlockSpec(memory_space=pl.ANY)
     return pl.pallas_call(
         weight_terms_body,
-        grid=(n_z + 1,),
-        out_shape=stored((n_x, n_z + 1, slab // n_x, both), bf16),
-        in_specs=[
-            pl.BlockSpec((slab, tokens), lambda z: (jnp.minimum(z, n_z - 1), 0)),
-            inside,
-            inside,
+        out_shape=stored((n_x, n_z + 1, rows, both), bf16),
+        in_specs=[far, near, near],
+        out_specs=far,
+        scratch_shapes=[
+            pltpu.VMEM((n_z, slab, tokens), bf16),
+            pltpu.VMEM((n_z + 1, n_x, rows, both), bf16),
+            pltpu.SemaphoreType.DMA((n_z,)),
+            pltpu.SemaphoreType.DMA((n_z + 1,)),
         ],
-        out_specs=pl.BlockSpec((n_x, 1, slab // n_x, both), lambda z: (0, z, 0, 0)),
         compiler_params=pltpu.CompilerParams(vmem_limit_bytes=20 * 1024 * 1024),
         name="weight_terms",
     )(

time: 125 us -> 123 us (0.984)
  Pallas kernels: 17.2 us -> 15 us
    pallas_call x1, Pallas kernels: 6.32 us -> 4.1 us  [weight_terms(): pl.pallas_call(weight_terms_body, out_shape=stored((n_x, n_z + 1, rows, b...]
where the time goes in v4:
time: 123 us; the launch traced here: 122 us
  blocking collectives  37.7 us (31%)
  starting transfers between devices  36.8 us (30%)
  waiting for transfers between devices  29.1 us (24%)
  Pallas kernels  15 us (12%)
  local copies, waits for them, and re-layouts  1.76 us (1%)
    all_to_all x2, blocking collectives, exchange(): return lax.all_to_all(array, axis, split_axis=0, concat_axis=0, tiled=True)  37.7 us
    all_to_all x3, starting transfers between devices, exchange(): return lax.all_to_all(array, axis, split_axis=0, concat_axis=0, tiled=True)  17.6 us
    all_to_all x3, waiting for transfers between devices, exchange(): return lax.all_to_all(array, axis, split_axis=0, concat_axis=0, tiled=True)  14.3 us
    ppermute x3, waiting for transfers between devices, sent_apart(): return lax.ppermute(array, DP, moves)  12.6 us
    ppermute x3, starting transfers between devices, swapped(): return lax.ppermute(array, 'dp_1', [(0, 1), (1, 0)])  11.9 us
    pallas_call x11, Pallas kernels, run(): return made(*operands)  10.9 us
    ppermute x3, starting transfers between devices, sent_apart(): return lax.ppermute(array, DP, moves)  7.21 us
    pallas_call x1, Pallas kernels, weight_terms(): pl.pallas_call(weight_terms_body, out_shape=stored((n_x, n_z + 1, rows, b...  4.1 us
  transfers between devices with their start and end apart: 9, of which 6 were waited for; matrix products, arithmetic and copies ran while one was open for 1% of the time, Pallas kernels for 5%

profile of v4, /device:TPU:1, one launch (start us, length us, event | category | flops | bytes accessed | tf_op | source)
XLA Modules:
  0.0 121.8 jit_solution(11186082414098354187)
XLA Ops:
  0.6 0.0 copy-start.1
  0.6 0.0 copy-start.4
  0.7 0.0 copy-start
  0.7 0.0 copy-start.5
  0.7 1.6 %shard_map.102 = bf16[8,64,256]{2,1,0:T(8,128)(2,1)} custom-call(bf16[64,128]{1,0:T(8,128)(2,1)} %content.1, bf16[64,128]{1,0:T(8,128)(2,1)} %gating.1), custom_call_target="tpu_custom_call" | custom-call | tf_op jit(solution)/shard_map/pallas_call | solution.py:79
  2.3 21.3 %all_to_all.25.arrived = bf16[8,64,256]{2,1,0:T(8,128)(2,1)S(1)} all-to-all(bf16[8,64,256]{2,1,0:T(8,128)(2,1)} %shard_map.102), channel_id=1, replica_groups=mesh['sp_0'=8,'sp_1'=4,'dp_0'=8,'dp_1'=2] {'sp_0'}, dimensions={0} | all-to-all | bytes 524288 | tf_op jit(solution)/shard_map/all_to_all | solution.py:23
  23.6 0.1 shard_map.103
  23.7 16.4 %all_to_all.26.weight = bf16[4,8,64,256]{3,2,1,0:T(8,128)(2,1)S(1)} all-to-all(bf16[4,8,64,256]{3,2,1,0:T(8,128)(2,1)S(1)} %shard_map.103), channel_id=1, replica_groups=mesh['sp_0'=8,'sp_1'=4,'dp_0'=8,'dp_1'=2] {'sp_1'}, dimensions={0} | all-to-all | bytes 2097152 | tf_op jit(solution)/shard_map/all_to_all | solution.py:23
  40.1 0.0 copy-done.1
  40.1 0.0 copy-done.4
  40.1 0.0 copy-done
  40.1 0.0 copy-done.5
  40.1 1.8 %shard_map.104 = (bf16[512,256]{1,0:T(8,128)(2,1)S(1)}, f32[16,4,512]{2,1,0:T(4,128)}) custom-call(bf16[512,2048]{1,0:T(8,128)(2,1)S(1)} %copy-done, bf16[4,8,64,256]{3,2,1,0:T(8,128)(2,1)S(1)} %all_to_all.26.weight, bf16[1,128,128]{2,1,0:T(8,128)(2,1)S(1)} %copy-done.4, f32[1,128]{1,0:T(1,128)S(1)} %bitcast.11, bf16[512,128]{1,0:T(8,128)(2,1)S(1)} %copy-done.1), custom_call_target="tpu_custom_call" | custom-call | tf_op jit(solution)/shard_map/pallas_call | solution.py:79
  42.0 0.0 copy-start.2
  42.0 0.7 copy-done.2
  42.7 10.6 %all-to-all-start.2 = ((f32[16,4,512]{2,1,0:T(4,128)}), f32[16,4,512]{2,1,0:T(4,128)S(1)}, u32[]{:S(2)}, u32[]{:S(2)}) async-start(f32[16,4,512]{2,1,0:T(4,128)} %get-tuple-element.21), calls=%async_computation.2 | async-start | bytes 262144 | tf_op jit(solution)/shard_map/all_to_all | solution.py:23
  53.2 0.0 copy-start.6
  53.3 1.9 %shard_map.110.hidden_t = bf16[2048,512]{1,0:T(8,128)(2,1)} custom-call(bf16[512,2048]{1,0:T(8,128)(2,1)S(1)} %copy-done), custom_call_target="tpu_custom_call" | custom-call | tf_op jit(solution)/shard_map/pallas_call | solution.py:79
  55.2 0.1 stack.44.where
  55.3 0.9 shard_map.105
  56.2 6.0 %all-to-all-done.2.sums = f32[16,4,512]{2,1,0:T(4,128)S(1)} async-done(((f32[16,4,512]{2,1,0:T(4,128)}), f32[16,4,512]{2,1,0:T(4,128)S(1)}, u32[]{:S(2)}, u32[]{:S(2)}) %all-to-all-start.2) | async-done | bytes 131104 | tf_op jit(solution)/shard_map/all_to_all | solution.py:23
  62.1 0.0 copy-done.6
  62.1 0.0 copy-start.3
  62.1 0.9 copy-done.3
  63.1 0.7 shard_map.106
  63.8 4.1 %weight_terms.1 = bf16[4,9,64,256]{3,2,1,0:T(8,128)(2,1)} custom-call(bf16[2048,512]{1,0:T(8,128)(2,1)} %shard_map.110.hidden_t, bf16[512,256]{1,0:T(8,128)(2,1)S(1)} %get-tuple-element.25.joined, bf16[64,256]{1,0:T(8,128)(2,1)S(1)} %get-tuple-element.34.mixing_term), custom_call_target="tpu_custom_call" | custom-call | tf_op jit(solution)/shard_map/weight_terms/pallas_call | solution.py:206
  67.9 3.5 %all-to-all-start.3 = ((bf16[4,9,64,256]{3,2,1,0:T(8,128)(2,1)}), bf16[4,9,64,256]{3,2,1,0:T(8,128)(2,1)S(1)}, u32[]{:S(2)}, u32[]{:S(2)}) async-start(bf16[4,9,64,256]{3,2,1,0:T(8,128)(2,1)} %weight_terms.1), calls=%async_computation.3 | async-start | bytes 2359296 | tf_op jit(solution)/shard_map/all_to_all | solution.py:23
  71.5 1.9 %collective-permute-start.1 = (bf16[1024,256]{1,0:T(8,128)(2,1)S(1)}, bf16[1024,256]{1,0:T(8,128)(2,1)S(1)}, u32[]{:S(2)}, u32[]{:S(2)}) collective-permute-start(bf16[1024,256]{1,0:T(8,128)(2,1)S(1)} %get-tuple-element.27), channel_id=1, source_target_pairs={{0,1},{1,0},{2,3},{3,2},{4,5},{5,4},{6,7},{7,6},{8,9},{9,8},{10,11... | collective-permute-start | bytes 1572872 | tf_op jit(solution)/shard_map/ppermute | solution.py:27
  73.4 2.4 %collective-permute-start = (bf16[512,256]{1,0:T(8,128)(2,1)S(1)}, bf16[512,256]{1,0:T(8,128)(2,1)S(1)}, u32[]{:S(2)}, u32[]{:S(2)}) collective-permute-start(bf16[512,256]{1,0:T(8,128)(2,1)S(1)} %get-tuple-element.25.joined), channel_id=1, source_target_pairs={{0,1},{1,0},{2,3},{3,2},{4,5},{5,4},{6,7},{7,6},{8,9},{9,8},{10,11... | collective-permute-start | bytes 786440 | tf_op jit(solution)/shard_map/ppermute | solution.py:27
  75.8 1.1 collective-permute-done.joined_far
  77.0 0.0 collective-permute-done.1.far
  77.0 0.9 shard_map.107
  77.8 2.0 %collective-permute-start.2 = (bf16[512,512]{1,0:T(8,128)(2,1)S(1)}, bf16[512,512]{1,0:T(8,128)(2,1)S(1)}, u32[]{:S(2)}, u32[]{:S(2)}) collective-permute-start(bf16[512,512]{1,0:T(8,128)(2,1)S(1)} %get-tuple-element.28), channel_id=1, source_target_pairs={{0,2},{1,15},{2,4},{3,1},{4,6},{5,3},{6,8},{7,5},{8,10},{9,7},{10,... | collective-permute-start | bytes 1572872 | tf_op jit(solution)/shard_map/ppermute | solution.py:36
  79.8 8.4 %all-to-all-done.3.arrived = bf16[4,9,64,256]{3,2,1,0:T(8,128)(2,1)S(1)} async-done(((bf16[4,9,64,256]{3,2,1,0:T(8,128)(2,1)}), bf16[4,9,64,256]{3,2,1,0:T(8,128)(2,1)S(1)}, u32[]{:S(2)}, u32[]{:S(2)}) %all-to-all-start.3) | async-done | bytes 1179680 | tf_op jit(solution)/shard_map/all_to_all | solution.py:23
  88.2 1.0 shard_map.111
  89.1 3.5 %all-to-all-start.4 = ((bf16[8,2,64,256]{3,2,1,0:T(8,128)(2,1)}), bf16[8,2,64,256]{3,2,1,0:T(8,128)(2,1)S(1)}, u32[]{:S(2)}, u32[]{:S(2)}) async-start(bf16[8,2,64,256]{3,2,1,0:T(8,128)(2,1)} %shard_map.111), calls=%async_computation.4 | async-start | bytes 1048576 | tf_op jit(solution)/shard_map/all_to_all | solution.py:23
  92.6 2.0 %collective-permute-start.3 = (bf16[512,128]{1,0:T(8,128)(2,1)S(1)}, bf16[512,128]{1,0:T(8,128)(2,1)S(1)}, u32[]{:S(2)}, u32[]{:S(2)}) collective-permute-start(bf16[512,128]{1,0:T(8,128)(2,1)S(1)} %get-tuple-element.30), channel_id=1, source_target_pairs={{0,4},{1,13},{2,6},{3,15},{4,8},{5,1},{6,10},{7,3},{8,12},{9,5},{1... | collective-permute-start | bytes 393224 | tf_op jit(solution)/shard_map/ppermute | solution.py:36
  94.6 6.2 %collective-permute-done.3.four = bf16[512,128]{1,0:T(8,128)(2,1)S(1)} collective-permute-done((bf16[512,128]{1,0:T(8,128)(2,1)S(1)}, bf16[512,128]{1,0:T(8,128)(2,1)S(1)}, u32[]{:S(2)}, u32[]{:S(2)}) %collective-permute-start.3) | collective-permute-done | bytes 131104 | tf_op jit(solution)/shard_map/ppermute | solution.py:36
  100.8 0.0 collective-permute-done.2.odd
  100.8 0.6 shard_map.108
  101.5 3.3 %collective-permute-start.4 = (bf16[512,256]{1,0:T(8,128)(2,1)S(1)}, bf16[512,256]{1,0:T(8,128)(2,1)S(1)}, u32[]{:S(2)}, u32[]{:S(2)}) collective-permute-start(bf16[512,256]{1,0:T(8,128)(2,1)S(1)} %shard_map.108), channel_id=1, source_target_pairs={{0,4},{1,13},{2,6},{3,15},{4,8},{5,1},{6,10},{7,3},{8,12},{9,5},{1... | collective-permute-start | bytes 786440 | tf_op jit(solution)/shard_map/ppermute | solution.py:36
  104.8 6.4 %collective-permute-done.4.two = bf16[512,256]{1,0:T(8,128)(2,1)S(1)} collective-permute-done((bf16[512,256]{1,0:T(8,128)(2,1)S(1)}, bf16[512,256]{1,0:T(8,128)(2,1)S(1)}, u32[]{:S(2)}, u32[]{:S(2)}) %collective-permute-start.4) | collective-permute-done | bytes 262176 | tf_op jit(solution)/shard_map/ppermute | solution.py:36
  111.2 0.6 shard_map.109
  111.8 7.6 %collective-permute-start.5 = (bf16[512,128]{1,0:T(8,128)(2,1)S(1)}, bf16[512,128]{1,0:T(8,128)(2,1)S(1)}, u32[]{:S(2)}, u32[]{:S(2)}) collective-permute-start(bf16[512,128]{1,0:T(8,128)(2,1)S(1)} %get-tuple-element.33), channel_id=1, source_target_pairs={{0,1},{1,0},{2,3},{3,2},{4,5},{5,4},{6,7},{7,6},{8,9},{9,8},{10,11... | collective-permute-start | bytes 393224 | tf_op jit(solution)/shard_map/ppermute | solution.py:27
  119.4 1.0 collective-permute-done.5
  120.4 0.7 add_convert_fusion
  121.1 0.0 all-to-all-done.4.arrived
  121.1 0.7 shard_map.112
Async XLA Ops:
  0.6 39.5 %copy-start.1 = (bf16[512,128]{1,0:T(8,128)(2,1)S(1)}, bf16[512,128]{1,0:T(8,128)(2,1)}, u32[]{:S(2)}) copy-start(bf16[512,128]{1,0:T(8,128)(2,1)} %grad.3) | copy-start | bytes 393220
  0.6 39.5 %copy-start.4 = (bf16[1,128,128]{2,1,0:T(8,128)(2,1)S(1)}, bf16[1,128,128]{2,1,0:T(8,128)(2,1)}, u32[]{:S(2)}) copy-start(bf16[1,128,128]{2,1,0:T(8,128)(2,1)} %mixing.3) | copy-start | bytes 98308
  0.7 39.5 %copy-start = (bf16[512,2048]{1,0:T(8,128)(2,1)S(1)}, bf16[512,2048]{1,0:T(8,128)(2,1)}, u32[]{:S(2)}) copy-start(bf16[512,2048]{1,0:T(8,128)(2,1)} %array.1) | copy-start | bytes 6291460
  0.7 39.5 %copy-start.5 = (f32[128]{0:T(128)S(1)}, f32[128]{0:T(128)}, u32[]{:S(2)}) copy-start(f32[128]{0:T(128)} %param.10) | copy-start | bytes 1540
  42.0 0.7 copy-start.2
  42.7 19.5 %all-to-all-start.2 = ((f32[16,4,512]{2,1,0:T(4,128)}), f32[16,4,512]{2,1,0:T(4,128)S(1)}, u32[]{:S(2)}, u32[]{:S(2)}) async-start(f32[16,4,512]{2,1,0:T(4,128)} %get-tuple-element.21), calls=%async_computation.2 | async-start | bytes 262144 | tf_op jit(solution)/shard_map/all_to_all | solution.py:23
  53.2 8.9 %copy-start.6 = (f32[1,128]{1,0:T(1,128)S(1)}, f32[1,128]{1,0:T(1,128)}, u32[]{:S(2)}) copy-start(f32[1,128]{1,0:T(1,128)} %bias.1) | copy-start | bytes 1540
  62.1 1.0 copy-start.3
  67.9 20.2 %all-to-all-start.3 = ((bf16[4,9,64,256]{3,2,1,0:T(8,128)(2,1)}), bf16[4,9,64,256]{3,2,1,0:T(8,128)(2,1)S(1)}, u32[]{:S(2)}, u32[]{:S(2)}) async-start(bf16[4,9,64,256]{3,2,1,0:T(8,128)(2,1)} %weight_terms.1), calls=%async_computation.3 | async-start | bytes 2359296 | tf_op jit(solution)/shard_map/all_to_all | solution.py:23
  71.5 5.5 %collective-permute-start.1 = (bf16[1024,256]{1,0:T(8,128)(2,1)S(1)}, bf16[1024,256]{1,0:T(8,128)(2,1)S(1)}, u32[]{:S(2)}, u32[]{:S(2)}) collective-permute-start(bf16[1024,256]{1,0:T(8,128)(2,1)S(1)} %get-tuple-element.27), channel_id=1, source_target_pairs={{0,1},{1,0},{2,3},{3,2},{4,5},{5,4},{6,7},{7,6},{8,9},{9,8},{10,11... | collective-permute-start | bytes 1572872 | tf_op jit(solution)/shard_map/ppermute | solution.py:27
  73.4 3.6 %collective-permute-start = (bf16[512,256]{1,0:T(8,128)(2,1)S(1)}, bf16[512,256]{1,0:T(8,128)(2,1)S(1)}, u32[]{:S(2)}, u32[]{:S(2)}) collective-permute-start(bf16[512,256]{1,0:T(8,128)(2,1)S(1)} %get-tuple-element.25.joined), channel_id=1, source_target_pairs={{0,1},{1,0},{2,3},{3,2},{4,5},{5,4},{6,7},{7,6},{8,9},{9,8},{10,11... | collective-permute-start | bytes 786440 | tf_op jit(solution)/shard_map/ppermute | solution.py:27
  77.8 23.0 %collective-permute-start.2 = (bf16[512,512]{1,0:T(8,128)(2,1)S(1)}, bf16[512,512]{1,0:T(8,128)(2,1)S(1)}, u32[]{:S(2)}, u32[]{:S(2)}) collective-permute-start(bf16[512,512]{1,0:T(8,128)(2,1)S(1)} %get-tuple-element.28), channel_id=1, source_target_pairs={{0,2},{1,15},{2,4},{3,1},{4,6},{5,3},{6,8},{7,5},{8,10},{9,7},{10,... | collective-permute-start | bytes 1572872 | tf_op jit(solution)/shard_map/ppermute | solution.py:36
  89.1 32.0 %all-to-all-start.4 = ((bf16[8,2,64,256]{3,2,1,0:T(8,128)(2,1)}), bf16[8,2,64,256]{3,2,1,0:T(8,128)(2,1)S(1)}, u32[]{:S(2)}, u32[]{:S(2)}) async-start(bf16[8,2,64,256]{3,2,1,0:T(8,128)(2,1)} %shard_map.111), calls=%async_computation.4 | async-start | bytes 1048576 | tf_op jit(solution)/shard_map/all_to_all | solution.py:23
  92.6 8.2 %collective-permute-start.3 = (bf16[512,128]{1,0:T(8,128)(2,1)S(1)}, bf16[512,128]{1,0:T(8,128)(2,1)S(1)}, u32[]{:S(2)}, u32[]{:S(2)}) collective-permute-start(bf16[512,128]{1,0:T(8,128)(2,1)S(1)} %get-tuple-element.30), channel_id=1, source_target_pairs={{0,4},{1,13},{2,6},{3,15},{4,8},{5,1},{6,10},{7,3},{8,12},{9,5},{1... | collective-permute-start | bytes 393224 | tf_op jit(solution)/shard_map/ppermute | solution.py:36
  101.5 9.7 %collective-permute-start.4 = (bf16[512,256]{1,0:T(8,128)(2,1)S(1)}, bf16[512,256]{1,0:T(8,128)(2,1)S(1)}, u32[]{:S(2)}, u32[]{:S(2)}) collective-permute-start(bf16[512,256]{1,0:T(8,128)(2,1)S(1)} %shard_map.108), channel_id=1, source_target_pairs={{0,4},{1,13},{2,6},{3,15},{4,8},{5,1},{6,10},{7,3},{8,12},{9,5},{1... | collective-permute-start | bytes 786440 | tf_op jit(solution)/shard_map/ppermute | solution.py:36
  111.8 8.6 %collective-permute-start.5 = (bf16[512,128]{1,0:T(8,128)(2,1)S(1)}, bf16[512,128]{1,0:T(8,128)(2,1)S(1)}, u32[]{:S(2)}, u32[]{:S(2)}) collective-permute-start(bf16[512,128]{1,0:T(8,128)(2,1)S(1)} %get-tuple-element.33), channel_id=1, source_target_pairs={{0,1},{1,0},{2,3},{3,2},{4,5},{5,4},{6,7},{7,6},{8,9},{9,8},{10,11... | collective-permute-start | bytes 393224 | tf_op jit(solution)/shard_map/ppermute | solution.py:27

commit v5 on v4

--- a/solution.py
+++ b/solution.py
@@ -27,12 +27,12 @@
     return lax.ppermute(array, "dp_1", [(0, 1), (1, 0)])
 
 
-def sent_apart(array, step):
+def sent_apart(array, step, cross=False):
     ring = lax.axis_size("dp_0")
     moves = []
     for y in range(ring):
-        moves.append((2 * y, 2 * ((y + step) % ring)))
-        moves.append((2 * y + 1, 2 * ((y - step) % ring) + 1))
+        for core, there in ((0, (y + step) % ring), (1, (y - step) % ring)):
+            moves.append((2 * y + core, 2 * there + (1 - core if cross else core)))
     return lax.ppermute(array, DP, moves)
 
 
@@ -176,11 +176,11 @@
 
 def weight_terms_body(hidden_t, joined, mixing_term, out, held, made, come, gone):
     n_x, n_all, rows, both = out.shape
-    n_z = n_all - 1
-    slab = n_x * rows
+    parts, chunk, _ = held.shape
+    deep = (n_all - 1) // parts
     loads = [
-        pltpu.make_async_copy(hidden_t.at[pl.ds(z * slab, slab)], held.at[z], come.at[z])
-        for z in range(n_z)
+        pltpu.make_async_copy(hidden_t.at[pl.ds(i * chunk, chunk)], held.at[i], come.at[i])
+        for i in range(parts)
     ]
     stores = [
         pltpu.make_async_copy(made.at[z], out.at[:, z], gone.at[z]) for z in range(n_all)
@@ -188,20 +188,22 @@
     for load in loads:
         load.start()
     for x in range(n_x):
-        made[n_z, x] = mixing_term[...]
-    stores[n_z].start()
-    for z in range(n_z):
-        loads[z].wait()
-        made[z] = nn(held[z], joined[...]).astype(bf16).reshape(n_x, rows, both)
-        stores[z].start()
+        made[n_all - 1, x] = mixing_term[...]
+    stores[n_all - 1].start()
+    for i in range(parts):
+        loads[i].wait()
+        term = nn(held[i], joined[...]).astype(bf16)
+        made[i * deep : (i + 1) * deep] = term.reshape(deep, n_x, rows, both)
+        for z in range(i * deep, (i + 1) * deep):
+            stores[z].start()
     for store in stores:
         store.wait()
 
 
 def weight_terms(hidden_t, joined, mixing_term, n_x, n_z):
     tokens, both = joined.shape
-    slab = hidden_t.shape[0] // n_z
-    rows = slab // n_x
+    rows = hidden_t.shape[0] // (n_x * n_z)
+    parts = 4
     near, far = pl.BlockSpec(memory_space=pltpu.VMEM), pl.BlockSpec(memory_space=pl.ANY)
     return pl.pallas_call(
         weight_terms_body,
@@ -209,9 +211,9 @@
         in_specs=[far, near, near],
         out_specs=far,
         scratch_shapes=[
-            pltpu.VMEM((n_z, slab, tokens), bf16),
+            pltpu.VMEM((parts, hidden_t.shape[0] // parts, tokens), bf16),
             pltpu.VMEM((n_z + 1, n_x, rows, both), bf16),
-            pltpu.SemaphoreType.DMA((n_z,)),
+            pltpu.SemaphoreType.DMA((parts,)),
             pltpu.SemaphoreType.DMA((n_z + 1,)),
         ],
         compiler_params=pltpu.CompilerParams(vmem_limit_bytes=20 * 1024 * 1024),
@@ -253,15 +255,24 @@
     own[...] = term(3 * pair + single, single)
 
 
-def merge_body(where, two, odd, four, out):
+def merge_body(where, two, odd, four, same_out, other_out, keep_out, send_out):
     half = four.shape[1]
     first = where[10] == 0
-    extra = four[...].astype(f32)
-    none = jnp.zeros_like(extra)
-    left = two[:, :half] + odd[:, :half].astype(f32) + jnp.where(first, extra, none)
-    right = two[:, half:] + odd[:, half : 2 * half].astype(f32) + jnp.where(first, none, extra)
-    out[:, :half] = left.astype(bf16)
-    out[:, half:] = right.astype(bf16)
+    both = two[...] + odd[:, : 2 * half].astype(f32)
+    left, right = both[:, :half], both[:, half:]
+    same_out[...] = (jnp.where(first, left, right) + four[...].astype(f32)).astype(bf16)
+    other_out[...] = jnp.where(first, right, left).astype(bf16)
+    left, right = odd[:, 2 * half : 3 * half], odd[:, 3 * half :]
+    left, right = left.astype(f32), right.astype(f32)
+    keep_out[...] = jnp.where(first, left, right).astype(bf16)
+    send_out[...] = jnp.where(first, right, left).astype(bf16)
+
+
+def total_body(own, same, other, keep, sent, out):
+    total = own[...]
+    for part in (same, other, keep, sent):
+        total = total + part[...].astype(f32)
+    out[...] = total.astype(bf16)
 
 
 def regroup_body(arrived, out):
@@ -285,15 +296,6 @@
     gating_out[...] = total[0][:, half:]
     mixing_out[0, : BLOCK // 2] = total[1][:, :half]
     mixing_out[0, BLOCK // 2 :] = total[1][:, half:]
-
-
-def gather_body(where, odd, two, own, keep_out, send_out):
-    half = own.shape[1]
-    total = odd[:, 2 * half :].astype(f32) + two[...].astype(f32)
-    first = where[10] == 0
-    left, right = total[:, :half], total[:, half:]
-    keep_out[...] = own[...] + jnp.where(first, left, right)
-    send_out[...] = jnp.where(first, right, left).astype(bf16)
 
 
 def step(
@@ -349,16 +351,16 @@
     )(joined, joined_far, mine, far)
     four = sent_apart(four, 2)
     odd = sent_apart(odd, 1)
-    two = call(merge_body, like(pair, bf16), scalars=True)(where, two, odd, four)
-    two = sent_apart(two, 2)
+    small = like(single, bf16)
+    same, other, keep, send = call(merge_body, (small,) * 4, scalars=True)(where, two, odd, four)
+    same = sent_apart(same, 2)
+    other = sent_apart(other, 2, True)
+    sent = swapped(send)
 
     regrouped = call(regroup_body, stored((n_z, 2, shard_rows, both), bf16))(along_x)
     arrived = exchange(regrouped, "sp_0")
 
-    keep, send = call(
-        gather_body, (like(single, f32), like(single, bf16)), scalars=True
-    )(where, odd, two, own)
-    input_grad = (keep + swapped(send).astype(f32)).astype(bf16)
+    input_grad = call(total_body, outside(single, bf16))(own, same, other, keep, sent)
 
     content_grad, gating_grad, mixing_grad = call(
         functools.partial(finish_body, grad_scale),

time: 123 us -> 123 us (level)
  the two profiles are of different devices: /device:TPU:1 before, /device:TPU:9 now
where the time goes in v5:
time: 123 us; the launch traced here: 122 us
  starting transfers between devices  41.7 us (34%)
  blocking collectives  36.9 us (30%)
  waiting for transfers between devices  26.7 us (22%)
  Pallas kernels  14.6 us (12%)
  local copies, waits for them, and re-layouts  1.77 us (1%)
    all_to_all x2, blocking collectives, exchange(): return lax.all_to_all(array, axis, split_axis=0, concat_axis=0, tiled=True)  36.9 us
    ppermute x4, starting transfers between devices, sent_apart(): return lax.ppermute(array, DP, moves)  17.7 us
    all_to_all x3, starting transfers between devices, exchange(): return lax.all_to_all(array, axis, split_axis=0, concat_axis=0, tiled=True)  17.7 us
    all_to_all x3, waiting for transfers between devices, exchange(): return lax.all_to_all(array, axis, split_axis=0, concat_axis=0, tiled=True)  17.2 us
    pallas_call x11, Pallas kernels, run(): return made(*operands)  11 us
    ppermute x4, waiting for transfers between devices, sent_apart(): return lax.ppermute(array, DP, moves)  9.51 us
    ppermute x3, starting transfers between devices, swapped(): return lax.ppermute(array, 'dp_1', [(0, 1), (1, 0)])  6.25 us
    pallas_call x1, Pallas kernels, weight_terms(): pl.pallas_call(weight_terms_body, out_shape=stored((n_x, n_z + 1, rows, b...  3.6 us
  transfers between devices with their start and end apart: 10, of which 4 were waited for; matrix products, arithmetic and copies ran while one was open for 0% of the time, Pallas kernels for 5%

profile of v5, /device:TPU:9, one launch (start us, length us, event | category | flops | bytes accessed | tf_op | source)
XLA Modules:
  0.0 122.5 jit_solution(13562748802324392790)
XLA Ops:
  0.6 0.0 copy-start.1
  0.6 0.0 copy-start.4
  0.7 0.0 copy-start
  0.7 0.0 copy-start.5
  0.7 1.6 %shard_map.102 = bf16[8,64,256]{2,1,0:T(8,128)(2,1)} custom-call(bf16[64,128]{1,0:T(8,128)(2,1)} %content.1, bf16[64,128]{1,0:T(8,128)(2,1)} %gating.1), custom_call_target="tpu_custom_call" | custom-call | tf_op jit(solution)/shard_map/pallas_call | solution.py:79
  2.3 20.5 %all_to_all.25.arrived = bf16[8,64,256]{2,1,0:T(8,128)(2,1)S(1)} all-to-all(bf16[8,64,256]{2,1,0:T(8,128)(2,1)} %shard_map.102), channel_id=1, replica_groups=mesh['sp_0'=8,'sp_1'=4,'dp_0'=8,'dp_1'=2] {'sp_0'}, dimensions={0} | all-to-all | bytes 524288 | tf_op jit(solution)/shard_map/all_to_all | solution.py:23
  22.8 0.1 shard_map.103
  22.9 16.4 %all_to_all.26.weight = bf16[4,8,64,256]{3,2,1,0:T(8,128)(2,1)S(1)} all-to-all(bf16[4,8,64,256]{3,2,1,0:T(8,128)(2,1)S(1)} %shard_map.103), channel_id=1, replica_groups=mesh['sp_0'=8,'sp_1'=4,'dp_0'=8,'dp_1'=2] {'sp_1'}, dimensions={0} | all-to-all | bytes 2097152 | tf_op jit(solution)/shard_map/all_to_all | solution.py:23
  39.3 0.0 copy-done.1
  39.3 0.0 copy-done.4
  39.3 0.0 copy-done
  39.3 0.0 copy-done.5
  39.3 1.8 %shard_map.104 = (bf16[512,256]{1,0:T(8,128)(2,1)S(1)}, f32[16,4,512]{2,1,0:T(4,128)}) custom-call(bf16[512,2048]{1,0:T(8,128)(2,1)S(1)} %copy-done, bf16[4,8,64,256]{3,2,1,0:T(8,128)(2,1)S(1)} %all_to_all.26.weight, bf16[1,128,128]{2,1,0:T(8,128)(2,1)S(1)} %copy-done.4, f32[1,128]{1,0:T(1,128)S(1)} %bitcast.11, bf16[512,128]{1,0:T(8,128)(2,1)S(1)} %copy-done.1), custom_call_target="tpu_custom_call" | custom-call | tf_op jit(solution)/shard_map/pallas_call | solution.py:79
  41.1 0.0 copy-start.2
  41.1 0.7 copy-done.2
  41.8 10.6 %all-to-all-start.2 = ((f32[16,4,512]{2,1,0:T(4,128)}), f32[16,4,512]{2,1,0:T(4,128)S(1)}, u32[]{:S(2)}, u32[]{:S(2)}) async-start(f32[16,4,512]{2,1,0:T(4,128)} %get-tuple-element.23), calls=%async_computation.2 | async-start | bytes 262144 | tf_op jit(solution)/shard_map/all_to_all | solution.py:23
  52.5 1.9 %shard_map.110.hidden_t = bf16[2048,512]{1,0:T(8,128)(2,1)} custom-call(bf16[512,2048]{1,0:T(8,128)(2,1)S(1)} %copy-done), custom_call_target="tpu_custom_call" | custom-call | tf_op jit(solution)/shard_map/pallas_call | solution.py:79
  54.4 0.1 stack.44.where
  54.5 0.9 shard_map.105
  55.4 4.9 %all-to-all-done.2.sums = f32[16,4,512]{2,1,0:T(4,128)S(1)} async-done(((f32[16,4,512]{2,1,0:T(4,128)}), f32[16,4,512]{2,1,0:T(4,128)S(1)}, u32[]{:S(2)}, u32[]{:S(2)}) %all-to-all-start.2) | async-done | bytes 131104 | tf_op jit(solution)/shard_map/all_to_all | solution.py:23
  60.3 0.0 copy-done.6
  60.3 0.9 copy-done.3
  61.2 0.7 shard_map.106
  62.0 3.6 %weight_terms.1 = bf16[4,9,64,256]{3,2,1,0:T(8,128)(2,1)} custom-call(bf16[2048,512]{1,0:T(8,128)(2,1)} %shard_map.110.hidden_t, bf16[512,256]{1,0:T(8,128)(2,1)S(1)} %get-tuple-element.27.joined, bf16[64,256]{1,0:T(8,128)(2,1)S(1)} %get-tuple-element.38.mixing_term), custom_call_target="tpu_custom_call" | custom-call | tf_op jit(solution)/shard_map/weight_terms/pallas_call | solution.py:208
  65.6 0.0 copy-done.7
  65.6 3.5 %all-to-all-start.3 = ((bf16[4,9,64,256]{3,2,1,0:T(8,128)(2,1)}), bf16[4,9,64,256]{3,2,1,0:T(8,128)(2,1)S(1)}, u32[]{:S(2)}, u32[]{:S(2)}) async-start(bf16[4,9,64,256]{3,2,1,0:T(8,128)(2,1)} %weight_terms.1), calls=%async_computation.3 | async-start | bytes 2359296 | tf_op jit(solution)/shard_map/all_to_all | solution.py:23
  69.1 1.9 %collective-permute-start.1 = (bf16[1024,256]{1,0:T(8,128)(2,1)}, bf16[1024,256]{1,0:T(8,128)(2,1)S(1)}, u32[]{:S(2)}, u32[]{:S(2)}) collective-permute-start(bf16[1024,256]{1,0:T(8,128)(2,1)} %copy-done.7), channel_id=1, source_target_pairs={{0,1},{1,0},{2,3},{3,2},{4,5},{5,4},{6,7},{7,6},{8,9},{9,8},{10,11... | collective-permute-start | bytes 1572872 | tf_op jit(solution)/shard_map/ppermute | solution.py:27
  71.1 2.4 %collective-permute-start = (bf16[512,256]{1,0:T(8,128)(2,1)S(1)}, bf16[512,256]{1,0:T(8,128)(2,1)S(1)}, u32[]{:S(2)}, u32[]{:S(2)}) collective-permute-start(bf16[512,256]{1,0:T(8,128)(2,1)S(1)} %get-tuple-element.27.joined), channel_id=1, source_target_pairs={{0,1},{1,0},{2,3},{3,2},{4,5},{5,4},{6,7},{7,6},{8,9},{9,8},{10,11... | collective-permute-start | bytes 786440 | tf_op jit(solution)/shard_map/ppermute | solution.py:27
  73.5 12.3 %all-to-all-done.3.arrived = bf16[4,9,64,256]{3,2,1,0:T(8,128)(2,1)S(1)} async-done(((bf16[4,9,64,256]{3,2,1,0:T(8,128)(2,1)}), bf16[4,9,64,256]{3,2,1,0:T(8,128)(2,1)S(1)}, u32[]{:S(2)}, u32[]{:S(2)}) %all-to-all-start.3) | async-done | bytes 1179680 | tf_op jit(solution)/shard_map/all_to_all | solution.py:23
  85.7 0.9 shard_map.111
  86.7 3.5 %all-to-all-start.4 = ((bf16[8,2,64,256]{3,2,1,0:T(8,128)(2,1)}), bf16[8,2,64,256]{3,2,1,0:T(8,128)(2,1)S(1)}, u32[]{:S(2)}, u32[]{:S(2)}) async-start(bf16[8,2,64,256]{3,2,1,0:T(8,128)(2,1)} %shard_map.111), calls=%async_computation.4 | async-start | bytes 1048576 | tf_op jit(solution)/shard_map/all_to_all | solution.py:23
  90.2 0.0 collective-permute-done.joined_far
  90.2 0.0 collective-permute-done.1.far
  90.2 0.9 shard_map.107
  91.1 3.2 %collective-permute-start.2 = (bf16[512,512]{1,0:T(8,128)(2,1)S(1)}, bf16[512,512]{1,0:T(8,128)(2,1)S(1)}, u32[]{:S(2)}, u32[]{:S(2)}) collective-permute-start(bf16[512,512]{1,0:T(8,128)(2,1)S(1)} %get-tuple-element.32), channel_id=1, source_target_pairs={{0,2},{1,15},{2,4},{3,1},{4,6},{5,3},{6,8},{7,5},{8,10},{9,7},{10,... | collective-permute-start | bytes 1572872 | tf_op jit(solution)/shard_map/ppermute | solution.py:36
  94.3 2.0 %collective-permute-start.3 = (bf16[512,128]{1,0:T(8,128)(2,1)S(1)}, bf16[512,128]{1,0:T(8,128)(2,1)S(1)}, u32[]{:S(2)}, u32[]{:S(2)}) collective-permute-start(bf16[512,128]{1,0:T(8,128)(2,1)S(1)} %get-tuple-element.33), channel_id=1, source_target_pairs={{0,4},{1,13},{2,6},{3,15},{4,8},{5,1},{6,10},{7,3},{8,12},{9,5},{1... | collective-permute-start | bytes 393224 | tf_op jit(solution)/shard_map/ppermute | solution.py:36
  96.3 6.6 %collective-permute-done.3.four = bf16[512,128]{1,0:T(8,128)(2,1)S(1)} collective-permute-done((bf16[512,128]{1,0:T(8,128)(2,1)S(1)}, bf16[512,128]{1,0:T(8,128)(2,1)S(1)}, u32[]{:S(2)}, u32[]{:S(2)}) %collective-permute-start.3) | collective-permute-done | bytes 131104 | tf_op jit(solution)/shard_map/ppermute | solution.py:36
  102.9 0.0 collective-permute-done.2.odd
  102.9 0.7 shard_map.108
  103.6 6.6 %collective-permute-start.4 = (bf16[512,128]{1,0:T(8,128)(2,1)S(1)}, bf16[512,128]{1,0:T(8,128)(2,1)S(1)}, u32[]{:S(2)}, u32[]{:S(2)}) collective-permute-start(bf16[512,128]{1,0:T(8,128)(2,1)S(1)} %get-tuple-element.34), channel_id=1, source_target_pairs={{0,4},{1,13},{2,6},{3,15},{4,8},{5,1},{6,10},{7,3},{8,12},{9,5},{1... | collective-permute-start | bytes 393224 | tf_op jit(solution)/shard_map/ppermute | solution.py:36
  110.2 6.0 %collective-permute-start.5 = (bf16[512,128]{1,0:T(8,128)(2,1)S(1)}, bf16[512,128]{1,0:T(8,128)(2,1)S(1)}, u32[]{:S(2)}, u32[]{:S(2)}) collective-permute-start(bf16[512,128]{1,0:T(8,128)(2,1)S(1)} %get-tuple-element.35), channel_id=1, source_target_pairs={{0,5},{1,12},{2,7},{3,14},{4,9},{5,0},{6,11},{7,2},{8,13},{9,4},{1... | collective-permute-start | bytes 393224 | tf_op jit(solution)/shard_map/ppermute | solution.py:36
  116.2 1.9 %collective-permute-start.6 = (bf16[512,128]{1,0:T(8,128)(2,1)S(1)}, bf16[512,128]{1,0:T(8,128)(2,1)S(1)}, u32[]{:S(2)}, u32[]{:S(2)}) collective-permute-start(bf16[512,128]{1,0:T(8,128)(2,1)S(1)} %get-tuple-element.37), channel_id=1, source_target_pairs={{0,1},{1,0},{2,3},{3,2},{4,5},{5,4},{6,7},{7,6},{8,9},{9,8},{10,11... | collective-permute-start | bytes 393224 | tf_op jit(solution)/shard_map/ppermute | solution.py:27
  118.1 0.0 collective-permute-done.4.same
  118.1 2.9 %collective-permute-done.5.other = bf16[512,128]{1,0:T(8,128)(2,1)S(1)} collective-permute-done((bf16[512,128]{1,0:T(8,128)(2,1)S(1)}, bf16[512,128]{1,0:T(8,128)(2,1)S(1)}, u32[]{:S(2)}, u32[]{:S(2)}) %collective-permute-start.5) | collective-permute-done | bytes 131104 | tf_op jit(solution)/shard_map/ppermute | solution.py:36
  121.0 0.0 collective-permute-done.6.sent
  121.0 0.7 shard_map.109
  121.7 0.0 all-to-all-done.4.arrived
  121.8 0.7 shard_map.112
  (3 shorter events, 0.0 us)
Async XLA Ops:
  0.6 38.6 %copy-start.1 = (bf16[512,128]{1,0:T(8,128)(2,1)S(1)}, bf16[512,128]{1,0:T(8,128)(2,1)}, u32[]{:S(2)}) copy-start(bf16[512,128]{1,0:T(8,128)(2,1)} %grad.3) | copy-start | bytes 393220
  0.6 38.6 %copy-start.4 = (bf16[1,128,128]{2,1,0:T(8,128)(2,1)S(1)}, bf16[1,128,128]{2,1,0:T(8,128)(2,1)}, u32[]{:S(2)}) copy-start(bf16[1,128,128]{2,1,0:T(8,128)(2,1)} %mixing.3) | copy-start | bytes 98308
  0.7 38.6 %copy-start = (bf16[512,2048]{1,0:T(8,128)(2,1)S(1)}, bf16[512,2048]{1,0:T(8,128)(2,1)}, u32[]{:S(2)}) copy-start(bf16[512,2048]{1,0:T(8,128)(2,1)} %array.1) | copy-start | bytes 6291460
  0.7 38.6 %copy-start.5 = (f32[128]{0:T(128)S(1)}, f32[128]{0:T(128)}, u32[]{:S(2)}) copy-start(f32[128]{0:T(128)} %param.10) | copy-start | bytes 1540
  41.1 0.7 copy-start.2
  41.8 18.5 %all-to-all-start.2 = ((f32[16,4,512]{2,1,0:T(4,128)}), f32[16,4,512]{2,1,0:T(4,128)S(1)}, u32[]{:S(2)}, u32[]{:S(2)}) async-start(f32[16,4,512]{2,1,0:T(4,128)} %get-tuple-element.23), calls=%async_computation.2 | async-start | bytes 262144 | tf_op jit(solution)/shard_map/all_to_all | solution.py:23
  52.5 7.8 %copy-start.6 = (f32[1,128]{1,0:T(1,128)S(1)}, f32[1,128]{1,0:T(1,128)}, u32[]{:S(2)}) copy-start(f32[1,128]{1,0:T(1,128)} %bias.1) | copy-start | bytes 1540
  55.4 10.2 %copy-start.7 = (bf16[1024,256]{1,0:T(8,128)(2,1)}, bf16[1024,256]{1,0:T(8,128)(2,1)S(1)}, u32[]{:S(2)}) copy-start(bf16[1024,256]{1,0:T(8,128)(2,1)S(1)} %get-tuple-element.29) | copy-start | bytes 1572868
  60.3 1.0 copy-start.3
  65.6 20.1 %all-to-all-start.3 = ((bf16[4,9,64,256]{3,2,1,0:T(8,128)(2,1)}), bf16[4,9,64,256]{3,2,1,0:T(8,128)(2,1)S(1)}, u32[]{:S(2)}, u32[]{:S(2)}) async-start(bf16[4,9,64,256]{3,2,1,0:T(8,128)(2,1)} %weight_terms.1), calls=%async_computation.3 | async-start | bytes 2359296 | tf_op jit(solution)/shard_map/all_to_all | solution.py:23
  69.1 21.1 %collective-permute-start.1 = (bf16[1024,256]{1,0:T(8,128)(2,1)}, bf16[1024,256]{1,0:T(8,128)(2,1)S(1)}, u32[]{:S(2)}, u32[]{:S(2)}) collective-permute-start(bf16[1024,256]{1,0:T(8,128)(2,1)} %copy-done.7), channel_id=1, source_target_pairs={{0,1},{1,0},{2,3},{3,2},{4,5},{5,4},{6,7},{7,6},{8,9},{9,8},{10,11... | collective-permute-start | bytes 1572872 | tf_op jit(solution)/shard_map/ppermute | solution.py:27
  71.1 19.1 %collective-permute-start = (bf16[512,256]{1,0:T(8,128)(2,1)S(1)}, bf16[512,256]{1,0:T(8,128)(2,1)S(1)}, u32[]{:S(2)}, u32[]{:S(2)}) collective-permute-start(bf16[512,256]{1,0:T(8,128)(2,1)S(1)} %get-tuple-element.27.joined), channel_id=1, source_target_pairs={{0,1},{1,0},{2,3},{3,2},{4,5},{5,4},{6,7},{7,6},{8,9},{9,8},{10,11... | collective-permute-start | bytes 786440 | tf_op jit(solution)/shard_map/ppermute | solution.py:27
  86.7 35.1 %all-to-all-start.4 = ((bf16[8,2,64,256]{3,2,1,0:T(8,128)(2,1)}), bf16[8,2,64,256]{3,2,1,0:T(8,128)(2,1)S(1)}, u32[]{:S(2)}, u32[]{:S(2)}) async-start(bf16[8,2,64,256]{3,2,1,0:T(8,128)(2,1)} %shard_map.111), calls=%async_computation.4 | async-start | bytes 1048576 | tf_op jit(solution)/shard_map/all_to_all | solution.py:23
  91.1 11.8 %collective-permute-start.2 = (bf16[512,512]{1,0:T(8,128)(2,1)S(1)}, bf16[512,512]{1,0:T(8,128)(2,1)S(1)}, u32[]{:S(2)}, u32[]{:S(2)}) collective-permute-start(bf16[512,512]{1,0:T(8,128)(2,1)S(1)} %get-tuple-element.32), channel_id=1, source_target_pairs={{0,2},{1,15},{2,4},{3,1},{4,6},{5,3},{6,8},{7,5},{8,10},{9,7},{10,... | collective-permute-start | bytes 1572872 | tf_op jit(solution)/shard_map/ppermute | solution.py:36
  94.3 8.6 %collective-permute-start.3 = (bf16[512,128]{1,0:T(8,128)(2,1)S(1)}, bf16[512,128]{1,0:T(8,128)(2,1)S(1)}, u32[]{:S(2)}, u32[]{:S(2)}) collective-permute-start(bf16[512,128]{1,0:T(8,128)(2,1)S(1)} %get-tuple-element.33), channel_id=1, source_target_pairs={{0,4},{1,13},{2,6},{3,15},{4,8},{5,1},{6,10},{7,3},{8,12},{9,5},{1... | collective-permute-start | bytes 393224 | tf_op jit(solution)/shard_map/ppermute | solution.py:36
  103.6 14.5 %collective-permute-start.4 = (bf16[512,128]{1,0:T(8,128)(2,1)S(1)}, bf16[512,128]{1,0:T(8,128)(2,1)S(1)}, u32[]{:S(2)}, u32[]{:S(2)}) collective-permute-start(bf16[512,128]{1,0:T(8,128)(2,1)S(1)} %get-tuple-element.34), channel_id=1, source_target_pairs={{0,4},{1,13},{2,6},{3,15},{4,8},{5,1},{6,10},{7,3},{8,12},{9,5},{1... | collective-permute-start | bytes 393224 | tf_op jit(solution)/shard_map/ppermute | solution.py:36
  110.2 10.8 %collective-permute-start.5 = (bf16[512,128]{1,0:T(8,128)(2,1)S(1)}, bf16[512,128]{1,0:T(8,128)(2,1)S(1)}, u32[]{:S(2)}, u32[]{:S(2)}) collective-permute-start(bf16[512,128]{1,0:T(8,128)(2,1)S(1)} %get-tuple-element.35), channel_id=1, source_target_pairs={{0,5},{1,12},{2,7},{3,14},{4,9},{5,0},{6,11},{7,2},{8,13},{9,4},{1... | collective-permute-start | bytes 393224 | tf_op jit(solution)/shard_map/ppermute | solution.py:36
  116.2 4.8 %collective-permute-start.6 = (bf16[512,128]{1,0:T(8,128)(2,1)S(1)}, bf16[512,128]{1,0:T(8,128)(2,1)S(1)}, u32[]{:S(2)}, u32[]{:S(2)}) collective-permute-start(bf16[512,128]{1,0:T(8,128)(2,1)S(1)} %get-tuple-element.37), channel_id=1, source_target_pairs={{0,1},{1,0},{2,3},{3,2},{4,5},{5,4},{6,7},{7,6},{8,9},{9,8},{10,11... | collective-permute-start | bytes 393224 | tf_op jit(solution)/shard_map/ppermute | solution.py:27

commit v6 on v5

--- a/solution.py
+++ b/solution.py
@@ -143,7 +143,19 @@
         out[at : at + step] = array[:, at : at + step].T
 
 
-def norm_body(full_width, sums, pre, grad, table, flipped, bias, gain, joined_out, mixing_out):
+def norm_terms_body(full_width, sums, pre, grad, table, flipped, bias, gain, hidden_t, joined_out, out, held, made, come, gone):
+    n_x, n_all, rows, both = out.shape
+    parts, chunk, _ = held.shape
+    deep = (n_all - 1) // parts
+    loads = [
+        pltpu.make_async_copy(hidden_t.at[pl.ds(i * chunk, chunk)], held.at[i], come.at[i])
+        for i in range(parts)
+    ]
+    stores = [
+        pltpu.make_async_copy(made.at[z], out.at[:, z], gone.at[z]) for z in range(n_all)
+    ]
+    for load in loads:
+        load.start()
     gating, mixed_grad, back, (pre_content, pre_gating) = branches(
         pre[...], grad[...], flipped[...], gain[...]
     )
@@ -162,37 +174,22 @@
     width = normed.shape[1]
     mixing_grad = None
     for at in range(0, normed.shape[0], BLOCK):
-        rows = slice(at, at + BLOCK)
-        mixed = nn(table[...], normed[rows]) + shift
-        joined_out[rows, :width] = (mixed * content_slope[rows]).astype(bf16)
-        term = nt(mixed_grad[rows], normed[rows])
+        block = slice(at, at + BLOCK)
+        mixed = nn(table[...], normed[block]) + shift
+        joined_out[block, :width] = (mixed * content_slope[block]).astype(bf16)
+        term = nt(mixed_grad[block], normed[block])
         mixing_grad = term if mixing_grad is None else mixing_grad + term
     gating_back = inv_std * (back - first - centred * second)
     joined_out[:, width:] = (gating_back * gelu_slope(pre_gating)).astype(bf16)
     mixing_grad = causal(mixing_grad).astype(bf16)
     half = BLOCK // 2
-    mixing_out[...] = jnp.concatenate([mixing_grad[:half], mixing_grad[half:]], axis=1)
-
-
-def weight_terms_body(hidden_t, joined, mixing_term, out, held, made, come, gone):
-    n_x, n_all, rows, both = out.shape
-    parts, chunk, _ = held.shape
-    deep = (n_all - 1) // parts
-    loads = [
-        pltpu.make_async_copy(hidden_t.at[pl.ds(i * chunk, chunk)], held.at[i], come.at[i])
-        for i in range(parts)
-    ]
-    stores = [
-        pltpu.make_async_copy(made.at[z], out.at[:, z], gone.at[z]) for z in range(n_all)
-    ]
-    for load in loads:
-        load.start()
+    mixing_term = jnp.concatenate([mixing_grad[:half], mixing_grad[half:]], axis=1)
     for x in range(n_x):
-        made[n_all - 1, x] = mixing_term[...]
+        made[n_all - 1, x] = mixing_term
     stores[n_all - 1].start()
     for i in range(parts):
         loads[i].wait()
-        term = nn(held[i], joined[...]).astype(bf16)
+        term = nn(held[i], joined_out[...]).astype(bf16)
         made[i * deep : (i + 1) * deep] = term.reshape(deep, n_x, rows, both)
         for z in range(i * deep, (i + 1) * deep):
             stores[z].start()
@@ -200,28 +197,28 @@
         store.wait()
 
 
-def weight_terms(hidden_t, joined, mixing_term, n_x, n_z):
-    tokens, both = joined.shape
-    rows = hidden_t.shape[0] // (n_x * n_z)
+def norm_terms(full_width, small, hidden_t, n_x, n_z):
+    width, tokens = hidden_t.shape
+    both = 2 * small[2].shape[1]
+    rows = width // (n_x * n_z)
     parts = 4
     near, far = pl.BlockSpec(memory_space=pltpu.VMEM), pl.BlockSpec(memory_space=pl.ANY)
     return pl.pallas_call(
-        weight_terms_body,
-        out_shape=stored((n_x, n_z + 1, rows, both), bf16),
-        in_specs=[far, near, near],
-        out_specs=far,
+        functools.partial(norm_terms_body, full_width),
+        out_shape=(like((tokens, both), bf16), stored((n_x, n_z + 1, rows, both), bf16)),
+        in_specs=[near] * len(small) + [far],
+        out_specs=(near, far),
         scratch_shapes=[
-            pltpu.VMEM((parts, hidden_t.shape[0] // parts, tokens), bf16),
+            pltpu.VMEM((parts, width // parts, tokens), bf16),
             pltpu.VMEM((n_z + 1, n_x, rows, both), bf16),
             pltpu.SemaphoreType.DMA((parts,)),
             pltpu.SemaphoreType.DMA((n_z + 1,)),
         ],
         compiler_params=pltpu.CompilerParams(vmem_limit_bytes=20 * 1024 * 1024),
-        name="weight_terms",
+        name="norm_terms",
     )(
+        *[pltpu.with_memory_space_constraint(a, pltpu.VMEM) for a in small],
         pltpu.with_memory_space_constraint(hidden_t, pltpu.HBM),
-        pltpu.with_memory_space_constraint(joined, pltpu.VMEM),
-        pltpu.with_memory_space_constraint(mixing_term, pltpu.VMEM),
     )
 
 
@@ -337,12 +334,10 @@
         project_body, (like(wide, bf16), stored((n_dp, 4, tok_rows), f32))
     )(hidden_in, weight, mixing_weight, gain, out_grad)
     sums = exchange(sums, DP)
-    joined, mixing_term = call(
-        functools.partial(norm_body, full_width), (like(wide, bf16), like((BLOCK // 2, both), bf16))
-    )(sums, pre, out_grad, table, flipped, mixing_bias, gain)
+    small = (sums, pre, out_grad, table, flipped, mixing_bias, gain)
+    joined, terms = norm_terms(full_width, small, hidden_t, n_x, n_z)
 
     joined_far = swapped(joined)
-    terms = weight_terms(hidden_t, joined, mixing_term, n_x, n_z)
     along_x = exchange(terms, "sp_1")
 
     odd, two, four, own = call(
@@ -351,8 +346,9 @@
     )(joined, joined_far, mine, far)
     four = sent_apart(four, 2)
     odd = sent_apart(odd, 1)
-    small = like(single, bf16)
-    same, other, keep, send = call(merge_body, (small,) * 4, scalars=True)(where, two, odd, four)
+    same, other, keep, send = call(merge_body, (like(single, bf16),) * 4, scalars=True)(
+        where, two, odd, four
+    )
     same = sent_apart(same, 2)
     other = sent_apart(other, 2, True)
     sent = swapped(send)

time: 123 us -> 123 us (level)
    pallas_call x11 -> x10, Pallas kernels: 11 us -> 10.3 us  [run(): return made(*operands)]
where the time goes in v6:
time: 123 us; the launch traced here: 122 us
  starting transfers between devices  41.7 us (34%)
  blocking collectives  36.9 us (30%)
  waiting for transfers between devices  26.7 us (22%)
  Pallas kernels  14.2 us (12%)
  local copies, waits for them, and re-layouts  1.77 us (1%)
    all_to_all x2, blocking collectives, exchange(): return lax.all_to_all(array, axis, split_axis=0, concat_axis=0, tiled=True)  36.9 us
    ppermute x4, starting transfers between devices, sent_apart(): return lax.ppermute(array, DP, moves)  17.7 us
    all_to_all x3, starting transfers between devices, exchange(): return lax.all_to_all(array, axis, split_axis=0, concat_axis=0, tiled=True)  17.7 us
    all_to_all x3, waiting for transfers between devices, exchange(): return lax.all_to_all(array, axis, split_axis=0, concat_axis=0, tiled=True)  17.2 us
    pallas_call x10, Pallas kernels, run(): return made(*operands)  10.3 us
    ppermute x4, waiting for transfers between devices, sent_apart(): return lax.ppermute(array, DP, moves)  9.52 us
    ppermute x3, starting transfers between devices, swapped(): return lax.ppermute(array, 'dp_1', [(0, 1), (1, 0)])  6.25 us
    pallas_call x1, Pallas kernels, norm_terms(): pl.pallas_call(functools.partial(norm_terms_body, full_width), out_shape=...  3.89 us
  transfers between devices with their start and end apart: 10, of which 4 were waited for; matrix products, arithmetic and copies ran while one was open for 0% of the time, Pallas kernels for 5%

profile of v6, /device:TPU:9, one launch (start us, length us, event | category | flops | bytes accessed | tf_op | source)
XLA Modules:
  0.0 122.0 jit_solution(16476582387547371843)
XLA Ops:
  0.6 0.0 copy-start.1
  0.6 0.0 copy-start.4
  0.7 0.0 copy-start
  0.7 0.0 copy-start.5
  0.7 1.6 %shard_map.102 = bf16[8,64,256]{2,1,0:T(8,128)(2,1)} custom-call(bf16[64,128]{1,0:T(8,128)(2,1)} %content.1, bf16[64,128]{1,0:T(8,128)(2,1)} %gating.1), custom_call_target="tpu_custom_call" | custom-call | tf_op jit(solution)/shard_map/pallas_call | solution.py:79
  2.3 20.5 %all_to_all.25.arrived = bf16[8,64,256]{2,1,0:T(8,128)(2,1)S(1)} all-to-all(bf16[8,64,256]{2,1,0:T(8,128)(2,1)} %shard_map.102), channel_id=1, replica_groups=mesh['sp_0'=8,'sp_1'=4,'dp_0'=8,'dp_1'=2] {'sp_0'}, dimensions={0} | all-to-all | bytes 524288 | tf_op jit(solution)/shard_map/all_to_all | solution.py:23
  22.8 0.1 shard_map.103
  22.9 16.4 %all_to_all.26.weight = bf16[4,8,64,256]{3,2,1,0:T(8,128)(2,1)S(1)} all-to-all(bf16[4,8,64,256]{3,2,1,0:T(8,128)(2,1)S(1)} %shard_map.103), channel_id=1, replica_groups=mesh['sp_0'=8,'sp_1'=4,'dp_0'=8,'dp_1'=2] {'sp_1'}, dimensions={0} | all-to-all | bytes 2097152 | tf_op jit(solution)/shard_map/all_to_all | solution.py:23
  39.3 0.0 copy-done.1
  39.3 0.0 copy-done.4
  39.3 0.0 copy-done
  39.3 0.0 copy-done.5
  39.3 1.8 %shard_map.104 = (bf16[512,256]{1,0:T(8,128)(2,1)S(1)}, f32[16,4,512]{2,1,0:T(4,128)}) custom-call(bf16[512,2048]{1,0:T(8,128)(2,1)S(1)} %copy-done, bf16[4,8,64,256]{3,2,1,0:T(8,128)(2,1)S(1)} %all_to_all.26.weight, bf16[1,128,128]{2,1,0:T(8,128)(2,1)S(1)} %copy-done.4, f32[1,128]{1,0:T(1,128)S(1)} %bitcast.11, bf16[512,128]{1,0:T(8,128)(2,1)S(1)} %copy-done.1), custom_call_target="tpu_custom_call" | custom-call | tf_op jit(solution)/shard_map/pallas_call | solution.py:79
  41.1 0.0 copy-start.2
  41.1 0.7 copy-done.2
  41.8 10.6 %all-to-all-start.2 = ((f32[16,4,512]{2,1,0:T(4,128)}), f32[16,4,512]{2,1,0:T(4,128)S(1)}, u32[]{:S(2)}, u32[]{:S(2)}) async-start(f32[16,4,512]{2,1,0:T(4,128)} %get-tuple-element.23), calls=%async_computation.2 | async-start | bytes 262144 | tf_op jit(solution)/shard_map/all_to_all | solution.py:23
  52.5 0.0 copy-start.6
  52.5 1.9 %shard_map.106.hidden_t = bf16[2048,512]{1,0:T(8,128)(2,1)} custom-call(bf16[512,2048]{1,0:T(8,128)(2,1)S(1)} %copy-done), custom_call_target="tpu_custom_call" | custom-call | tf_op jit(solution)/shard_map/pallas_call | solution.py:79
  54.4 0.1 stack.44.where
  54.5 0.9 shard_map.105
  55.4 4.9 %all-to-all-done.2.sums = f32[16,4,512]{2,1,0:T(4,128)S(1)} async-done(((f32[16,4,512]{2,1,0:T(4,128)}), f32[16,4,512]{2,1,0:T(4,128)S(1)}, u32[]{:S(2)}, u32[]{:S(2)}) %all-to-all-start.2) | async-done | bytes 131104 | tf_op jit(solution)/shard_map/all_to_all | solution.py:23
  60.3 0.0 copy-done.6
  60.3 0.9 copy-done.3
  61.2 3.9 %norm_terms.1 = (bf16[512,256]{1,0:T(8,128)(2,1)S(1)}, bf16[4,9,64,256]{3,2,1,0:T(8,128)(2,1)}) custom-call(f32[16,4,512]{2,1,0:T(4,128)S(1)} %all-to-all-done.2.sums, bf16[512,256]{1,0:T(8,128)(2,1)S(1)} %copy-done.3, bf16[512,128]{1,0:T(8,128)(2,1)S(1)} %copy-done.1, bf16[128,128]{1,0:T(8,128)(2,1)S(1)} %get-tuple-element.25.table, ...), custom_call_target="tpu_custom_call" | custom-call | tf_op jit(solution)/shard_map/norm_terms/pallas_call | solution.py:206
  65.1 0.0 copy-done.7
  65.2 3.5 %all-to-all-start.3 = ((bf16[4,9,64,256]{3,2,1,0:T(8,128)(2,1)}), bf16[4,9,64,256]{3,2,1,0:T(8,128)(2,1)S(1)}, u32[]{:S(2)}, u32[]{:S(2)}) async-start(bf16[4,9,64,256]{3,2,1,0:T(8,128)(2,1)} %get-tuple-element.38), calls=%async_computation.3 | async-start | bytes 2359296 | tf_op jit(solution)/shard_map/all_to_all | solution.py:23
  68.7 1.9 %collective-permute-start.1 = (bf16[1024,256]{1,0:T(8,128)(2,1)}, bf16[1024,256]{1,0:T(8,128)(2,1)S(1)}, u32[]{:S(2)}, u32[]{:S(2)}) collective-permute-start(bf16[1024,256]{1,0:T(8,128)(2,1)} %copy-done.7), channel_id=1, source_target_pairs={{0,1},{1,0},{2,3},{3,2},{4,5},{5,4},{6,7},{7,6},{8,9},{9,8},{10,11... | collective-permute-start | bytes 1572872 | tf_op jit(solution)/shard_map/ppermute | solution.py:27
  70.6 2.4 %collective-permute-start = (bf16[512,256]{1,0:T(8,128)(2,1)S(1)}, bf16[512,256]{1,0:T(8,128)(2,1)S(1)}, u32[]{:S(2)}, u32[]{:S(2)}) collective-permute-start(bf16[512,256]{1,0:T(8,128)(2,1)S(1)} %get-tuple-element.27.joined), channel_id=1, source_target_pairs={{0,1},{1,0},{2,3},{3,2},{4,5},{5,4},{6,7},{7,6},{8,9},{9,8},{10,11... | collective-permute-start | bytes 786440 | tf_op jit(solution)/shard_map/ppermute | solution.py:27
  73.0 12.3 %all-to-all-done.3.arrived = bf16[4,9,64,256]{3,2,1,0:T(8,128)(2,1)S(1)} async-done(((bf16[4,9,64,256]{3,2,1,0:T(8,128)(2,1)}), bf16[4,9,64,256]{3,2,1,0:T(8,128)(2,1)S(1)}, u32[]{:S(2)}, u32[]{:S(2)}) %all-to-all-start.3) | async-done | bytes 1179680 | tf_op jit(solution)/shard_map/all_to_all | solution.py:23
  85.3 0.9 shard_map.110
  86.2 3.5 %all-to-all-start.4 = ((bf16[8,2,64,256]{3,2,1,0:T(8,128)(2,1)}), bf16[8,2,64,256]{3,2,1,0:T(8,128)(2,1)S(1)}, u32[]{:S(2)}, u32[]{:S(2)}) async-start(bf16[8,2,64,256]{3,2,1,0:T(8,128)(2,1)} %shard_map.110), calls=%async_computation.4 | async-start | bytes 1048576 | tf_op jit(solution)/shard_map/all_to_all | solution.py:23
  89.7 0.0 collective-permute-done.joined_far
  89.8 0.0 collective-permute-done.1.far
  89.8 0.9 shard_map.107
  90.6 3.2 %collective-permute-start.2 = (bf16[512,512]{1,0:T(8,128)(2,1)S(1)}, bf16[512,512]{1,0:T(8,128)(2,1)S(1)}, u32[]{:S(2)}, u32[]{:S(2)}) collective-permute-start(bf16[512,512]{1,0:T(8,128)(2,1)S(1)} %get-tuple-element.32), channel_id=1, source_target_pairs={{0,2},{1,15},{2,4},{3,1},{4,6},{5,3},{6,8},{7,5},{8,10},{9,7},{10,... | collective-permute-start | bytes 1572872 | tf_op jit(solution)/shard_map/ppermute | solution.py:36
  93.8 2.0 %collective-permute-start.3 = (bf16[512,128]{1,0:T(8,128)(2,1)S(1)}, bf16[512,128]{1,0:T(8,128)(2,1)S(1)}, u32[]{:S(2)}, u32[]{:S(2)}) collective-permute-start(bf16[512,128]{1,0:T(8,128)(2,1)S(1)} %get-tuple-element.33), channel_id=1, source_target_pairs={{0,4},{1,13},{2,6},{3,15},{4,8},{5,1},{6,10},{7,3},{8,12},{9,5},{1... | collective-permute-start | bytes 393224 | tf_op jit(solution)/shard_map/ppermute | solution.py:36
  95.8 6.6 %collective-permute-done.3.four = bf16[512,128]{1,0:T(8,128)(2,1)S(1)} collective-permute-done((bf16[512,128]{1,0:T(8,128)(2,1)S(1)}, bf16[512,128]{1,0:T(8,128)(2,1)S(1)}, u32[]{:S(2)}, u32[]{:S(2)}) %collective-permute-start.3) | collective-permute-done | bytes 131104 | tf_op jit(solution)/shard_map/ppermute | solution.py:36
  102.4 0.0 collective-permute-done.2.odd
  102.4 0.7 shard_map.108
  103.1 6.6 %collective-permute-start.4 = (bf16[512,128]{1,0:T(8,128)(2,1)S(1)}, bf16[512,128]{1,0:T(8,128)(2,1)S(1)}, u32[]{:S(2)}, u32[]{:S(2)}) collective-permute-start(bf16[512,128]{1,0:T(8,128)(2,1)S(1)} %get-tuple-element.34), channel_id=1, source_target_pairs={{0,4},{1,13},{2,6},{3,15},{4,8},{5,1},{6,10},{7,3},{8,12},{9,5},{1... | collective-permute-start | bytes 393224 | tf_op jit(solution)/shard_map/ppermute | solution.py:36
  109.7 6.0 %collective-permute-start.5 = (bf16[512,128]{1,0:T(8,128)(2,1)S(1)}, bf16[512,128]{1,0:T(8,128)(2,1)S(1)}, u32[]{:S(2)}, u32[]{:S(2)}) collective-permute-start(bf16[512,128]{1,0:T(8,128)(2,1)S(1)} %get-tuple-element.35), channel_id=1, source_target_pairs={{0,5},{1,12},{2,7},{3,14},{4,9},{5,0},{6,11},{7,2},{8,13},{9,4},{1... | collective-permute-start | bytes 393224 | tf_op jit(solution)/shard_map/ppermute | solution.py:36
  115.7 1.9 %collective-permute-start.6 = (bf16[512,128]{1,0:T(8,128)(2,1)S(1)}, bf16[512,128]{1,0:T(8,128)(2,1)S(1)}, u32[]{:S(2)}, u32[]{:S(2)}) collective-permute-start(bf16[512,128]{1,0:T(8,128)(2,1)S(1)} %get-tuple-element.37), channel_id=1, source_target_pairs={{0,1},{1,0},{2,3},{3,2},{4,5},{5,4},{6,7},{7,6},{8,9},{9,8},{10,11... | collective-permute-start | bytes 393224 | tf_op jit(solution)/shard_map/ppermute | solution.py:27
  117.7 0.0 collective-permute-done.4.same
  117.7 2.9 %collective-permute-done.5.other = bf16[512,128]{1,0:T(8,128)(2,1)S(1)} collective-permute-done((bf16[512,128]{1,0:T(8,128)(2,1)S(1)}, bf16[512,128]{1,0:T(8,128)(2,1)S(1)}, u32[]{:S(2)}, u32[]{:S(2)}) %collective-permute-start.5) | collective-permute-done | bytes 131104 | tf_op jit(solution)/shard_map/ppermute | solution.py:36
  120.6 0.0 collective-permute-done.6.sent
  120.6 0.7 shard_map.109
  121.3 0.0 all-to-all-done.4.arrived
  121.3 0.7 shard_map.111
  (2 shorter events, 0.0 us)
Async XLA Ops:
  0.6 38.6 %copy-start.1 = (bf16[512,128]{1,0:T(8,128)(2,1)S(1)}, bf16[512,128]{1,0:T(8,128)(2,1)}, u32[]{:S(2)}) copy-start(bf16[512,128]{1,0:T(8,128)(2,1)} %grad.3) | copy-start | bytes 393220
  0.6 38.6 %copy-start.4 = (bf16[1,128,128]{2,1,0:T(8,128)(2,1)S(1)}, bf16[1,128,128]{2,1,0:T(8,128)(2,1)}, u32[]{:S(2)}) copy-start(bf16[1,128,128]{2,1,0:T(8,128)(2,1)} %mixing.3) | copy-start | bytes 98308
  0.7 38.6 %copy-start = (bf16[512,2048]{1,0:T(8,128)(2,1)S(1)}, bf16[512,2048]{1,0:T(8,128)(2,1)}, u32[]{:S(2)}) copy-start(bf16[512,2048]{1,0:T(8,128)(2,1)} %array.1) | copy-start | bytes 6291460
  0.7 38.6 %copy-start.5 = (f32[128]{0:T(128)S(1)}, f32[128]{0:T(128)}, u32[]{:S(2)}) copy-start(f32[128]{0:T(128)} %param.10) | copy-start | bytes 1540
  41.1 0.7 copy-start.2
  41.8 18.5 %all-to-all-start.2 = ((f32[16,4,512]{2,1,0:T(4,128)}), f32[16,4,512]{2,1,0:T(4,128)S(1)}, u32[]{:S(2)}, u32[]{:S(2)}) async-start(f32[16,4,512]{2,1,0:T(4,128)} %get-tuple-element.23), calls=%async_computation.2 | async-start | bytes 262144 | tf_op jit(solution)/shard_map/all_to_all | solution.py:23
  52.5 7.8 %copy-start.6 = (f32[1,128]{1,0:T(1,128)S(1)}, f32[1,128]{1,0:T(1,128)}, u32[]{:S(2)}) copy-start(f32[1,128]{1,0:T(1,128)} %bias.1) | copy-start | bytes 1540
  55.4 9.8 %copy-start.7 = (bf16[1024,256]{1,0:T(8,128)(2,1)}, bf16[1024,256]{1,0:T(8,128)(2,1)S(1)}, u32[]{:S(2)}) copy-start(bf16[1024,256]{1,0:T(8,128)(2,1)S(1)} %get-tuple-element.29) | copy-start | bytes 1572868
  60.3 1.0 copy-start.3
  65.2 20.1 %all-to-all-start.3 = ((bf16[4,9,64,256]{3,2,1,0:T(8,128)(2,1)}), bf16[4,9,64,256]{3,2,1,0:T(8,128)(2,1)S(1)}, u32[]{:S(2)}, u32[]{:S(2)}) async-start(bf16[4,9,64,256]{3,2,1,0:T(8,128)(2,1)} %get-tuple-element.38), calls=%async_computation.3 | async-start | bytes 2359296 | tf_op jit(solution)/shard_map/all_to_all | solution.py:23
  68.7 21.1 %collective-permute-start.1 = (bf16[1024,256]{1,0:T(8,128)(2,1)}, bf16[1024,256]{1,0:T(8,128)(2,1)S(1)}, u32[]{:S(2)}, u32[]{:S(2)}) collective-permute-start(bf16[1024,256]{1,0:T(8,128)(2,1)} %copy-done.7), channel_id=1, source_target_pairs={{0,1},{1,0},{2,3},{3,2},{4,5},{5,4},{6,7},{7,6},{8,9},{9,8},{10,11... | collective-permute-start | bytes 1572872 | tf_op jit(solution)/shard_map/ppermute | solution.py:27
  70.6 19.1 %collective-permute-start = (bf16[512,256]{1,0:T(8,128)(2,1)S(1)}, bf16[512,256]{1,0:T(8,128)(2,1)S(1)}, u32[]{:S(2)}, u32[]{:S(2)}) collective-permute-start(bf16[512,256]{1,0:T(8,128)(2,1)S(1)} %get-tuple-element.27.joined), channel_id=1, source_target_pairs={{0,1},{1,0},{2,3},{3,2},{4,5},{5,4},{6,7},{7,6},{8,9},{9,8},{10,11... | collective-permute-start | bytes 786440 | tf_op jit(solution)/shard_map/ppermute | solution.py:27
  86.2 35.1 %all-to-all-start.4 = ((bf16[8,2,64,256]{3,2,1,0:T(8,128)(2,1)}), bf16[8,2,64,256]{3,2,1,0:T(8,128)(2,1)S(1)}, u32[]{:S(2)}, u32[]{:S(2)}) async-start(bf16[8,2,64,256]{3,2,1,0:T(8,128)(2,1)} %shard_map.110), calls=%async_computation.4 | async-start | bytes 1048576 | tf_op jit(solution)/shard_map/all_to_all | solution.py:23
  90.6 11.8 %collective-permute-start.2 = (bf16[512,512]{1,0:T(8,128)(2,1)S(1)}, bf16[512,512]{1,0:T(8,128)(2,1)S(1)}, u32[]{:S(2)}, u32[]{:S(2)}) collective-permute-start(bf16[512,512]{1,0:T(8,128)(2,1)S(1)} %get-tuple-element.32), channel_id=1, source_target_pairs={{0,2},{1,15},{2,4},{3,1},{4,6},{5,3},{6,8},{7,5},{8,10},{9,7},{10,... | collective-permute-start | bytes 1572872 | tf_op jit(solution)/shard_map/ppermute | solution.py:36
  93.8 8.6 %collective-permute-start.3 = (bf16[512,128]{1,0:T(8,128)(2,1)S(1)}, bf16[512,128]{1,0:T(8,128)(2,1)S(1)}, u32[]{:S(2)}, u32[]{:S(2)}) collective-permute-start(bf16[512,128]{1,0:T(8,128)(2,1)S(1)} %get-tuple-element.33), channel_id=1, source_target_pairs={{0,4},{1,13},{2,6},{3,15},{4,8},{5,1},{6,10},{7,3},{8,12},{9,5},{1... | collective-permute-start | bytes 393224 | tf_op jit(solution)/shard_map/ppermute | solution.py:36
  103.1 14.5 %collective-permute-start.4 = (bf16[512,128]{1,0:T(8,128)(2,1)S(1)}, bf16[512,128]{1,0:T(8,128)(2,1)S(1)}, u32[]{:S(2)}, u32[]{:S(2)}) collective-permute-start(bf16[512,128]{1,0:T(8,128)(2,1)S(1)} %get-tuple-element.34), channel_id=1, source_target_pairs={{0,4},{1,13},{2,6},{3,15},{4,8},{5,1},{6,10},{7,3},{8,12},{9,5},{1... | collective-permute-start | bytes 393224 | tf_op jit(solution)/shard_map/ppermute | solution.py:36
  109.7 10.8 %collective-permute-start.5 = (bf16[512,128]{1,0:T(8,128)(2,1)S(1)}, bf16[512,128]{1,0:T(8,128)(2,1)S(1)}, u32[]{:S(2)}, u32[]{:S(2)}) collective-permute-start(bf16[512,128]{1,0:T(8,128)(2,1)S(1)} %get-tuple-element.35), channel_id=1, source_target_pairs={{0,5},{1,12},{2,7},{3,14},{4,9},{5,0},{6,11},{7,2},{8,13},{9,4},{1... | collective-permute-start | bytes 393224 | tf_op jit(solution)/shard_map/ppermute | solution.py:36
  115.7 4.8 %collective-permute-start.6 = (bf16[512,128]{1,0:T(8,128)(2,1)S(1)}, bf16[512,128]{1,0:T(8,128)(2,1)S(1)}, u32[]{:S(2)}, u32[]{:S(2)}) collective-permute-start(bf16[512,128]{1,0:T(8,128)(2,1)S(1)} %get-tuple-element.37), channel_id=1, source_target_pairs={{0,1},{1,0},{2,3},{3,2},{4,5},{5,4},{6,7},{7,6},{8,9},{9,8},{10,11... | collective-permute-start | bytes 393224 | tf_op jit(solution)/shard_map/ppermute | solution.py:27

commit v7 on v6

--- a/solution.py
+++ b/solution.py
@@ -49,6 +49,34 @@
     rows = lax.broadcasted_iota(jnp.int32, (BLOCK, BLOCK), 0)
     cols = lax.broadcasted_iota(jnp.int32, (BLOCK, BLOCK), 1)
     return jnp.where(cols <= rows, weights, jnp.zeros_like(weights))
+
+
+PACKED = BLOCK // 4 + 8
+
+
+def packed(grad):
+    half = BLOCK // 2
+    rows = lax.broadcasted_iota(jnp.int32, (half, BLOCK), 0)
+    cols = lax.broadcasted_iota(jnp.int32, (half, BLOCK), 1)
+    turned = pltpu.roll(grad.T, half, 1)[:half]
+    body = grad[half:] + jnp.where(cols - half > rows, turned, 0.0)
+    spine = jnp.sum(jnp.where(rows == cols, grad[:half], 0.0), axis=0, keepdims=True)
+    spine = jnp.broadcast_to(spine, (8, BLOCK))
+    body = jnp.concatenate([body[: half // 2], body[half // 2 :]], axis=1)
+    return jnp.concatenate([body, jnp.concatenate([spine, spine], axis=1)], axis=0)
+
+
+def unpacked(terms):
+    half = BLOCK // 2
+    rows = lax.broadcasted_iota(jnp.int32, (half, BLOCK), 0)
+    cols = lax.broadcasted_iota(jnp.int32, (half, BLOCK), 1)
+    body = terms[: half // 2]
+    body = jnp.concatenate([body[:, :BLOCK], body[:, BLOCK:]], axis=0)
+    spine = jnp.broadcast_to(terms[half // 2 : half // 2 + 1, :BLOCK], (half, BLOCK))
+    above = jnp.where(cols - half > rows, body, 0.0)
+    top = jnp.concatenate([above, jnp.zeros_like(above)], axis=0).T[half:]
+    top = top + jnp.where(rows == cols, spine, 0.0)
+    return top, jnp.where(cols - half <= rows, body, 0.0)
 
 
 def nt(a, b, **kw):
@@ -143,17 +171,23 @@
         out[at : at + step] = array[:, at : at + step].T
 
 
-def norm_terms_body(full_width, sums, pre, grad, table, flipped, bias, gain, hidden_t, joined_out, out, held, made, come, gone):
-    n_x, n_all, rows, both = out.shape
+def norm_terms_body(full_width, sums, pre, grad, table, flipped, bias, gain, hidden_t, joined_out, out, held, made, mixed_made, come, gone):
+    deep, n_x, rows, both = made.shape[1:]
     parts, chunk, _ = held.shape
-    deep = (n_all - 1) // parts
+    n_z = parts * deep
     loads = [
         pltpu.make_async_copy(hidden_t.at[pl.ds(i * chunk, chunk)], held.at[i], come.at[i])
         for i in range(parts)
     ]
     stores = [
-        pltpu.make_async_copy(made.at[z], out.at[:, z], gone.at[z]) for z in range(n_all)
+        pltpu.make_async_copy(
+            made.at[z // deep, z % deep], out.at[:, pl.ds(z * rows, rows)], gone.at[z]
+        )
+        for z in range(n_z)
     ]
+    stores.append(
+        pltpu.make_async_copy(mixed_made, out.at[:, pl.ds(n_z * rows, PACKED)], gone.at[n_z])
+    )
     for load in loads:
         load.start()
     gating, mixed_grad, back, (pre_content, pre_gating) = branches(
@@ -181,16 +215,14 @@
         mixing_grad = term if mixing_grad is None else mixing_grad + term
     gating_back = inv_std * (back - first - centred * second)
     joined_out[:, width:] = (gating_back * gelu_slope(pre_gating)).astype(bf16)
-    mixing_grad = causal(mixing_grad).astype(bf16)
-    half = BLOCK // 2
-    mixing_term = jnp.concatenate([mixing_grad[:half], mixing_grad[half:]], axis=1)
+    mixing_term = packed(causal(mixing_grad)).astype(bf16)
     for x in range(n_x):
-        made[n_all - 1, x] = mixing_term
-    stores[n_all - 1].start()
+        mixed_made[x] = mixing_term
+    stores[n_z].start()
     for i in range(parts):
         loads[i].wait()
         term = nn(held[i], joined_out[...]).astype(bf16)
-        made[i * deep : (i + 1) * deep] = term.reshape(deep, n_x, rows, both)
+        made[i] = term.reshape(deep, n_x, rows, both)
         for z in range(i * deep, (i + 1) * deep):
             stores[z].start()
     for store in stores:
@@ -205,12 +237,13 @@
     near, far = pl.BlockSpec(memory_space=pltpu.VMEM), pl.BlockSpec(memory_space=pl.ANY)
     return pl.pallas_call(
         functools.partial(norm_terms_body, full_width),
-        out_shape=(like((tokens, both), bf16), stored((n_x, n_z + 1, rows, both), bf16)),
+        out_shape=(like((tokens, both), bf16), stored((n_x, n_z * rows + PACKED, both), bf16)),
         in_specs=[near] * len(small) + [far],
         out_specs=(near, far),
         scratch_shapes=[
             pltpu.VMEM((parts, width // parts, tokens), bf16),
-            pltpu.VMEM((n_z + 1, n_x, rows, both), bf16),
+            pltpu.VMEM((parts, n_z // parts, n_x, rows, both), bf16),
+            pltpu.VMEM((n_x, PACKED, both), bf16),
             pltpu.SemaphoreType.DMA((parts,)),
             pltpu.SemaphoreType.DMA((n_z + 1,)),
         ],
@@ -274,13 +307,14 @@
 
 def regroup_body(arrived, out):
     n_z = out.shape[0]
+    rows = out.shape[1] - PACKED
     total = arrived[0].astype(f32)
     for x in range(1, arrived.shape[0]):
         total = total + arrived[x].astype(f32)
     total = total.astype(bf16)
     for z in range(n_z):
-        out[z, 0] = total[z]
-        out[z, 1] = total[n_z]
+        out[z, :rows] = total[z * rows : (z + 1) * rows]
+        out[z, rows:] = total[n_z * rows :]
 
 
 def finish_body(scale, arrived, content_out, gating_out, mixing_out):
@@ -288,11 +322,12 @@
     for z in range(1, arrived.shape[0]):
         total = total + arrived[z].astype(f32)
     total = total * scale
-    half = content_out.shape[1]
-    content_out[...] = total[0][:, :half]
-    gating_out[...] = total[0][:, half:]
-    mixing_out[0, : BLOCK // 2] = total[1][:, :half]
-    mixing_out[0, BLOCK // 2 :] = total[1][:, half:]
+    rows, half = content_out.shape
+    content_out[...] = total[:rows, :half]
+    gating_out[...] = total[:rows, half:]
+    top, bottom = unpacked(total[rows:])
+    mixing_out[0, : BLOCK // 2] = top
+    mixing_out[0, BLOCK // 2 :] = bottom
 
 
 def step(
@@ -353,7 +388,7 @@
     other = sent_apart(other, 2, True)
     sent = swapped(send)
 
-    regrouped = call(regroup_body, stored((n_z, 2, shard_rows, both), bf16))(along_x)
+    regrouped = call(regroup_body, stored((n_z, shard_rows + PACKED, both), bf16))(along_x)
     arrived = exchange(regrouped, "sp_0")
 
     input_grad = call(total_body, outside(single, bf16))(own, same, other, keep, sent)

time: 123 us -> 122 us (level)
  no operation moved by 1% of the time
where the time goes in v7:
time: 122 us; the launch traced here: 121 us
  starting transfers between devices  41.9 us (34%)
  blocking collectives  36.9 us (30%)
  waiting for transfers between devices  25.9 us (21%)
  Pallas kernels  14.1 us (12%)
  local copies, waits for them, and re-layouts  1.77 us (1%)
    all_to_all x2, blocking collectives, exchange(): return lax.all_to_all(array, axis, split_axis=0, concat_axis=0, tiled=True)  36.9 us
    ppermute x4, starting transfers between devices, sent_apart(): return lax.ppermute(array, DP, moves)  18 us
    all_to_all x3, starting transfers between devices, exchange(): return lax.all_to_all(array, axis, split_axis=0, concat_axis=0, tiled=True)  17.6 us
    all_to_all x3, waiting for transfers between devices, exchange(): return lax.all_to_all(array, axis, split_axis=0, concat_axis=0, tiled=True)  16.6 us
    pallas_call x10, Pallas kernels, run(): return made(*operands)  10.3 us
    ppermute x4, waiting for transfers between devices, sent_apart(): return lax.ppermute(array, DP, moves)  9.23 us
    ppermute x3, starting transfers between devices, swapped(): return lax.ppermute(array, 'dp_1', [(0, 1), (1, 0)])  6.25 us
    pallas_call x1, Pallas kernels, norm_terms(): pl.pallas_call(functools.partial(norm_terms_body, full_width), out_shape=...  3.86 us
  transfers between devices with their start and end apart: 10, of which 4 were waited for; matrix products, arithmetic and copies ran while one was open for 0% of the time, Pallas kernels for 5%

profile of v7, /device:TPU:9, one launch (start us, length us, event | category | flops | bytes accessed | tf_op | source)
XLA Modules:
  0.0 121.4 jit_solution(16069106767270931459)
XLA Ops:
  0.6 0.0 copy-start.1
  0.6 0.0 copy-start.4
  0.7 0.0 copy-start
  0.7 0.0 copy-start.5
  0.7 1.6 %shard_map.102 = bf16[8,64,256]{2,1,0:T(8,128)(2,1)} custom-call(bf16[64,128]{1,0:T(8,128)(2,1)} %content.1, bf16[64,128]{1,0:T(8,128)(2,1)} %gating.1), custom_call_target="tpu_custom_call" | custom-call | tf_op jit(solution)/shard_map/pallas_call | solution.py:107
  2.3 20.5 %all_to_all.25.arrived = bf16[8,64,256]{2,1,0:T(8,128)(2,1)S(1)} all-to-all(bf16[8,64,256]{2,1,0:T(8,128)(2,1)} %shard_map.102), channel_id=1, replica_groups=mesh['sp_0'=8,'sp_1'=4,'dp_0'=8,'dp_1'=2] {'sp_0'}, dimensions={0} | all-to-all | bytes 524288 | tf_op jit(solution)/shard_map/all_to_all | solution.py:23
  22.8 0.1 shard_map.103
  22.9 16.4 %all_to_all.26.weight = bf16[4,8,64,256]{3,2,1,0:T(8,128)(2,1)S(1)} all-to-all(bf16[4,8,64,256]{3,2,1,0:T(8,128)(2,1)S(1)} %shard_map.103), channel_id=1, replica_groups=mesh['sp_0'=8,'sp_1'=4,'dp_0'=8,'dp_1'=2] {'sp_1'}, dimensions={0} | all-to-all | bytes 2097152 | tf_op jit(solution)/shard_map/all_to_all | solution.py:23
  39.3 0.0 copy-done.1
  39.3 0.0 copy-done.4
  39.3 0.0 copy-done
  39.3 0.0 copy-done.5
  39.3 1.8 %shard_map.104 = (bf16[512,256]{1,0:T(8,128)(2,1)S(1)}, f32[16,4,512]{2,1,0:T(4,128)}) custom-call(bf16[512,2048]{1,0:T(8,128)(2,1)S(1)} %copy-done, bf16[4,8,64,256]{3,2,1,0:T(8,128)(2,1)S(1)} %all_to_all.26.weight, bf16[1,128,128]{2,1,0:T(8,128)(2,1)S(1)} %copy-done.4, f32[1,128]{1,0:T(1,128)S(1)} %bitcast.11, bf16[512,128]{1,0:T(8,128)(2,1)S(1)} %copy-done.1), custom_call_target="tpu_custom_call" | custom-call | tf_op jit(solution)/shard_map/pallas_call | solution.py:107
  41.1 0.0 copy-start.2
  41.1 0.7 copy-done.2
  41.8 10.6 %all-to-all-start.2 = ((f32[16,4,512]{2,1,0:T(4,128)}), f32[16,4,512]{2,1,0:T(4,128)S(1)}, u32[]{:S(2)}, u32[]{:S(2)}) async-start(f32[16,4,512]{2,1,0:T(4,128)} %get-tuple-element.23), calls=%async_computation.2 | async-start | bytes 262144 | tf_op jit(solution)/shard_map/all_to_all | solution.py:23
  52.5 0.0 copy-start.6
  52.5 1.9 %shard_map.106.hidden_t = bf16[2048,512]{1,0:T(8,128)(2,1)} custom-call(bf16[512,2048]{1,0:T(8,128)(2,1)S(1)} %copy-done), custom_call_target="tpu_custom_call" | custom-call | tf_op jit(solution)/shard_map/pallas_call | solution.py:107
  54.4 0.1 stack.44.where
  54.5 0.9 shard_map.105
  55.4 4.9 %all-to-all-done.2.sums = f32[16,4,512]{2,1,0:T(4,128)S(1)} async-done(((f32[16,4,512]{2,1,0:T(4,128)}), f32[16,4,512]{2,1,0:T(4,128)S(1)}, u32[]{:S(2)}, u32[]{:S(2)}) %all-to-all-start.2) | async-done | bytes 131104 | tf_op jit(solution)/shard_map/all_to_all | solution.py:23
  60.3 0.0 copy-done.6
  60.3 0.9 copy-done.3
  61.2 3.9 %norm_terms.1 = (bf16[512,256]{1,0:T(8,128)(2,1)S(1)}, bf16[4,552,256]{2,1,0:T(8,128)(2,1)}) custom-call(f32[16,4,512]{2,1,0:T(4,128)S(1)} %all-to-all-done.2.sums, bf16[512,256]{1,0:T(8,128)(2,1)S(1)} %copy-done.3, bf16[512,128]{1,0:T(8,128)(2,1)S(1)} %copy-done.1, bf16[128,128]{1,0:T(8,128)(2,1)S(1)} %get-tuple-element.25.table, ...), custom_call_target="tpu_custom_call" | custom-call | tf_op jit(solution)/shard_map/norm_terms/pallas_call | solution.py:238
  65.1 0.0 copy-done.7
  65.1 3.5 %all-to-all-start.3 = ((bf16[4,552,256]{2,1,0:T(8,128)(2,1)}), bf16[4,552,256]{2,1,0:T(8,128)(2,1)S(1)}, u32[]{:S(2)}, u32[]{:S(2)}) async-start(bf16[4,552,256]{2,1,0:T(8,128)(2,1)} %get-tuple-element.38), calls=%async_computation.3 | async-start | bytes 2260992 | tf_op jit(solution)/shard_map/all_to_all | solution.py:23
  68.7 1.9 %collective-permute-start.1 = (bf16[1024,256]{1,0:T(8,128)(2,1)}, bf16[1024,256]{1,0:T(8,128)(2,1)S(1)}, u32[]{:S(2)}, u32[]{:S(2)}) collective-permute-start(bf16[1024,256]{1,0:T(8,128)(2,1)} %copy-done.7), channel_id=1, source_target_pairs={{0,1},{1,0},{2,3},{3,2},{4,5},{5,4},{6,7},{7,6},{8,9},{9,8},{10,11... | collective-permute-start | bytes 1572872 | tf_op jit(solution)/shard_map/ppermute | solution.py:27
  70.6 2.4 %collective-permute-start = (bf16[512,256]{1,0:T(8,128)(2,1)S(1)}, bf16[512,256]{1,0:T(8,128)(2,1)S(1)}, u32[]{:S(2)}, u32[]{:S(2)}) collective-permute-start(bf16[512,256]{1,0:T(8,128)(2,1)S(1)} %get-tuple-element.27.joined), channel_id=1, source_target_pairs={{0,1},{1,0},{2,3},{3,2},{4,5},{5,4},{6,7},{7,6},{8,9},{9,8},{10,11... | collective-permute-start | bytes 786440 | tf_op jit(solution)/shard_map/ppermute | solution.py:27
  73.0 11.7 %all-to-all-done.3.arrived = bf16[4,552,256]{2,1,0:T(8,128)(2,1)S(1)} async-done(((bf16[4,552,256]{2,1,0:T(8,128)(2,1)}), bf16[4,552,256]{2,1,0:T(8,128)(2,1)S(1)}, u32[]{:S(2)}, u32[]{:S(2)}) %all-to-all-start.3) | async-done | bytes 1130528 | tf_op jit(solution)/shard_map/all_to_all | solution.py:23
  84.7 0.9 shard_map.110
  85.6 3.5 %all-to-all-start.4 = ((bf16[8,104,256]{2,1,0:T(8,128)(2,1)}), bf16[8,104,256]{2,1,0:T(8,128)(2,1)S(1)}, u32[]{:S(2)}, u32[]{:S(2)}) async-start(bf16[8,104,256]{2,1,0:T(8,128)(2,1)} %shard_map.110), calls=%async_computation.4 | async-start | bytes 851968 | tf_op jit(solution)/shard_map/all_to_all | solution.py:23
  89.1 0.0 collective-permute-done.joined_far
  89.1 0.0 collective-permute-done.1.far
  89.1 0.9 shard_map.107
  90.0 3.2 %collective-permute-start.2 = (bf16[512,512]{1,0:T(8,128)(2,1)S(1)}, bf16[512,512]{1,0:T(8,128)(2,1)S(1)}, u32[]{:S(2)}, u32[]{:S(2)}) collective-permute-start(bf16[512,512]{1,0:T(8,128)(2,1)S(1)} %get-tuple-element.32), channel_id=1, source_target_pairs={{0,2},{1,15},{2,4},{3,1},{4,6},{5,3},{6,8},{7,5},{8,10},{9,7},{10,... | collective-permute-start | bytes 1572872 | tf_op jit(solution)/shard_map/ppermute | solution.py:36
  93.2 2.0 %collective-permute-start.3 = (bf16[512,128]{1,0:T(8,128)(2,1)S(1)}, bf16[512,128]{1,0:T(8,128)(2,1)S(1)}, u32[]{:S(2)}, u32[]{:S(2)}) collective-permute-start(bf16[512,128]{1,0:T(8,128)(2,1)S(1)} %get-tuple-element.33), channel_id=1, source_target_pairs={{0,4},{1,13},{2,6},{3,15},{4,8},{5,1},{6,10},{7,3},{8,12},{9,5},{1... | collective-permute-start | bytes 393224 | tf_op jit(solution)/shard_map/ppermute | solution.py:36
  95.2 6.4 %collective-permute-done.3.four = bf16[512,128]{1,0:T(8,128)(2,1)S(1)} collective-permute-done((bf16[512,128]{1,0:T(8,128)(2,1)S(1)}, bf16[512,128]{1,0:T(8,128)(2,1)S(1)}, u32[]{:S(2)}, u32[]{:S(2)}) %collective-permute-start.3) | collective-permute-done | bytes 131104 | tf_op jit(solution)/shard_map/ppermute | solution.py:36
  101.6 0.0 collective-permute-done.2.odd
  101.6 0.7 shard_map.108
  102.3 6.5 %collective-permute-start.4 = (bf16[512,128]{1,0:T(8,128)(2,1)S(1)}, bf16[512,128]{1,0:T(8,128)(2,1)S(1)}, u32[]{:S(2)}, u32[]{:S(2)}) collective-permute-start(bf16[512,128]{1,0:T(8,128)(2,1)S(1)} %get-tuple-element.34), channel_id=1, source_target_pairs={{0,4},{1,13},{2,6},{3,15},{4,8},{5,1},{6,10},{7,3},{8,12},{9,5},{1... | collective-permute-start | bytes 393224 | tf_op jit(solution)/shard_map/ppermute | solution.py:36
  108.8 6.3 %collective-permute-start.5 = (bf16[512,128]{1,0:T(8,128)(2,1)S(1)}, bf16[512,128]{1,0:T(8,128)(2,1)S(1)}, u32[]{:S(2)}, u32[]{:S(2)}) collective-permute-start(bf16[512,128]{1,0:T(8,128)(2,1)S(1)} %get-tuple-element.35), channel_id=1, source_target_pairs={{0,5},{1,12},{2,7},{3,14},{4,9},{5,0},{6,11},{7,2},{8,13},{9,4},{1... | collective-permute-start | bytes 393224 | tf_op jit(solution)/shard_map/ppermute | solution.py:36
  115.1 1.9 %collective-permute-start.6 = (bf16[512,128]{1,0:T(8,128)(2,1)S(1)}, bf16[512,128]{1,0:T(8,128)(2,1)S(1)}, u32[]{:S(2)}, u32[]{:S(2)}) collective-permute-start(bf16[512,128]{1,0:T(8,128)(2,1)S(1)} %get-tuple-element.37), channel_id=1, source_target_pairs={{0,1},{1,0},{2,3},{3,2},{4,5},{5,4},{6,7},{7,6},{8,9},{9,8},{10,11... | collective-permute-start | bytes 393224 | tf_op jit(solution)/shard_map/ppermute | solution.py:27
  117.0 0.0 collective-permute-done.4.same
  117.0 2.8 %collective-permute-done.5.other = bf16[512,128]{1,0:T(8,128)(2,1)S(1)} collective-permute-done((bf16[512,128]{1,0:T(8,128)(2,1)S(1)}, bf16[512,128]{1,0:T(8,128)(2,1)S(1)}, u32[]{:S(2)}, u32[]{:S(2)}) %collective-permute-start.5) | collective-permute-done | bytes 131104 | tf_op jit(solution)/shard_map/ppermute | solution.py:36
  119.9 0.0 collective-permute-done.6.sent
  119.9 0.7 shard_map.109
  120.6 0.0 all-to-all-done.4.arrived
  120.6 0.7 shard_map.111
  (2 shorter events, 0.0 us)
Async XLA Ops:
  0.6 38.6 %copy-start.1 = (bf16[512,128]{1,0:T(8,128)(2,1)S(1)}, bf16[512,128]{1,0:T(8,128)(2,1)}, u32[]{:S(2)}) copy-start(bf16[512,128]{1,0:T(8,128)(2,1)} %grad.3) | copy-start | bytes 393220
  0.6 38.6 %copy-start.4 = (bf16[1,128,128]{2,1,0:T(8,128)(2,1)S(1)}, bf16[1,128,128]{2,1,0:T(8,128)(2,1)}, u32[]{:S(2)}) copy-start(bf16[1,128,128]{2,1,0:T(8,128)(2,1)} %mixing.3) | copy-start | bytes 98308
  0.7 38.6 %copy-start = (bf16[512,2048]{1,0:T(8,128)(2,1)S(1)}, bf16[512,2048]{1,0:T(8,128)(2,1)}, u32[]{:S(2)}) copy-start(bf16[512,2048]{1,0:T(8,128)(2,1)} %array.1) | copy-start | bytes 6291460
  0.7 38.6 %copy-start.5 = (f32[128]{0:T(128)S(1)}, f32[128]{0:T(128)}, u32[]{:S(2)}) copy-start(f32[128]{0:T(128)} %param.10) | copy-start | bytes 1540
  41.1 0.7 copy-start.2
  41.8 18.5 %all-to-all-start.2 = ((f32[16,4,512]{2,1,0:T(4,128)}), f32[16,4,512]{2,1,0:T(4,128)S(1)}, u32[]{:S(2)}, u32[]{:S(2)}) async-start(f32[16,4,512]{2,1,0:T(4,128)} %get-tuple-element.23), calls=%async_computation.2 | async-start | bytes 262144 | tf_op jit(solution)/shard_map/all_to_all | solution.py:23
  52.5 7.8 %copy-start.6 = (f32[1,128]{1,0:T(1,128)S(1)}, f32[1,128]{1,0:T(1,128)}, u32[]{:S(2)}) copy-start(f32[1,128]{1,0:T(1,128)} %bias.1) | copy-start | bytes 1540
  55.4 9.7 %copy-start.7 = (bf16[1024,256]{1,0:T(8,128)(2,1)}, bf16[1024,256]{1,0:T(8,128)(2,1)S(1)}, u32[]{:S(2)}) copy-start(bf16[1024,256]{1,0:T(8,128)(2,1)S(1)} %get-tuple-element.29) | copy-start | bytes 1572868
  60.3 1.0 copy-start.3
  65.1 19.6 %all-to-all-start.3 = ((bf16[4,552,256]{2,1,0:T(8,128)(2,1)}), bf16[4,552,256]{2,1,0:T(8,128)(2,1)S(1)}, u32[]{:S(2)}, u32[]{:S(2)}) async-start(bf16[4,552,256]{2,1,0:T(8,128)(2,1)} %get-tuple-element.38), calls=%async_computation.3 | async-start | bytes 2260992 | tf_op jit(solution)/shard_map/all_to_all | solution.py:23
  68.7 20.5 %collective-permute-start.1 = (bf16[1024,256]{1,0:T(8,128)(2,1)}, bf16[1024,256]{1,0:T(8,128)(2,1)S(1)}, u32[]{:S(2)}, u32[]{:S(2)}) collective-permute-start(bf16[1024,256]{1,0:T(8,128)(2,1)} %copy-done.7), channel_id=1, source_target_pairs={{0,1},{1,0},{2,3},{3,2},{4,5},{5,4},{6,7},{7,6},{8,9},{9,8},{10,11... | collective-permute-start | bytes 1572872 | tf_op jit(solution)/shard_map/ppermute | solution.py:27
  70.6 18.5 %collective-permute-start = (bf16[512,256]{1,0:T(8,128)(2,1)S(1)}, bf16[512,256]{1,0:T(8,128)(2,1)S(1)}, u32[]{:S(2)}, u32[]{:S(2)}) collective-permute-start(bf16[512,256]{1,0:T(8,128)(2,1)S(1)} %get-tuple-element.27.joined), channel_id=1, source_target_pairs={{0,1},{1,0},{2,3},{3,2},{4,5},{5,4},{6,7},{7,6},{8,9},{9,8},{10,11... | collective-permute-start | bytes 786440 | tf_op jit(solution)/shard_map/ppermute | solution.py:27
  85.6 35.0 %all-to-all-start.4 = ((bf16[8,104,256]{2,1,0:T(8,128)(2,1)}), bf16[8,104,256]{2,1,0:T(8,128)(2,1)S(1)}, u32[]{:S(2)}, u32[]{:S(2)}) async-start(bf16[8,104,256]{2,1,0:T(8,128)(2,1)} %shard_map.110), calls=%async_computation.4 | async-start | bytes 851968 | tf_op jit(solution)/shard_map/all_to_all | solution.py:23
  90.0 11.6 %collective-permute-start.2 = (bf16[512,512]{1,0:T(8,128)(2,1)S(1)}, bf16[512,512]{1,0:T(8,128)(2,1)S(1)}, u32[]{:S(2)}, u32[]{:S(2)}) collective-permute-start(bf16[512,512]{1,0:T(8,128)(2,1)S(1)} %get-tuple-element.32), channel_id=1, source_target_pairs={{0,2},{1,15},{2,4},{3,1},{4,6},{5,3},{6,8},{7,5},{8,10},{9,7},{10,... | collective-permute-start | bytes 1572872 | tf_op jit(solution)/shard_map/ppermute | solution.py:36
  93.2 8.4 %collective-permute-start.3 = (bf16[512,128]{1,0:T(8,128)(2,1)S(1)}, bf16[512,128]{1,0:T(8,128)(2,1)S(1)}, u32[]{:S(2)}, u32[]{:S(2)}) collective-permute-start(bf16[512,128]{1,0:T(8,128)(2,1)S(1)} %get-tuple-element.33), channel_id=1, source_target_pairs={{0,4},{1,13},{2,6},{3,15},{4,8},{5,1},{6,10},{7,3},{8,12},{9,5},{1... | collective-permute-start | bytes 393224 | tf_op jit(solution)/shard_map/ppermute | solution.py:36
  102.3 14.8 %collective-permute-start.4 = (bf16[512,128]{1,0:T(8,128)(2,1)S(1)}, bf16[512,128]{1,0:T(8,128)(2,1)S(1)}, u32[]{:S(2)}, u32[]{:S(2)}) collective-permute-start(bf16[512,128]{1,0:T(8,128)(2,1)S(1)} %get-tuple-element.34), channel_id=1, source_target_pairs={{0,4},{1,13},{2,6},{3,15},{4,8},{5,1},{6,10},{7,3},{8,12},{9,5},{1... | collective-permute-start | bytes 393224 | tf_op jit(solution)/shard_map/ppermute | solution.py:36
  108.8 11.1 %collective-permute-start.5 = (bf16[512,128]{1,0:T(8,128)(2,1)S(1)}, bf16[512,128]{1,0:T(8,128)(2,1)S(1)}, u32[]{:S(2)}, u32[]{:S(2)}) collective-permute-start(bf16[512,128]{1,0:T(8,128)(2,1)S(1)} %get-tuple-element.35), channel_id=1, source_target_pairs={{0,5},{1,12},{2,7},{3,14},{4,9},{5,0},{6,11},{7,2},{8,13},{9,4},{1... | collective-permute-start | bytes 393224 | tf_op jit(solution)/shard_map/ppermute | solution.py:36
  115.1 4.8 %collective-permute-start.6 = (bf16[512,128]{1,0:T(8,128)(2,1)S(1)}, bf16[512,128]{1,0:T(8,128)(2,1)S(1)}, u32[]{:S(2)}, u32[]{:S(2)}) collective-permute-start(bf16[512,128]{1,0:T(8,128)(2,1)S(1)} %get-tuple-element.37), channel_id=1, source_target_pairs={{0,1},{1,0},{2,3},{3,2},{4,5},{5,4},{6,7},{7,6},{8,9},{9,8},{10,11... | collective-permute-start | bytes 393224 | tf_op jit(solution)/shard_map/ppermute | solution.py:27

commit v8 on v7

--- a/solution.py
+++ b/solution.py
@@ -165,19 +165,22 @@
         out[peer] = arrived[...]
 
 
-def flip_body(array, out):
-    step = 256
-    for at in range(0, array.shape[1], step):
-        out[at : at + step] = array[:, at : at + step].T
-
-
-def norm_terms_body(full_width, sums, pre, grad, table, flipped, bias, gain, hidden_t, joined_out, out, held, made, mixed_made, come, gone):
+def flip_body(array, top, bottom):
+    step, half = 256, top.shape[0]
+    for at in range(0, half, step):
+        top[at : at + step] = array[:, at : at + step].T
+        bottom[at : at + step] = array[:, half + at : half + at + step].T
+
+
+def norm_terms_body(full_width, sums, pre, grad, table, flipped, bias, gain, top, bottom, joined_out, out, held, made, mixed_made, come, gone):
     deep, n_x, rows, both = made.shape[1:]
-    parts, chunk, _ = held.shape
+    later, chunk, _ = held.shape
+    parts = made.shape[0]
+    ready = parts - later
     n_z = parts * deep
     loads = [
-        pltpu.make_async_copy(hidden_t.at[pl.ds(i * chunk, chunk)], held.at[i], come.at[i])
-        for i in range(parts)
+        pltpu.make_async_copy(bottom.at[pl.ds(i * chunk, chunk)], held.at[i], come.at[i])
+        for i in range(later)
     ]
     stores = [
         pltpu.make_async_copy(
@@ -220,8 +223,12 @@
         mixed_made[x] = mixing_term
     stores[n_z].start()
     for i in range(parts):
-        loads[i].wait()
-        term = nn(held[i], joined_out[...]).astype(bf16)
+        if i < ready:
+            slab = top[i * chunk : (i + 1) * chunk]
+        else:
+            loads[i - ready].wait()
+            slab = held[i - ready]
+        term = nn(slab, joined_out[...]).astype(bf16)
         made[i] = term.reshape(deep, n_x, rows, both)
         for z in range(i * deep, (i + 1) * deep):
             stores[z].start()
@@ -229,8 +236,8 @@
         store.wait()
 
 
-def norm_terms(full_width, small, hidden_t, n_x, n_z):
-    width, tokens = hidden_t.shape
+def norm_terms(full_width, small, top, bottom, n_x, n_z):
+    width, tokens = 2 * top.shape[0], top.shape[1]
     both = 2 * small[2].shape[1]
     rows = width // (n_x * n_z)
     parts = 4
@@ -238,20 +245,20 @@
     return pl.pallas_call(
         functools.partial(norm_terms_body, full_width),
         out_shape=(like((tokens, both), bf16), stored((n_x, n_z * rows + PACKED, both), bf16)),
-        in_specs=[near] * len(small) + [far],
+        in_specs=[near] * (len(small) + 1) + [far],
         out_specs=(near, far),
         scratch_shapes=[
-            pltpu.VMEM((parts, width // parts, tokens), bf16),
+            pltpu.VMEM((parts // 2, width // parts, tokens), bf16),
             pltpu.VMEM((parts, n_z // parts, n_x, rows, both), bf16),
             pltpu.VMEM((n_x, PACKED, both), bf16),
-            pltpu.SemaphoreType.DMA((parts,)),
+            pltpu.SemaphoreType.DMA((parts // 2,)),
             pltpu.SemaphoreType.DMA((n_z + 1,)),
         ],
         compiler_params=pltpu.CompilerParams(vmem_limit_bytes=20 * 1024 * 1024),
         name="norm_terms",
     )(
-        *[pltpu.with_memory_space_constraint(a, pltpu.VMEM) for a in small],
-        pltpu.with_memory_space_constraint(hidden_t, pltpu.HBM),
+        *[pltpu.with_memory_space_constraint(a, pltpu.VMEM) for a in (*small, top)],
+        pltpu.with_memory_space_constraint(bottom, pltpu.HBM),
     )
 
 
@@ -349,7 +356,8 @@
     where = jnp.stack(ahead + behind + [core]).astype(jnp.int32)
     gain = norm_gain[None, :]
 
-    hidden_t = call(flip_body, stored((width, tok_rows), bf16))(hidden_in)
+    half = (width // 2, tok_rows)
+    top, bottom = call(flip_body, (like(half, bf16), stored(half, bf16)))(hidden_in)
     shards = call(join_body, stored((n_z, shard_rows, both), bf16), cold=(0, 1))(
         content_weight, gating_weight
     )
@@ -360,7 +368,10 @@
     wide_pair, picked = (tok_rows, 4 * out_cols), (width // 2, both)
     square = like((BLOCK, BLOCK), bf16)
     mine, theirs, table, flipped = call(
-        pick_body, (like(picked, bf16), like(picked, bf16), square, square), scalars=True, cold=(2,)
+        pick_body,
+        (stored(picked, bf16), stored(picked, bf16), square, square),
+        scalars=True,
+        cold=(2,),
     )(where, weight, mixing_weight)
     far = swapped(theirs)
 
@@ -370,7 +381,7 @@
     )(hidden_in, weight, mixing_weight, gain, out_grad)
     sums = exchange(sums, DP)
     small = (sums, pre, out_grad, table, flipped, mixing_bias, gain)
-    joined, terms = norm_terms(full_width, small, hidden_t, n_x, n_z)
+    joined, terms = norm_terms(full_width, small, top, bottom, n_x, n_z)
 
     joined_far = swapped(joined)
     along_x = exchange(terms, "sp_1")
@@ -378,6 +389,7 @@
     odd, two, four, own = call(
         input_terms_body,
         (like(wide_pair, bf16), like(pair, f32), like(single, bf16), like(single, f32)),
+        cold=(2,),
     )(joined, joined_far, mine, far)
     four = sent_apart(four, 2)
     odd = sent_apart(odd, 1)

time: 122 us -> 123 us (level)
  Pallas kernels: 14.1 us -> 15.8 us
  waiting for transfers between devices: 25.9 us -> 24.5 us
    all_to_all x3, waiting for transfers between devices: 16.6 us -> 15 us  [exchange(): return lax.all_to_all(array, axis, split_axis=0, concat_axis=0, tiled=True)]
    pallas_call x10, Pallas kernels: 10.3 us -> 11.9 us  [run(): return made(*operands)]
    unnamed x16 -> x18, local copies, waits for them, and re-layouts: 1.68 us -> 2.67 us
  transfers between devices with their start and end apart: 10 -> 10, of which waited for: 4 -> 4; matrix products, arithmetic and copies ran while one was open for 0% -> 0% of each run, Pallas kernels for 5% -> 6%
where the time goes in v8:
time: 123 us; the launch traced here: 122 us
  starting transfers between devices  41.6 us (34%)
  blocking collectives  37.1 us (30%)
  waiting for transfers between devices  24.5 us (20%)
  Pallas kernels  15.8 us (13%)
  local copies, waits for them, and re-layouts  2.75 us (2%)
    all_to_all x2, blocking collectives, exchange(): return lax.all_to_all(array, axis, split_axis=0, concat_axis=0, tiled=True)  37.1 us
    ppermute x4, starting transfers between devices, sent_apart(): return lax.ppermute(array, DP, moves)  17.7 us
    all_to_all x3, starting transfers between devices, exchange(): return lax.all_to_all(array, axis, split_axis=0, concat_axis=0, tiled=True)  17.6 us
    all_to_all x3, waiting for transfers between devices, exchange(): return lax.all_to_all(array, axis, split_axis=0, concat_axis=0, tiled=True)  15 us
    pallas_call x10, Pallas kernels, run(): return made(*operands)  11.9 us
    ppermute x4, waiting for transfers between devices, sent_apart(): return lax.ppermute(array, DP, moves)  9.49 us
    ppermute x3, starting transfers between devices, swapped(): return lax.ppermute(array, 'dp_1', [(0, 1), (1, 0)])  6.25 us
    pallas_call x1, Pallas kernels, norm_terms(): pl.pallas_call(functools.partial(norm_terms_body, full_width), out_shape=...  3.9 us
  transfers between devices with their start and end apart: 10, of which 4 were waited for; matrix products, arithmetic and copies ran while one was open for 0% of the time, Pallas kernels for 6%

profile of v8, /device:TPU:9, one launch (start us, length us, event | category | flops | bytes accessed | tf_op | source)
XLA Modules:
  0.0 122.4 jit_solution(172620706181673229)
XLA Ops:
  0.6 1.5 %shard_map.102 = bf16[8,64,256]{2,1,0:T(8,128)(2,1)} custom-call(bf16[64,128]{1,0:T(8,128)(2,1)} %content.1, bf16[64,128]{1,0:T(8,128)(2,1)} %gating.1), custom_call_target="tpu_custom_call" | custom-call | tf_op jit(solution)/shard_map/pallas_call | solution.py:107
  2.1 20.5 %all_to_all.25.arrived = bf16[8,64,256]{2,1,0:T(8,128)(2,1)S(1)} all-to-all(bf16[8,64,256]{2,1,0:T(8,128)(2,1)} %shard_map.102), channel_id=1, replica_groups=mesh['sp_0'=8,'sp_1'=4,'dp_0'=8,'dp_1'=2] {'sp_0'}, dimensions={0} | all-to-all | bytes 524288 | tf_op jit(solution)/shard_map/all_to_all | solution.py:23
  22.6 0.0 copy-start.3
  22.6 0.0 copy-start.6
  22.6 0.1 shard_map.103
  22.7 0.0 copy-start
  22.7 0.0 copy-start.7
  22.7 16.5 %all_to_all.26.weight = bf16[4,8,64,256]{3,2,1,0:T(8,128)(2,1)S(1)} all-to-all(bf16[4,8,64,256]{3,2,1,0:T(8,128)(2,1)S(1)} %shard_map.103), channel_id=1, replica_groups=mesh['sp_0'=8,'sp_1'=4,'dp_0'=8,'dp_1'=2] {'sp_1'}, dimensions={0} | all-to-all | bytes 2097152 | tf_op jit(solution)/shard_map/all_to_all | solution.py:23
  39.3 0.0 copy-done.3
  39.3 0.0 copy-done.6
  39.3 0.0 copy-done
  39.3 0.0 copy-done.7
  39.3 1.8 %shard_map.104 = (bf16[512,256]{1,0:T(8,128)(2,1)S(1)}, f32[16,4,512]{2,1,0:T(4,128)}) custom-call(bf16[512,2048]{1,0:T(8,128)(2,1)S(1)} %copy-done, bf16[4,8,64,256]{3,2,1,0:T(8,128)(2,1)S(1)} %all_to_all.26.weight, bf16[1,128,128]{2,1,0:T(8,128)(2,1)S(1)} %copy-done.6, f32[1,128]{1,0:T(1,128)S(1)} %bitcast.11, bf16[512,128]{1,0:T(8,128)(2,1)S(1)} %copy-done.3), custom_call_target="tpu_custom_call" | custom-call | tf_op jit(solution)/shard_map/pallas_call | solution.py:107
  41.1 0.0 copy-start.4
  41.1 0.7 copy-done.4
  41.8 10.6 %all-to-all-start.2 = ((f32[16,4,512]{2,1,0:T(4,128)}), f32[16,4,512]{2,1,0:T(4,128)S(1)}, u32[]{:S(2)}, u32[]{:S(2)}) async-start(f32[16,4,512]{2,1,0:T(4,128)} %get-tuple-element.25), calls=%async_computation.2 | async-start | bytes 262144 | tf_op jit(solution)/shard_map/all_to_all | solution.py:23
  52.5 1.6 %shard_map.106 = (bf16[1024,512]{1,0:T(8,128)(2,1)S(1)}, bf16[1024,512]{1,0:T(8,128)(2,1)}) custom-call(bf16[512,2048]{1,0:T(8,128)(2,1)S(1)} %copy-done), custom_call_target="tpu_custom_call" | custom-call | tf_op jit(solution)/shard_map/pallas_call | solution.py:107
  54.1 1.0 copy-done.1
  55.1 0.1 stack.44.where
  55.1 1.9 %shard_map.105 = (bf16[1024,256]{1,0:T(8,128)(2,1)}, bf16[1024,256]{1,0:T(8,128)(2,1)}, bf16[128,128]{1,0:T(8,128)(2,1)S(1)}, bf16[128,128]{1,0:T(8,128)(2,1)S(1)}) custom-call(s32[11]{0:T(128)S(1)} %stack.44.where, bf16[4,8,64,256]{3,2,1,0:T(8,128)(2,1)S(1)} %all_to_all.26.weight, bf16[1,128,128]{2,1,0:T(8,128)(2,1)} %mixing.3), custom_call_target="tpu_custom_call" | custom-call | tf_op jit(solution)/shard_map/pallas_call | solution.py:107
  57.0 3.2 %all-to-all-done.2.sums = f32[16,4,512]{2,1,0:T(4,128)S(1)} async-done(((f32[16,4,512]{2,1,0:T(4,128)}), f32[16,4,512]{2,1,0:T(4,128)S(1)}, u32[]{:S(2)}, u32[]{:S(2)}) %all-to-all-start.2) | async-done | bytes 131104 | tf_op jit(solution)/shard_map/all_to_all | solution.py:23
  60.3 0.0 copy-done.8
  60.3 0.0 copy-done.2
  60.3 0.9 copy-done.5
  61.2 3.9 %norm_terms.1 = (bf16[512,256]{1,0:T(8,128)(2,1)S(1)}, bf16[4,552,256]{2,1,0:T(8,128)(2,1)}) custom-call(f32[16,4,512]{2,1,0:T(4,128)S(1)} %all-to-all-done.2.sums, bf16[512,256]{1,0:T(8,128)(2,1)S(1)} %copy-done.5, bf16[512,128]{1,0:T(8,128)(2,1)S(1)} %copy-done.3, bf16[128,128]{1,0:T(8,128)(2,1)S(1)} %get-tuple-element.27.table, ...), custom_call_target="tpu_custom_call" | custom-call | tf_op jit(solution)/shard_map/norm_terms/pallas_call | solution.py:245
  65.1 3.5 %all-to-all-start.3 = ((bf16[4,552,256]{2,1,0:T(8,128)(2,1)}), bf16[4,552,256]{2,1,0:T(8,128)(2,1)S(1)}, u32[]{:S(2)}, u32[]{:S(2)}) async-start(bf16[4,552,256]{2,1,0:T(8,128)(2,1)} %get-tuple-element.42), calls=%async_computation.3 | async-start | bytes 2260992 | tf_op jit(solution)/shard_map/all_to_all | solution.py:23
  68.7 1.9 %collective-permute-start.1 = (bf16[1024,256]{1,0:T(8,128)(2,1)}, bf16[1024,256]{1,0:T(8,128)(2,1)S(1)}, u32[]{:S(2)}, u32[]{:S(2)}) collective-permute-start(bf16[1024,256]{1,0:T(8,128)(2,1)} %get-tuple-element.33), channel_id=1, source_target_pairs={{0,1},{1,0},{2,3},{3,2},{4,5},{5,4},{6,7},{7,6},{8,9},{9,8},{10,11... | collective-permute-start | bytes 1572872 | tf_op jit(solution)/shard_map/ppermute | solution.py:27
  70.6 2.4 %collective-permute-start = (bf16[512,256]{1,0:T(8,128)(2,1)S(1)}, bf16[512,256]{1,0:T(8,128)(2,1)S(1)}, u32[]{:S(2)}, u32[]{:S(2)}) collective-permute-start(bf16[512,256]{1,0:T(8,128)(2,1)S(1)} %get-tuple-element.31.joined), channel_id=1, source_target_pairs={{0,1},{1,0},{2,3},{3,2},{4,5},{5,4},{6,7},{7,6},{8,9},{9,8},{10,11... | collective-permute-start | bytes 786440 | tf_op jit(solution)/shard_map/ppermute | solution.py:27
  73.0 11.7 %all-to-all-done.3.arrived = bf16[4,552,256]{2,1,0:T(8,128)(2,1)S(1)} async-done(((bf16[4,552,256]{2,1,0:T(8,128)(2,1)}), bf16[4,552,256]{2,1,0:T(8,128)(2,1)S(1)}, u32[]{:S(2)}, u32[]{:S(2)}) %all-to-all-start.3) | async-done | bytes 1130528 | tf_op jit(solution)/shard_map/all_to_all | solution.py:23
  84.7 0.9 shard_map.110
  85.7 3.5 %all-to-all-start.4 = ((bf16[8,104,256]{2,1,0:T(8,128)(2,1)}), bf16[8,104,256]{2,1,0:T(8,128)(2,1)S(1)}, u32[]{:S(2)}, u32[]{:S(2)}) async-start(bf16[8,104,256]{2,1,0:T(8,128)(2,1)} %shard_map.110), calls=%async_computation.4 | async-start | bytes 851968 | tf_op jit(solution)/shard_map/all_to_all | solution.py:23
  89.1 0.0 collective-permute-done.joined_far
  89.1 0.0 collective-permute-done.1.far
  89.1 1.9 %shard_map.107 = (bf16[512,512]{1,0:T(8,128)(2,1)S(1)}, f32[512,256]{1,0:T(8,128)S(1)}, bf16[512,128]{1,0:T(8,128)(2,1)S(1)}, f32[512,128]{1,0:T(8,128)S(1)}) custom-call(bf16[512,256]{1,0:T(8,128)(2,1)S(1)} %get-tuple-element.31.joined, bf16[512,256]{1,0:T(8,128)(2,1)S(1)} %collective-permute-done.joined_far, bf16[1024,256]{1,0:T(8,128)(2,1)} %get-tuple-element.32.mine, ...), custom_call_target="tpu_custom_call" | custom-call | tf_op jit(solution)/shard_map/pallas_call | solution.py:107
  91.1 3.2 %collective-permute-start.2 = (bf16[512,512]{1,0:T(8,128)(2,1)S(1)}, bf16[512,512]{1,0:T(8,128)(2,1)S(1)}, u32[]{:S(2)}, u32[]{:S(2)}) collective-permute-start(bf16[512,512]{1,0:T(8,128)(2,1)S(1)} %get-tuple-element.36), channel_id=1, source_target_pairs={{0,2},{1,15},{2,4},{3,1},{4,6},{5,3},{6,8},{7,5},{8,10},{9,7},{10,... | collective-permute-start | bytes 1572872 | tf_op jit(solution)/shard_map/ppermute | solution.py:36
  94.3 2.0 %collective-permute-start.3 = (bf16[512,128]{1,0:T(8,128)(2,1)S(1)}, bf16[512,128]{1,0:T(8,128)(2,1)S(1)}, u32[]{:S(2)}, u32[]{:S(2)}) collective-permute-start(bf16[512,128]{1,0:T(8,128)(2,1)S(1)} %get-tuple-element.37), channel_id=1, source_target_pairs={{0,4},{1,13},{2,6},{3,15},{4,8},{5,1},{6,10},{7,3},{8,12},{9,5},{1... | collective-permute-start | bytes 393224 | tf_op jit(solution)/shard_map/ppermute | solution.py:36
  96.2 6.6 %collective-permute-done.3.four = bf16[512,128]{1,0:T(8,128)(2,1)S(1)} collective-permute-done((bf16[512,128]{1,0:T(8,128)(2,1)S(1)}, bf16[512,128]{1,0:T(8,128)(2,1)S(1)}, u32[]{:S(2)}, u32[]{:S(2)}) %collective-permute-start.3) | collective-permute-done | bytes 131104 | tf_op jit(solution)/shard_map/ppermute | solution.py:36
  102.9 0.0 collective-permute-done.2.odd
  102.9 0.7 shard_map.108
  103.6 6.3 %collective-permute-start.4 = (bf16[512,128]{1,0:T(8,128)(2,1)S(1)}, bf16[512,128]{1,0:T(8,128)(2,1)S(1)}, u32[]{:S(2)}, u32[]{:S(2)}) collective-permute-start(bf16[512,128]{1,0:T(8,128)(2,1)S(1)} %get-tuple-element.38), channel_id=1, source_target_pairs={{0,4},{1,13},{2,6},{3,15},{4,8},{5,1},{6,10},{7,3},{8,12},{9,5},{1... | collective-permute-start | bytes 393224 | tf_op jit(solution)/shard_map/ppermute | solution.py:36
  109.9 6.3 %collective-permute-start.5 = (bf16[512,128]{1,0:T(8,128)(2,1)S(1)}, bf16[512,128]{1,0:T(8,128)(2,1)S(1)}, u32[]{:S(2)}, u32[]{:S(2)}) collective-permute-start(bf16[512,128]{1,0:T(8,128)(2,1)S(1)} %get-tuple-element.39), channel_id=1, source_target_pairs={{0,5},{1,12},{2,7},{3,14},{4,9},{5,0},{6,11},{7,2},{8,13},{9,4},{1... | collective-permute-start | bytes 393224 | tf_op jit(solution)/shard_map/ppermute | solution.py:36
  116.2 1.9 %collective-permute-start.6 = (bf16[512,128]{1,0:T(8,128)(2,1)S(1)}, bf16[512,128]{1,0:T(8,128)(2,1)S(1)}, u32[]{:S(2)}, u32[]{:S(2)}) collective-permute-start(bf16[512,128]{1,0:T(8,128)(2,1)S(1)} %get-tuple-element.41), channel_id=1, source_target_pairs={{0,1},{1,0},{2,3},{3,2},{4,5},{5,4},{6,7},{7,6},{8,9},{9,8},{10,11... | collective-permute-start | bytes 393224 | tf_op jit(solution)/shard_map/ppermute | solution.py:27
  118.1 0.0 collective-permute-done.4.same
  118.1 2.8 %collective-permute-done.5.other = bf16[512,128]{1,0:T(8,128)(2,1)S(1)} collective-permute-done((bf16[512,128]{1,0:T(8,128)(2,1)S(1)}, bf16[512,128]{1,0:T(8,128)(2,1)S(1)}, u32[]{:S(2)}, u32[]{:S(2)}) %collective-permute-start.5) | collective-permute-done | bytes 131104 | tf_op jit(solution)/shard_map/ppermute | solution.py:36
  120.9 0.0 collective-permute-done.6.sent
  120.9 0.7 shard_map.109
  121.7 0.0 all-to-all-done.4.arrived
  121.7 0.7 shard_map.111
  (4 shorter events, 0.0 us)
Async XLA Ops:
  22.6 16.6 %copy-start.3 = (bf16[512,128]{1,0:T(8,128)(2,1)S(1)}, bf16[512,128]{1,0:T(8,128)(2,1)}, u32[]{:S(2)}) copy-start(bf16[512,128]{1,0:T(8,128)(2,1)} %grad.3) | copy-start | bytes 393220
  22.6 16.6 %copy-start.6 = (bf16[1,128,128]{2,1,0:T(8,128)(2,1)S(1)}, bf16[1,128,128]{2,1,0:T(8,128)(2,1)}, u32[]{:S(2)}) copy-start(bf16[1,128,128]{2,1,0:T(8,128)(2,1)} %mixing.3) | copy-start | bytes 98308
  22.7 16.6 %copy-start = (bf16[512,2048]{1,0:T(8,128)(2,1)S(1)}, bf16[512,2048]{1,0:T(8,128)(2,1)}, u32[]{:S(2)}) copy-start(bf16[512,2048]{1,0:T(8,128)(2,1)} %array.1) | copy-start | bytes 6291460
  22.7 16.5 %copy-start.7 = (f32[128]{0:T(128)S(1)}, f32[128]{0:T(128)}, u32[]{:S(2)}) copy-start(f32[128]{0:T(128)} %param.10) | copy-start | bytes 1540
  41.1 0.7 copy-start.4
  41.8 18.5 %all-to-all-start.2 = ((f32[16,4,512]{2,1,0:T(4,128)}), f32[16,4,512]{2,1,0:T(4,128)S(1)}, u32[]{:S(2)}, u32[]{:S(2)}) async-start(f32[16,4,512]{2,1,0:T(4,128)} %get-tuple-element.25), calls=%async_computation.2 | async-start | bytes 262144 | tf_op jit(solution)/shard_map/all_to_all | solution.py:23
  52.5 7.8 %copy-start.8 = (f32[1,128]{1,0:T(1,128)S(1)}, f32[1,128]{1,0:T(1,128)}, u32[]{:S(2)}) copy-start(f32[1,128]{1,0:T(1,128)} %bias.1) | copy-start | bytes 1540
  54.1 1.0 copy-start.1
  55.1 5.2 %copy-start.2 = (bf16[1024,512]{1,0:T(8,128)(2,1)S(1)}, bf16[1024,512]{1,0:T(8,128)(2,1)}, u32[]{:S(2)}) copy-start(bf16[1024,512]{1,0:T(8,128)(2,1)} %copy-done.1) | copy-start | bytes 3145732
  60.3 1.0 copy-start.5
  65.1 19.6 %all-to-all-start.3 = ((bf16[4,552,256]{2,1,0:T(8,128)(2,1)}), bf16[4,552,256]{2,1,0:T(8,128)(2,1)S(1)}, u32[]{:S(2)}, u32[]{:S(2)}) async-start(bf16[4,552,256]{2,1,0:T(8,128)(2,1)} %get-tuple-element.42), calls=%async_computation.3 | async-start | bytes 2260992 | tf_op jit(solution)/shard_map/all_to_all | solution.py:23
  68.7 20.5 %collective-permute-start.1 = (bf16[1024,256]{1,0:T(8,128)(2,1)}, bf16[1024,256]{1,0:T(8,128)(2,1)S(1)}, u32[]{:S(2)}, u32[]{:S(2)}) collective-permute-start(bf16[1024,256]{1,0:T(8,128)(2,1)} %get-tuple-element.33), channel_id=1, source_target_pairs={{0,1},{1,0},{2,3},{3,2},{4,5},{5,4},{6,7},{7,6},{8,9},{9,8},{10,11... | collective-permute-start | bytes 1572872 | tf_op jit(solution)/shard_map/ppermute | solution.py:27
  70.6 18.5 %collective-permute-start = (bf16[512,256]{1,0:T(8,128)(2,1)S(1)}, bf16[512,256]{1,0:T(8,128)(2,1)S(1)}, u32[]{:S(2)}, u32[]{:S(2)}) collective-permute-start(bf16[512,256]{1,0:T(8,128)(2,1)S(1)} %get-tuple-element.31.joined), channel_id=1, source_target_pairs={{0,1},{1,0},{2,3},{3,2},{4,5},{5,4},{6,7},{7,6},{8,9},{9,8},{10,11... | collective-permute-start | bytes 786440 | tf_op jit(solution)/shard_map/ppermute | solution.py:27
  85.7 36.0 %all-to-all-start.4 = ((bf16[8,104,256]{2,1,0:T(8,128)(2,1)}), bf16[8,104,256]{2,1,0:T(8,128)(2,1)S(1)}, u32[]{:S(2)}, u32[]{:S(2)}) async-start(bf16[8,104,256]{2,1,0:T(8,128)(2,1)} %shard_map.110), calls=%async_computation.4 | async-start | bytes 851968 | tf_op jit(solution)/shard_map/all_to_all | solution.py:23
  91.1 11.8 %collective-permute-start.2 = (bf16[512,512]{1,0:T(8,128)(2,1)S(1)}, bf16[512,512]{1,0:T(8,128)(2,1)S(1)}, u32[]{:S(2)}, u32[]{:S(2)}) collective-permute-start(bf16[512,512]{1,0:T(8,128)(2,1)S(1)} %get-tuple-element.36), channel_id=1, source_target_pairs={{0,2},{1,15},{2,4},{3,1},{4,6},{5,3},{6,8},{7,5},{8,10},{9,7},{10,... | collective-permute-start | bytes 1572872 | tf_op jit(solution)/shard_map/ppermute | solution.py:36
  94.3 8.6 %collective-permute-start.3 = (bf16[512,128]{1,0:T(8,128)(2,1)S(1)}, bf16[512,128]{1,0:T(8,128)(2,1)S(1)}, u32[]{:S(2)}, u32[]{:S(2)}) collective-permute-start(bf16[512,128]{1,0:T(8,128)(2,1)S(1)} %get-tuple-element.37), channel_id=1, source_target_pairs={{0,4},{1,13},{2,6},{3,15},{4,8},{5,1},{6,10},{7,3},{8,12},{9,5},{1... | collective-permute-start | bytes 393224 | tf_op jit(solution)/shard_map/ppermute | solution.py:36
  103.6 14.5 %collective-permute-start.4 = (bf16[512,128]{1,0:T(8,128)(2,1)S(1)}, bf16[512,128]{1,0:T(8,128)(2,1)S(1)}, u32[]{:S(2)}, u32[]{:S(2)}) collective-permute-start(bf16[512,128]{1,0:T(8,128)(2,1)S(1)} %get-tuple-element.38), channel_id=1, source_target_pairs={{0,4},{1,13},{2,6},{3,15},{4,8},{5,1},{6,10},{7,3},{8,12},{9,5},{1... | collective-permute-start | bytes 393224 | tf_op jit(solution)/shard_map/ppermute | solution.py:36
  109.9 11.1 %collective-permute-start.5 = (bf16[512,128]{1,0:T(8,128)(2,1)S(1)}, bf16[512,128]{1,0:T(8,128)(2,1)S(1)}, u32[]{:S(2)}, u32[]{:S(2)}) collective-permute-start(bf16[512,128]{1,0:T(8,128)(2,1)S(1)} %get-tuple-element.39), channel_id=1, source_target_pairs={{0,5},{1,12},{2,7},{3,14},{4,9},{5,0},{6,11},{7,2},{8,13},{9,4},{1... | collective-permute-start | bytes 393224 | tf_op jit(solution)/shard_map/ppermute | solution.py:36
  116.2 4.8 %collective-permute-start.6 = (bf16[512,128]{1,0:T(8,128)(2,1)S(1)}, bf16[512,128]{1,0:T(8,128)(2,1)S(1)}, u32[]{:S(2)}, u32[]{:S(2)}) collective-permute-start(bf16[512,128]{1,0:T(8,128)(2,1)S(1)} %get-tuple-element.41), channel_id=1, source_target_pairs={{0,1},{1,0},{2,3},{3,2},{4,5},{5,4},{6,7},{7,6},{8,9},{9,8},{10,11... | collective-permute-start | bytes 393224 | tf_op jit(solution)/shard_map/ppermute | solution.py:27

commit v9 on v8

--- a/solution.py
+++ b/solution.py
@@ -172,25 +172,14 @@
         bottom[at : at + step] = array[:, half + at : half + at + step].T
 
 
-def norm_terms_body(full_width, sums, pre, grad, table, flipped, bias, gain, top, bottom, joined_out, out, held, made, mixed_made, come, gone):
-    deep, n_x, rows, both = made.shape[1:]
+def norm_terms_body(full_width, rows, sums, pre, grad, table, flipped, bias, gain, top, bottom, joined_out, out, held, come):
+    n_x, tall, _ = out.shape
+    n_z = (tall - PACKED) // rows
     later, chunk, _ = held.shape
-    parts = made.shape[0]
-    ready = parts - later
-    n_z = parts * deep
     loads = [
         pltpu.make_async_copy(bottom.at[pl.ds(i * chunk, chunk)], held.at[i], come.at[i])
         for i in range(later)
     ]
-    stores = [
-        pltpu.make_async_copy(
-            made.at[z // deep, z % deep], out.at[:, pl.ds(z * rows, rows)], gone.at[z]
-        )
-        for z in range(n_z)
-    ]
-    stores.append(
-        pltpu.make_async_copy(mixed_made, out.at[:, pl.ds(n_z * rows, PACKED)], gone.at[n_z])
-    )
     for load in loads:
         load.start()
     gating, mixed_grad, back, (pre_content, pre_gating) = branches(
@@ -220,39 +209,35 @@
     joined_out[:, width:] = (gating_back * gelu_slope(pre_gating)).astype(bf16)
     mixing_term = packed(causal(mixing_grad)).astype(bf16)
     for x in range(n_x):
-        mixed_made[x] = mixing_term
-    stores[n_z].start()
-    for i in range(parts):
-        if i < ready:
-            slab = top[i * chunk : (i + 1) * chunk]
+        out[x, n_z * rows :] = mixing_term
+    slab = n_x * rows
+    ready = top.shape[0] // slab
+    for z in range(n_z):
+        if z < ready:
+            part = top[z * slab : (z + 1) * slab]
         else:
-            loads[i - ready].wait()
-            slab = held[i - ready]
-        term = nn(slab, joined_out[...]).astype(bf16)
-        made[i] = term.reshape(deep, n_x, rows, both)
-        for z in range(i * deep, (i + 1) * deep):
-            stores[z].start()
-    for store in stores:
-        store.wait()
+            at = (z - ready) * slab
+            if at % chunk == 0:
+                loads[at // chunk].wait()
+            part = held[at // chunk, at % chunk : at % chunk + slab]
+        term = nn(part, joined_out[...]).astype(bf16)
+        for x in range(n_x):
+            out[x, z * rows : (z + 1) * rows] = term[x * rows : (x + 1) * rows]
 
 
 def norm_terms(full_width, small, top, bottom, n_x, n_z):
     width, tokens = 2 * top.shape[0], top.shape[1]
     both = 2 * small[2].shape[1]
     rows = width // (n_x * n_z)
-    parts = 4
     near, far = pl.BlockSpec(memory_space=pltpu.VMEM), pl.BlockSpec(memory_space=pl.ANY)
     return pl.pallas_call(
-        functools.partial(norm_terms_body, full_width),
+        functools.partial(norm_terms_body, full_width, rows),
         out_shape=(like((tokens, both), bf16), stored((n_x, n_z * rows + PACKED, both), bf16)),
         in_specs=[near] * (len(small) + 1) + [far],
-        out_specs=(near, far),
+        out_specs=(near, pl.BlockSpec()),
         scratch_shapes=[
-            pltpu.VMEM((parts // 2, width // parts, tokens), bf16),
-            pltpu.VMEM((parts, n_z // parts, n_x, rows, both), bf16),
-            pltpu.VMEM((n_x, PACKED, both), bf16),
-            pltpu.SemaphoreType.DMA((parts // 2,)),
-            pltpu.SemaphoreType.DMA((n_z + 1,)),
+            pltpu.VMEM((1, bottom.shape[0], tokens), bf16),
+            pltpu.SemaphoreType.DMA((1,)),
         ],
         compiler_params=pltpu.CompilerParams(vmem_limit_bytes=20 * 1024 * 1024),
         name="norm_terms",

time: 123 us -> 122 us (level)
  no operation moved by 1% of the time
where the time goes in v9:
time: 122 us; the launch traced here: 121 us
  starting transfers between devices  41.6 us (34%)
  blocking collectives  37.1 us (30%)
  waiting for transfers between devices  24.5 us (20%)
  Pallas kernels  14.6 us (12%)
  local copies, waits for them, and re-layouts  2.75 us (2%)
    all_to_all x2, blocking collectives, exchange(): return lax.all_to_all(array, axis, split_axis=0, concat_axis=0, tiled=True)  37.1 us
    ppermute x4, starting transfers between devices, sent_apart(): return lax.ppermute(array, DP, moves)  17.7 us
    all_to_all x3, starting transfers between devices, exchange(): return lax.all_to_all(array, axis, split_axis=0, concat_axis=0, tiled=True)  17.6 us
    all_to_all x3, waiting for transfers between devices, exchange(): return lax.all_to_all(array, axis, split_axis=0, concat_axis=0, tiled=True)  15 us
    pallas_call x10, Pallas kernels, run(): return made(*operands)  11.9 us
    ppermute x4, waiting for transfers between devices, sent_apart(): return lax.ppermute(array, DP, moves)  9.48 us
    ppermute x3, starting transfers between devices, swapped(): return lax.ppermute(array, 'dp_1', [(0, 1), (1, 0)])  6.25 us
    pallas_call x1, Pallas kernels, norm_terms(): pl.pallas_call(functools.partial(norm_terms_body, full_width, rows), out_...  2.79 us
  transfers between devices with their start and end apart: 10, of which 4 were waited for; matrix products, arithmetic and copies ran while one was open for 0% of the time, Pallas kernels for 6%

profile of v9, /device:TPU:9, one launch (start us, length us, event | category | flops | bytes accessed | tf_op | source)
XLA Modules:
  0.0 121.3 jit_solution(6548891150620608344)
XLA Ops:
  0.6 1.5 %shard_map.102 = bf16[8,64,256]{2,1,0:T(8,128)(2,1)} custom-call(bf16[64,128]{1,0:T(8,128)(2,1)} %content.1, bf16[64,128]{1,0:T(8,128)(2,1)} %gating.1), custom_call_target="tpu_custom_call" | custom-call | tf_op jit(solution)/shard_map/pallas_call | solution.py:107
  2.1 20.5 %all_to_all.25.arrived = bf16[8,64,256]{2,1,0:T(8,128)(2,1)S(1)} all-to-all(bf16[8,64,256]{2,1,0:T(8,128)(2,1)} %shard_map.102), channel_id=1, replica_groups=mesh['sp_0'=8,'sp_1'=4,'dp_0'=8,'dp_1'=2] {'sp_0'}, dimensions={0} | all-to-all | bytes 524288 | tf_op jit(solution)/shard_map/all_to_all | solution.py:23
  22.6 0.0 copy-start.3
  22.6 0.0 copy-start.6
  22.6 0.1 shard_map.103
  22.7 0.0 copy-start
  22.7 0.0 copy-start.7
  22.7 16.5 %all_to_all.26.weight = bf16[4,8,64,256]{3,2,1,0:T(8,128)(2,1)S(1)} all-to-all(bf16[4,8,64,256]{3,2,1,0:T(8,128)(2,1)S(1)} %shard_map.103), channel_id=1, replica_groups=mesh['sp_0'=8,'sp_1'=4,'dp_0'=8,'dp_1'=2] {'sp_1'}, dimensions={0} | all-to-all | bytes 2097152 | tf_op jit(solution)/shard_map/all_to_all | solution.py:23
  39.3 0.0 copy-done.3
  39.3 0.0 copy-done.6
  39.3 0.0 copy-done
  39.3 0.0 copy-done.7
  39.3 1.8 %shard_map.104 = (bf16[512,256]{1,0:T(8,128)(2,1)S(1)}, f32[16,4,512]{2,1,0:T(4,128)}) custom-call(bf16[512,2048]{1,0:T(8,128)(2,1)S(1)} %copy-done, bf16[4,8,64,256]{3,2,1,0:T(8,128)(2,1)S(1)} %all_to_all.26.weight, bf16[1,128,128]{2,1,0:T(8,128)(2,1)S(1)} %copy-done.6, f32[1,128]{1,0:T(1,128)S(1)} %bitcast.11, bf16[512,128]{1,0:T(8,128)(2,1)S(1)} %copy-done.3), custom_call_target="tpu_custom_call" | custom-call | tf_op jit(solution)/shard_map/pallas_call | solution.py:107
  41.1 0.0 copy-start.4
  41.1 0.7 copy-done.4
  41.8 10.6 %all-to-all-start.2 = ((f32[16,4,512]{2,1,0:T(4,128)}), f32[16,4,512]{2,1,0:T(4,128)S(1)}, u32[]{:S(2)}, u32[]{:S(2)}) async-start(f32[16,4,512]{2,1,0:T(4,128)} %get-tuple-element.25), calls=%async_computation.2 | async-start | bytes 262144 | tf_op jit(solution)/shard_map/all_to_all | solution.py:23
  52.5 1.6 %shard_map.106 = (bf16[1024,512]{1,0:T(8,128)(2,1)S(1)}, bf16[1024,512]{1,0:T(8,128)(2,1)}) custom-call(bf16[512,2048]{1,0:T(8,128)(2,1)S(1)} %copy-done), custom_call_target="tpu_custom_call" | custom-call | tf_op jit(solution)/shard_map/pallas_call | solution.py:107
  54.1 1.0 copy-done.1
  55.1 0.1 stack.44.where
  55.1 1.9 %shard_map.105 = (bf16[1024,256]{1,0:T(8,128)(2,1)}, bf16[1024,256]{1,0:T(8,128)(2,1)}, bf16[128,128]{1,0:T(8,128)(2,1)S(1)}, bf16[128,128]{1,0:T(8,128)(2,1)S(1)}) custom-call(s32[11]{0:T(128)S(1)} %stack.44.where, bf16[4,8,64,256]{3,2,1,0:T(8,128)(2,1)S(1)} %all_to_all.26.weight, bf16[1,128,128]{2,1,0:T(8,128)(2,1)} %mixing.3), custom_call_target="tpu_custom_call" | custom-call | tf_op jit(solution)/shard_map/pallas_call | solution.py:107
  57.0 3.2 %all-to-all-done.2.sums = f32[16,4,512]{2,1,0:T(4,128)S(1)} async-done(((f32[16,4,512]{2,1,0:T(4,128)}), f32[16,4,512]{2,1,0:T(4,128)S(1)}, u32[]{:S(2)}, u32[]{:S(2)}) %all-to-all-start.2) | async-done | bytes 131104 | tf_op jit(solution)/shard_map/all_to_all | solution.py:23
  60.3 0.0 copy-done.8
  60.3 0.0 copy-done.2
  60.3 0.9 copy-done.5
  61.2 2.8 %norm_terms.1 = (bf16[512,256]{1,0:T(8,128)(2,1)S(1)}, bf16[4,552,256]{2,1,0:T(8,128)(2,1)}) custom-call(f32[16,4,512]{2,1,0:T(4,128)S(1)} %all-to-all-done.2.sums, bf16[512,256]{1,0:T(8,128)(2,1)S(1)} %copy-done.5, bf16[512,128]{1,0:T(8,128)(2,1)S(1)} %copy-done.3, bf16[128,128]{1,0:T(8,128)(2,1)S(1)} %get-tuple-element.27.table, ...), custom_call_target="tpu_custom_call" | custom-call | tf_op jit(solution)/shard_map/norm_terms/pallas_call | solution.py:233
  64.0 3.5 %all-to-all-start.3 = ((bf16[4,552,256]{2,1,0:T(8,128)(2,1)}), bf16[4,552,256]{2,1,0:T(8,128)(2,1)S(1)}, u32[]{:S(2)}, u32[]{:S(2)}) async-start(bf16[4,552,256]{2,1,0:T(8,128)(2,1)} %get-tuple-element.42), calls=%async_computation.3 | async-start | bytes 2260992 | tf_op jit(solution)/shard_map/all_to_all | solution.py:23
  67.6 1.9 %collective-permute-start.1 = (bf16[1024,256]{1,0:T(8,128)(2,1)}, bf16[1024,256]{1,0:T(8,128)(2,1)S(1)}, u32[]{:S(2)}, u32[]{:S(2)}) collective-permute-start(bf16[1024,256]{1,0:T(8,128)(2,1)} %get-tuple-element.33), channel_id=1, source_target_pairs={{0,1},{1,0},{2,3},{3,2},{4,5},{5,4},{6,7},{7,6},{8,9},{9,8},{10,11... | collective-permute-start | bytes 1572872 | tf_op jit(solution)/shard_map/ppermute | solution.py:27
  69.5 2.4 %collective-permute-start = (bf16[512,256]{1,0:T(8,128)(2,1)S(1)}, bf16[512,256]{1,0:T(8,128)(2,1)S(1)}, u32[]{:S(2)}, u32[]{:S(2)}) collective-permute-start(bf16[512,256]{1,0:T(8,128)(2,1)S(1)} %get-tuple-element.31.joined), channel_id=1, source_target_pairs={{0,1},{1,0},{2,3},{3,2},{4,5},{5,4},{6,7},{7,6},{8,9},{9,8},{10,11... | collective-permute-start | bytes 786440 | tf_op jit(solution)/shard_map/ppermute | solution.py:27
  71.9 11.7 %all-to-all-done.3.arrived = bf16[4,552,256]{2,1,0:T(8,128)(2,1)S(1)} async-done(((bf16[4,552,256]{2,1,0:T(8,128)(2,1)}), bf16[4,552,256]{2,1,0:T(8,128)(2,1)S(1)}, u32[]{:S(2)}, u32[]{:S(2)}) %all-to-all-start.3) | async-done | bytes 1130528 | tf_op jit(solution)/shard_map/all_to_all | solution.py:23
  83.6 0.9 shard_map.110
  84.5 3.5 %all-to-all-start.4 = ((bf16[8,104,256]{2,1,0:T(8,128)(2,1)}), bf16[8,104,256]{2,1,0:T(8,128)(2,1)S(1)}, u32[]{:S(2)}, u32[]{:S(2)}) async-start(bf16[8,104,256]{2,1,0:T(8,128)(2,1)} %shard_map.110), calls=%async_computation.4 | async-start | bytes 851968 | tf_op jit(solution)/shard_map/all_to_all | solution.py:23
  88.0 0.0 collective-permute-done.joined_far
  88.0 0.0 collective-permute-done.1.far
  88.0 1.9 %shard_map.107 = (bf16[512,512]{1,0:T(8,128)(2,1)S(1)}, f32[512,256]{1,0:T(8,128)S(1)}, bf16[512,128]{1,0:T(8,128)(2,1)S(1)}, f32[512,128]{1,0:T(8,128)S(1)}) custom-call(bf16[512,256]{1,0:T(8,128)(2,1)S(1)} %get-tuple-element.31.joined, bf16[512,256]{1,0:T(8,128)(2,1)S(1)} %collective-permute-done.joined_far, bf16[1024,256]{1,0:T(8,128)(2,1)} %get-tuple-element.32.mine, ...), custom_call_target="tpu_custom_call" | custom-call | tf_op jit(solution)/shard_map/pallas_call | solution.py:107
  90.0 3.2 %collective-permute-start.2 = (bf16[512,512]{1,0:T(8,128)(2,1)S(1)}, bf16[512,512]{1,0:T(8,128)(2,1)S(1)}, u32[]{:S(2)}, u32[]{:S(2)}) collective-permute-start(bf16[512,512]{1,0:T(8,128)(2,1)S(1)} %get-tuple-element.36), channel_id=1, source_target_pairs={{0,2},{1,15},{2,4},{3,1},{4,6},{5,3},{6,8},{7,5},{8,10},{9,7},{10,... | collective-permute-start | bytes 1572872 | tf_op jit(solution)/shard_map/ppermute | solution.py:36
  93.2 2.0 %collective-permute-start.3 = (bf16[512,128]{1,0:T(8,128)(2,1)S(1)}, bf16[512,128]{1,0:T(8,128)(2,1)S(1)}, u32[]{:S(2)}, u32[]{:S(2)}) collective-permute-start(bf16[512,128]{1,0:T(8,128)(2,1)S(1)} %get-tuple-element.37), channel_id=1, source_target_pairs={{0,4},{1,13},{2,6},{3,15},{4,8},{5,1},{6,10},{7,3},{8,12},{9,5},{1... | collective-permute-start | bytes 393224 | tf_op jit(solution)/shard_map/ppermute | solution.py:36
  95.1 6.6 %collective-permute-done.3.four = bf16[512,128]{1,0:T(8,128)(2,1)S(1)} collective-permute-done((bf16[512,128]{1,0:T(8,128)(2,1)S(1)}, bf16[512,128]{1,0:T(8,128)(2,1)S(1)}, u32[]{:S(2)}, u32[]{:S(2)}) %collective-permute-start.3) | collective-permute-done | bytes 131104 | tf_op jit(solution)/shard_map/ppermute | solution.py:36
  101.8 0.0 collective-permute-done.2.odd
  101.8 0.7 shard_map.108
  102.5 6.3 %collective-permute-start.4 = (bf16[512,128]{1,0:T(8,128)(2,1)S(1)}, bf16[512,128]{1,0:T(8,128)(2,1)S(1)}, u32[]{:S(2)}, u32[]{:S(2)}) collective-permute-start(bf16[512,128]{1,0:T(8,128)(2,1)S(1)} %get-tuple-element.38), channel_id=1, source_target_pairs={{0,4},{1,13},{2,6},{3,15},{4,8},{5,1},{6,10},{7,3},{8,12},{9,5},{1... | collective-permute-start | bytes 393224 | tf_op jit(solution)/shard_map/ppermute | solution.py:36
  108.8 6.3 %collective-permute-start.5 = (bf16[512,128]{1,0:T(8,128)(2,1)S(1)}, bf16[512,128]{1,0:T(8,128)(2,1)S(1)}, u32[]{:S(2)}, u32[]{:S(2)}) collective-permute-start(bf16[512,128]{1,0:T(8,128)(2,1)S(1)} %get-tuple-element.39), channel_id=1, source_target_pairs={{0,5},{1,12},{2,7},{3,14},{4,9},{5,0},{6,11},{7,2},{8,13},{9,4},{1... | collective-permute-start | bytes 393224 | tf_op jit(solution)/shard_map/ppermute | solution.py:36
  115.1 1.9 %collective-permute-start.6 = (bf16[512,128]{1,0:T(8,128)(2,1)S(1)}, bf16[512,128]{1,0:T(8,128)(2,1)S(1)}, u32[]{:S(2)}, u32[]{:S(2)}) collective-permute-start(bf16[512,128]{1,0:T(8,128)(2,1)S(1)} %get-tuple-element.41), channel_id=1, source_target_pairs={{0,1},{1,0},{2,3},{3,2},{4,5},{5,4},{6,7},{7,6},{8,9},{9,8},{10,11... | collective-permute-start | bytes 393224 | tf_op jit(solution)/shard_map/ppermute | solution.py:27
  117.0 0.0 collective-permute-done.4.same
  117.0 2.8 %collective-permute-done.5.other = bf16[512,128]{1,0:T(8,128)(2,1)S(1)} collective-permute-done((bf16[512,128]{1,0:T(8,128)(2,1)S(1)}, bf16[512,128]{1,0:T(8,128)(2,1)S(1)}, u32[]{:S(2)}, u32[]{:S(2)}) %collective-permute-start.5) | collective-permute-done | bytes 131104 | tf_op jit(solution)/shard_map/ppermute | solution.py:36
  119.8 0.0 collective-permute-done.6.sent
  119.8 0.7 shard_map.109
  120.6 0.0 all-to-all-done.4.arrived
  120.6 0.7 shard_map.111
  (4 shorter events, 0.0 us)
Async XLA Ops:
  22.6 16.6 %copy-start.3 = (bf16[512,128]{1,0:T(8,128)(2,1)S(1)}, bf16[512,128]{1,0:T(8,128)(2,1)}, u32[]{:S(2)}) copy-start(bf16[512,128]{1,0:T(8,128)(2,1)} %grad.3) | copy-start | bytes 393220
  22.6 16.6 %copy-start.6 = (bf16[1,128,128]{2,1,0:T(8,128)(2,1)S(1)}, bf16[1,128,128]{2,1,0:T(8,128)(2,1)}, u32[]{:S(2)}) copy-start(bf16[1,128,128]{2,1,0:T(8,128)(2,1)} %mixing.3) | copy-start | bytes 98308
  22.7 16.6 %copy-start = (bf16[512,2048]{1,0:T(8,128)(2,1)S(1)}, bf16[512,2048]{1,0:T(8,128)(2,1)}, u32[]{:S(2)}) copy-start(bf16[512,2048]{1,0:T(8,128)(2,1)} %array.1) | copy-start | bytes 6291460
  22.7 16.5 %copy-start.7 = (f32[128]{0:T(128)S(1)}, f32[128]{0:T(128)}, u32[]{:S(2)}) copy-start(f32[128]{0:T(128)} %param.10) | copy-start | bytes 1540
  41.1 0.7 copy-start.4
  41.8 18.5 %all-to-all-start.2 = ((f32[16,4,512]{2,1,0:T(4,128)}), f32[16,4,512]{2,1,0:T(4,128)S(1)}, u32[]{:S(2)}, u32[]{:S(2)}) async-start(f32[16,4,512]{2,1,0:T(4,128)} %get-tuple-element.25), calls=%async_computation.2 | async-start | bytes 262144 | tf_op jit(solution)/shard_map/all_to_all | solution.py:23
  52.5 7.8 %copy-start.8 = (f32[1,128]{1,0:T(1,128)S(1)}, f32[1,128]{1,0:T(1,128)}, u32[]{:S(2)}) copy-start(f32[1,128]{1,0:T(1,128)} %bias.1) | copy-start | bytes 1540
  54.1 1.0 copy-start.1
  55.1 5.2 %copy-start.2 = (bf16[1024,512]{1,0:T(8,128)(2,1)S(1)}, bf16[1024,512]{1,0:T(8,128)(2,1)}, u32[]{:S(2)}) copy-start(bf16[1024,512]{1,0:T(8,128)(2,1)} %copy-done.1) | copy-start | bytes 3145732
  60.3 1.0 copy-start.5
  64.0 19.6 %all-to-all-start.3 = ((bf16[4,552,256]{2,1,0:T(8,128)(2,1)}), bf16[4,552,256]{2,1,0:T(8,128)(2,1)S(1)}, u32[]{:S(2)}, u32[]{:S(2)}) async-start(bf16[4,552,256]{2,1,0:T(8,128)(2,1)} %get-tuple-element.42), calls=%async_computation.3 | async-start | bytes 2260992 | tf_op jit(solution)/shard_map/all_to_all | solution.py:23
  67.6 20.5 %collective-permute-start.1 = (bf16[1024,256]{1,0:T(8,128)(2,1)}, bf16[1024,256]{1,0:T(8,128)(2,1)S(1)}, u32[]{:S(2)}, u32[]{:S(2)}) collective-permute-start(bf16[1024,256]{1,0:T(8,128)(2,1)} %get-tuple-element.33), channel_id=1, source_target_pairs={{0,1},{1,0},{2,3},{3,2},{4,5},{5,4},{6,7},{7,6},{8,9},{9,8},{10,11... | collective-permute-start | bytes 1572872 | tf_op jit(solution)/shard_map/ppermute | solution.py:27
  69.5 18.5 %collective-permute-start = (bf16[512,256]{1,0:T(8,128)(2,1)S(1)}, bf16[512,256]{1,0:T(8,128)(2,1)S(1)}, u32[]{:S(2)}, u32[]{:S(2)}) collective-permute-start(bf16[512,256]{1,0:T(8,128)(2,1)S(1)} %get-tuple-element.31.joined), channel_id=1, source_target_pairs={{0,1},{1,0},{2,3},{3,2},{4,5},{5,4},{6,7},{7,6},{8,9},{9,8},{10,11... | collective-permute-start | bytes 786440 | tf_op jit(solution)/shard_map/ppermute | solution.py:27
  84.5 36.0 %all-to-all-start.4 = ((bf16[8,104,256]{2,1,0:T(8,128)(2,1)}), bf16[8,104,256]{2,1,0:T(8,128)(2,1)S(1)}, u32[]{:S(2)}, u32[]{:S(2)}) async-start(bf16[8,104,256]{2,1,0:T(8,128)(2,1)} %shard_map.110), calls=%async_computation.4 | async-start | bytes 851968 | tf_op jit(solution)/shard_map/all_to_all | solution.py:23
  90.0 11.8 %collective-permute-start.2 = (bf16[512,512]{1,0:T(8,128)(2,1)S(1)}, bf16[512,512]{1,0:T(8,128)(2,1)S(1)}, u32[]{:S(2)}, u32[]{:S(2)}) collective-permute-start(bf16[512,512]{1,0:T(8,128)(2,1)S(1)} %get-tuple-element.36), channel_id=1, source_target_pairs={{0,2},{1,15},{2,4},{3,1},{4,6},{5,3},{6,8},{7,5},{8,10},{9,7},{10,... | collective-permute-start | bytes 1572872 | tf_op jit(solution)/shard_map/ppermute | solution.py:36
  93.2 8.6 %collective-permute-start.3 = (bf16[512,128]{1,0:T(8,128)(2,1)S(1)}, bf16[512,128]{1,0:T(8,128)(2,1)S(1)}, u32[]{:S(2)}, u32[]{:S(2)}) collective-permute-start(bf16[512,128]{1,0:T(8,128)(2,1)S(1)} %get-tuple-element.37), channel_id=1, source_target_pairs={{0,4},{1,13},{2,6},{3,15},{4,8},{5,1},{6,10},{7,3},{8,12},{9,5},{1... | collective-permute-start | bytes 393224 | tf_op jit(solution)/shard_map/ppermute | solution.py:36
  102.5 14.5 %collective-permute-start.4 = (bf16[512,128]{1,0:T(8,128)(2,1)S(1)}, bf16[512,128]{1,0:T(8,128)(2,1)S(1)}, u32[]{:S(2)}, u32[]{:S(2)}) collective-permute-start(bf16[512,128]{1,0:T(8,128)(2,1)S(1)} %get-tuple-element.38), channel_id=1, source_target_pairs={{0,4},{1,13},{2,6},{3,15},{4,8},{5,1},{6,10},{7,3},{8,12},{9,5},{1... | collective-permute-start | bytes 393224 | tf_op jit(solution)/shard_map/ppermute | solution.py:36
  108.8 11.1 %collective-permute-start.5 = (bf16[512,128]{1,0:T(8,128)(2,1)S(1)}, bf16[512,128]{1,0:T(8,128)(2,1)S(1)}, u32[]{:S(2)}, u32[]{:S(2)}) collective-permute-start(bf16[512,128]{1,0:T(8,128)(2,1)S(1)} %get-tuple-element.39), channel_id=1, source_target_pairs={{0,5},{1,12},{2,7},{3,14},{4,9},{5,0},{6,11},{7,2},{8,13},{9,4},{1... | collective-permute-start | bytes 393224 | tf_op jit(solution)/shard_map/ppermute | solution.py:36
  115.1 4.8 %collective-permute-start.6 = (bf16[512,128]{1,0:T(8,128)(2,1)S(1)}, bf16[512,128]{1,0:T(8,128)(2,1)S(1)}, u32[]{:S(2)}, u32[]{:S(2)}) collective-permute-start(bf16[512,128]{1,0:T(8,128)(2,1)S(1)} %get-tuple-element.41), channel_id=1, source_target_pairs={{0,1},{1,0},{2,3},{3,2},{4,5},{5,4},{6,7},{7,6},{8,9},{9,8},{10,11... | collective-permute-start | bytes 393224 | tf_op jit(solution)/shard_map/ppermute | solution.py:27

commit v10 on v9

--- a/solution.py
+++ b/solution.py
@@ -154,10 +154,31 @@
     return gating, mixed_grad, jnp.concatenate(pieces, axis=0), (pre_content, pre_gating)
 
 
-def join_body(content, gating, out):
-    both = jnp.concatenate([content[...], gating[...]], axis=1)
+def join_body(content, gating, out, done):
+    width = content.shape[1]
+    moves = []
     for peer in range(out.shape[0]):
-        out[peer] = both
+        for side, array in enumerate((content, gating)):
+            slot = out.at[peer, :, pl.ds(side * width, width)]
+            moves.append(pltpu.make_async_copy(array, slot, done.at[peer, side]))
+    for move in moves:
+        move.start()
+    for move in moves:
+        move.wait()
+
+
+def join(content, gating, n_z):
+    rows, width = content.shape
+    far = pl.BlockSpec(memory_space=pl.ANY)
+    return pl.pallas_call(
+        join_body,
+        out_shape=stored((n_z, rows, 2 * width), bf16),
+        in_specs=[far, far],
+        out_specs=far,
+        scratch_shapes=[pltpu.SemaphoreType.DMA((n_z, 2))],
+        compiler_params=pltpu.CompilerParams(vmem_limit_bytes=20 * 1024 * 1024),
+        name="join",
+    )(*[pltpu.with_memory_space_constraint(a, pltpu.HBM) for a in (content, gating)])
 
 
 def spread_body(arrived, out):
@@ -297,16 +318,37 @@
     out[...] = total.astype(bf16)
 
 
-def regroup_body(arrived, out):
-    n_z = out.shape[0]
-    rows = out.shape[1] - PACKED
-    total = arrived[0].astype(f32)
-    for x in range(1, arrived.shape[0]):
-        total = total + arrived[x].astype(f32)
-    total = total.astype(bf16)
+def regroup_body(arrived, out, made, done):
+    n_z, tall, _ = made.shape
+    rows = tall - PACKED
+
+    def summed(at, n):
+        total = arrived[0, at : at + n].astype(f32)
+        for x in range(1, arrived.shape[0]):
+            total = total + arrived[x, at : at + n].astype(f32)
+        return total.astype(bf16)
+
+    stores = [pltpu.make_async_copy(made.at[z], out.at[z], done.at[z]) for z in range(n_z)]
+    shared = summed(n_z * rows, PACKED)
     for z in range(n_z):
-        out[z, :rows] = total[z * rows : (z + 1) * rows]
-        out[z, rows:] = total[n_z * rows :]
+        made[z, :rows] = summed(z * rows, rows)
+        made[z, rows:] = shared
+        stores[z].start()
+    for store in stores:
+        store.wait()
+
+
+def regroup(arrived, n_z, rows):
+    shape = (n_z, rows + PACKED, arrived.shape[2])
+    return pl.pallas_call(
+        regroup_body,
+        out_shape=stored(shape, bf16),
+        in_specs=[pl.BlockSpec(memory_space=pltpu.VMEM)],
+        out_specs=pl.BlockSpec(memory_space=pl.ANY),
+        scratch_shapes=[pltpu.VMEM(shape, bf16), pltpu.SemaphoreType.DMA((n_z,))],
+        compiler_params=pltpu.CompilerParams(vmem_limit_bytes=20 * 1024 * 1024),
+        name="regroup",
+    )(pltpu.with_memory_space_constraint(arrived, pltpu.VMEM))
 
 
 def finish_body(scale, arrived, content_out, gating_out, mixing_out):
@@ -343,9 +385,7 @@
 
     half = (width // 2, tok_rows)
     top, bottom = call(flip_body, (like(half, bf16), stored(half, bf16)))(hidden_in)
-    shards = call(join_body, stored((n_z, shard_rows, both), bf16), cold=(0, 1))(
-        content_weight, gating_weight
-    )
+    shards = join(content_weight, gating_weight, n_z)
     along_z = exchange(shards, "sp_0")
     spread = call(spread_body, like((n_x, n_z, shard_rows, both), bf16))(along_z)
     weight = exchange(spread, "sp_1")
@@ -385,7 +425,7 @@
     other = sent_apart(other, 2, True)
     sent = swapped(send)
 
-    regrouped = call(regroup_body, stored((n_z, shard_rows + PACKED, both), bf16))(along_x)
+    regrouped = regroup(along_x, n_z, shard_rows)
     arrived = exchange(regrouped, "sp_0")
 
     input_grad = call(total_body, outside(single, bf16))(own, same, other, keep, sent)

time: 122 us -> 130 us (1.066)
  Pallas kernels: 14.6 us -> 22.3 us
    pallas_call x0 -> x2, Pallas kernels: none -> 10.1 us  [the longest x1 9.19 us: join(): pl.pallas_call(join_body, out_shape=stored((n_z, rows, 2 * width), bf16),...]
    pallas_call x10 -> x8, Pallas kernels: 11.9 us -> 9.47 us  [run(): return made(*operands)]
where the time goes in v10:
time: 130 us; the launch traced here: 129 us
  starting transfers between devices  41.6 us (32%)
  blocking collectives  37.1 us (29%)
  waiting for transfers between devices  24.5 us (19%)
  Pallas kernels  22.3 us (17%)
  local copies, waits for them, and re-layouts  2.75 us (2%)
    all_to_all x2, blocking collectives, exchange(): return lax.all_to_all(array, axis, split_axis=0, concat_axis=0, tiled=True)  37.1 us
    ppermute x4, starting transfers between devices, sent_apart(): return lax.ppermute(array, DP, moves)  17.7 us
    all_to_all x3, starting transfers between devices, exchange(): return lax.all_to_all(array, axis, split_axis=0, concat_axis=0, tiled=True)  17.7 us
    all_to_all x3, waiting for transfers between devices, exchange(): return lax.all_to_all(array, axis, split_axis=0, concat_axis=0, tiled=True)  15 us
    pallas_call x8, Pallas kernels, run(): return made(*operands)  9.47 us
    ppermute x4, waiting for transfers between devices, sent_apart(): return lax.ppermute(array, DP, moves)  9.47 us
    pallas_call x1, Pallas kernels, join(): pl.pallas_call(join_body, out_shape=stored((n_z, rows, 2 * width), bf16),...  9.19 us
    ppermute x3, starting transfers between devices, swapped(): return lax.ppermute(array, 'dp_1', [(0, 1), (1, 0)])  6.25 us
  transfers between devices with their start and end apart: 10, of which 4 were waited for; matrix products, arithmetic and copies ran while one was open for 0% of the time, Pallas kernels for 6%

profile of v10, /device:TPU:9, one launch (start us, length us, event | category | flops | bytes accessed | tf_op | source)
XLA Modules:
  0.0 129.0 jit_solution(12965608142213212613)
XLA Ops:
  0.6 9.2 %join.1 = bf16[8,64,256]{2,1,0:T(8,128)(2,1)} custom-call(bf16[64,128]{1,0:T(8,128)(2,1)} %content.1, bf16[64,128]{1,0:T(8,128)(2,1)} %gating.1), custom_call_target="tpu_custom_call" | custom-call | tf_op jit(solution)/shard_map/join/pallas_call | solution.py:173
  9.8 20.5 %all_to_all.25.arrived = bf16[8,64,256]{2,1,0:T(8,128)(2,1)S(1)} all-to-all(bf16[8,64,256]{2,1,0:T(8,128)(2,1)} %join.1), channel_id=1, replica_groups=mesh['sp_0'=8,'sp_1'=4,'dp_0'=8,'dp_1'=2] {'sp_0'}, dimensions={0} | all-to-all | bytes 524288 | tf_op jit(solution)/shard_map/all_to_all | solution.py:23
  30.4 0.0 copy-start.3
  30.4 0.0 copy-start.6
  30.4 0.1 shard_map.102
  30.4 0.0 copy-start
  30.5 0.0 copy-start.7
  30.5 16.5 %all_to_all.26.weight = bf16[4,8,64,256]{3,2,1,0:T(8,128)(2,1)S(1)} all-to-all(bf16[4,8,64,256]{3,2,1,0:T(8,128)(2,1)S(1)} %shard_map.102), channel_id=1, replica_groups=mesh['sp_0'=8,'sp_1'=4,'dp_0'=8,'dp_1'=2] {'sp_1'}, dimensions={0} | all-to-all | bytes 2097152 | tf_op jit(solution)/shard_map/all_to_all | solution.py:23
  47.0 0.0 copy-done.3
  47.0 0.0 copy-done.6
  47.0 0.0 copy-done
  47.0 0.0 copy-done.7
  47.0 1.8 %shard_map.103 = (bf16[512,256]{1,0:T(8,128)(2,1)S(1)}, f32[16,4,512]{2,1,0:T(4,128)}) custom-call(bf16[512,2048]{1,0:T(8,128)(2,1)S(1)} %copy-done, bf16[4,8,64,256]{3,2,1,0:T(8,128)(2,1)S(1)} %all_to_all.26.weight, bf16[1,128,128]{2,1,0:T(8,128)(2,1)S(1)} %copy-done.6, f32[1,128]{1,0:T(1,128)S(1)} %bitcast.11, bf16[512,128]{1,0:T(8,128)(2,1)S(1)} %copy-done.3), custom_call_target="tpu_custom_call" | custom-call | tf_op jit(solution)/shard_map/pallas_call | solution.py:107
  48.8 0.0 copy-start.4
  48.8 0.7 copy-done.4
  49.5 10.6 %all-to-all-start.2 = ((f32[16,4,512]{2,1,0:T(4,128)}), f32[16,4,512]{2,1,0:T(4,128)S(1)}, u32[]{:S(2)}, u32[]{:S(2)}) async-start(f32[16,4,512]{2,1,0:T(4,128)} %get-tuple-element.25), calls=%async_computation.2 | async-start | bytes 262144 | tf_op jit(solution)/shard_map/all_to_all | solution.py:23
  60.2 1.6 %shard_map.105 = (bf16[1024,512]{1,0:T(8,128)(2,1)S(1)}, bf16[1024,512]{1,0:T(8,128)(2,1)}) custom-call(bf16[512,2048]{1,0:T(8,128)(2,1)S(1)} %copy-done), custom_call_target="tpu_custom_call" | custom-call | tf_op jit(solution)/shard_map/pallas_call | solution.py:107
  61.8 1.0 copy-done.1
  62.8 0.1 stack.44.where
  62.9 1.9 %shard_map.104 = (bf16[1024,256]{1,0:T(8,128)(2,1)}, bf16[1024,256]{1,0:T(8,128)(2,1)}, bf16[128,128]{1,0:T(8,128)(2,1)S(1)}, bf16[128,128]{1,0:T(8,128)(2,1)S(1)}) custom-call(s32[11]{0:T(128)S(1)} %stack.44.where, bf16[4,8,64,256]{3,2,1,0:T(8,128)(2,1)S(1)} %all_to_all.26.weight, bf16[1,128,128]{2,1,0:T(8,128)(2,1)} %mixing.3), custom_call_target="tpu_custom_call" | custom-call | tf_op jit(solution)/shard_map/pallas_call | solution.py:107
  64.8 3.2 %all-to-all-done.2.sums = f32[16,4,512]{2,1,0:T(4,128)S(1)} async-done(((f32[16,4,512]{2,1,0:T(4,128)}), f32[16,4,512]{2,1,0:T(4,128)S(1)}, u32[]{:S(2)}, u32[]{:S(2)}) %all-to-all-start.2) | async-done | bytes 131104 | tf_op jit(solution)/shard_map/all_to_all | solution.py:23
  68.0 0.0 copy-done.8
  68.0 0.0 copy-done.2
  68.0 0.9 copy-done.5
  69.0 2.8 %norm_terms.1 = (bf16[512,256]{1,0:T(8,128)(2,1)S(1)}, bf16[4,552,256]{2,1,0:T(8,128)(2,1)}) custom-call(f32[16,4,512]{2,1,0:T(4,128)S(1)} %all-to-all-done.2.sums, bf16[512,256]{1,0:T(8,128)(2,1)S(1)} %copy-done.5, bf16[512,128]{1,0:T(8,128)(2,1)S(1)} %copy-done.3, bf16[128,128]{1,0:T(8,128)(2,1)S(1)} %get-tuple-element.27.table, ...), custom_call_target="tpu_custom_call" | custom-call | tf_op jit(solution)/shard_map/norm_terms/pallas_call | solution.py:254
  71.8 3.5 %all-to-all-start.3 = ((bf16[4,552,256]{2,1,0:T(8,128)(2,1)}), bf16[4,552,256]{2,1,0:T(8,128)(2,1)S(1)}, u32[]{:S(2)}, u32[]{:S(2)}) async-start(bf16[4,552,256]{2,1,0:T(8,128)(2,1)} %get-tuple-element.42), calls=%async_computation.3 | async-start | bytes 2260992 | tf_op jit(solution)/shard_map/all_to_all | solution.py:23
  75.3 1.9 %collective-permute-start.1 = (bf16[1024,256]{1,0:T(8,128)(2,1)}, bf16[1024,256]{1,0:T(8,128)(2,1)S(1)}, u32[]{:S(2)}, u32[]{:S(2)}) collective-permute-start(bf16[1024,256]{1,0:T(8,128)(2,1)} %get-tuple-element.33), channel_id=1, source_target_pairs={{0,1},{1,0},{2,3},{3,2},{4,5},{5,4},{6,7},{7,6},{8,9},{9,8},{10,11... | collective-permute-start | bytes 1572872 | tf_op jit(solution)/shard_map/ppermute | solution.py:27
  77.2 2.4 %collective-permute-start = (bf16[512,256]{1,0:T(8,128)(2,1)S(1)}, bf16[512,256]{1,0:T(8,128)(2,1)S(1)}, u32[]{:S(2)}, u32[]{:S(2)}) collective-permute-start(bf16[512,256]{1,0:T(8,128)(2,1)S(1)} %get-tuple-element.31.joined), channel_id=1, source_target_pairs={{0,1},{1,0},{2,3},{3,2},{4,5},{5,4},{6,7},{7,6},{8,9},{9,8},{10,11... | collective-permute-start | bytes 786440 | tf_op jit(solution)/shard_map/ppermute | solution.py:27
  79.6 11.7 %all-to-all-done.3.arrived = bf16[4,552,256]{2,1,0:T(8,128)(2,1)S(1)} async-done(((bf16[4,552,256]{2,1,0:T(8,128)(2,1)}), bf16[4,552,256]{2,1,0:T(8,128)(2,1)S(1)}, u32[]{:S(2)}, u32[]{:S(2)}) %all-to-all-start.3) | async-done | bytes 1130528 | tf_op jit(solution)/shard_map/all_to_all | solution.py:23
  91.4 0.9 regroup.1
  92.3 3.5 %all-to-all-start.4 = ((bf16[8,104,256]{2,1,0:T(8,128)(2,1)}), bf16[8,104,256]{2,1,0:T(8,128)(2,1)S(1)}, u32[]{:S(2)}, u32[]{:S(2)}) async-start(bf16[8,104,256]{2,1,0:T(8,128)(2,1)} %regroup.1), calls=%async_computation.4 | async-start | bytes 851968 | tf_op jit(solution)/shard_map/all_to_all | solution.py:23
  95.7 0.0 collective-permute-done.joined_far
  95.7 0.0 collective-permute-done.1.far
  95.8 1.9 %shard_map.106 = (bf16[512,512]{1,0:T(8,128)(2,1)S(1)}, f32[512,256]{1,0:T(8,128)S(1)}, bf16[512,128]{1,0:T(8,128)(2,1)S(1)}, f32[512,128]{1,0:T(8,128)S(1)}) custom-call(bf16[512,256]{1,0:T(8,128)(2,1)S(1)} %get-tuple-element.31.joined, bf16[512,256]{1,0:T(8,128)(2,1)S(1)} %collective-permute-done.joined_far, bf16[1024,256]{1,0:T(8,128)(2,1)} %get-tuple-element.32.mine, ...), custom_call_target="tpu_custom_call" | custom-call | tf_op jit(solution)/shard_map/pallas_call | solution.py:107
  97.7 3.2 %collective-permute-start.2 = (bf16[512,512]{1,0:T(8,128)(2,1)S(1)}, bf16[512,512]{1,0:T(8,128)(2,1)S(1)}, u32[]{:S(2)}, u32[]{:S(2)}) collective-permute-start(bf16[512,512]{1,0:T(8,128)(2,1)S(1)} %get-tuple-element.36), channel_id=1, source_target_pairs={{0,2},{1,15},{2,4},{3,1},{4,6},{5,3},{6,8},{7,5},{8,10},{9,7},{10,... | collective-permute-start | bytes 1572872 | tf_op jit(solution)/shard_map/ppermute | solution.py:36
  100.9 2.0 %collective-permute-start.3 = (bf16[512,128]{1,0:T(8,128)(2,1)S(1)}, bf16[512,128]{1,0:T(8,128)(2,1)S(1)}, u32[]{:S(2)}, u32[]{:S(2)}) collective-permute-start(bf16[512,128]{1,0:T(8,128)(2,1)S(1)} %get-tuple-element.37), channel_id=1, source_target_pairs={{0,4},{1,13},{2,6},{3,15},{4,8},{5,1},{6,10},{7,3},{8,12},{9,5},{1... | collective-permute-start | bytes 393224 | tf_op jit(solution)/shard_map/ppermute | solution.py:36
  102.9 6.6 %collective-permute-done.3.four = bf16[512,128]{1,0:T(8,128)(2,1)S(1)} collective-permute-done((bf16[512,128]{1,0:T(8,128)(2,1)S(1)}, bf16[512,128]{1,0:T(8,128)(2,1)S(1)}, u32[]{:S(2)}, u32[]{:S(2)}) %collective-permute-start.3) | collective-permute-done | bytes 131104 | tf_op jit(solution)/shard_map/ppermute | solution.py:36
  109.5 0.0 collective-permute-done.2.odd
  109.5 0.7 shard_map.107
  110.2 6.3 %collective-permute-start.4 = (bf16[512,128]{1,0:T(8,128)(2,1)S(1)}, bf16[512,128]{1,0:T(8,128)(2,1)S(1)}, u32[]{:S(2)}, u32[]{:S(2)}) collective-permute-start(bf16[512,128]{1,0:T(8,128)(2,1)S(1)} %get-tuple-element.38), channel_id=1, source_target_pairs={{0,4},{1,13},{2,6},{3,15},{4,8},{5,1},{6,10},{7,3},{8,12},{9,5},{1... | collective-permute-start | bytes 393224 | tf_op jit(solution)/shard_map/ppermute | solution.py:36
  116.5 6.3 %collective-permute-start.5 = (bf16[512,128]{1,0:T(8,128)(2,1)S(1)}, bf16[512,128]{1,0:T(8,128)(2,1)S(1)}, u32[]{:S(2)}, u32[]{:S(2)}) collective-permute-start(bf16[512,128]{1,0:T(8,128)(2,1)S(1)} %get-tuple-element.39), channel_id=1, source_target_pairs={{0,5},{1,12},{2,7},{3,14},{4,9},{5,0},{6,11},{7,2},{8,13},{9,4},{1... | collective-permute-start | bytes 393224 | tf_op jit(solution)/shard_map/ppermute | solution.py:36
  122.8 1.9 %collective-permute-start.6 = (bf16[512,128]{1,0:T(8,128)(2,1)S(1)}, bf16[512,128]{1,0:T(8,128)(2,1)S(1)}, u32[]{:S(2)}, u32[]{:S(2)}) collective-permute-start(bf16[512,128]{1,0:T(8,128)(2,1)S(1)} %get-tuple-element.41), channel_id=1, source_target_pairs={{0,1},{1,0},{2,3},{3,2},{4,5},{5,4},{6,7},{7,6},{8,9},{9,8},{10,11... | collective-permute-start | bytes 393224 | tf_op jit(solution)/shard_map/ppermute | solution.py:27
  124.7 0.0 collective-permute-done.4.same
  124.7 2.8 %collective-permute-done.5.other = bf16[512,128]{1,0:T(8,128)(2,1)S(1)} collective-permute-done((bf16[512,128]{1,0:T(8,128)(2,1)S(1)}, bf16[512,128]{1,0:T(8,128)(2,1)S(1)}, u32[]{:S(2)}, u32[]{:S(2)}) %collective-permute-start.5) | collective-permute-done | bytes 131104 | tf_op jit(solution)/shard_map/ppermute | solution.py:36
  127.5 0.0 collective-permute-done.6.sent
  127.5 0.7 shard_map.108
  128.3 0.0 all-to-all-done.4.arrived
  128.3 0.7 shard_map.109
  (4 shorter events, 0.0 us)
Async XLA Ops:
  30.4 16.6 %copy-start.3 = (bf16[512,128]{1,0:T(8,128)(2,1)S(1)}, bf16[512,128]{1,0:T(8,128)(2,1)}, u32[]{:S(2)}) copy-start(bf16[512,128]{1,0:T(8,128)(2,1)} %grad.3) | copy-start | bytes 393220
  30.4 16.6 %copy-start.6 = (bf16[1,128,128]{2,1,0:T(8,128)(2,1)S(1)}, bf16[1,128,128]{2,1,0:T(8,128)(2,1)}, u32[]{:S(2)}) copy-start(bf16[1,128,128]{2,1,0:T(8,128)(2,1)} %mixing.3) | copy-start | bytes 98308
  30.4 16.6 %copy-start = (bf16[512,2048]{1,0:T(8,128)(2,1)S(1)}, bf16[512,2048]{1,0:T(8,128)(2,1)}, u32[]{:S(2)}) copy-start(bf16[512,2048]{1,0:T(8,128)(2,1)} %array.1) | copy-start | bytes 6291460
  30.5 16.5 %copy-start.7 = (f32[128]{0:T(128)S(1)}, f32[128]{0:T(128)}, u32[]{:S(2)}) copy-start(f32[128]{0:T(128)} %param.10) | copy-start | bytes 1540
  48.8 0.7 copy-start.4
  49.5 18.5 %all-to-all-start.2 = ((f32[16,4,512]{2,1,0:T(4,128)}), f32[16,4,512]{2,1,0:T(4,128)S(1)}, u32[]{:S(2)}, u32[]{:S(2)}) async-start(f32[16,4,512]{2,1,0:T(4,128)} %get-tuple-element.25), calls=%async_computation.2 | async-start | bytes 262144 | tf_op jit(solution)/shard_map/all_to_all | solution.py:23
  60.2 7.8 %copy-start.8 = (f32[1,128]{1,0:T(1,128)S(1)}, f32[1,128]{1,0:T(1,128)}, u32[]{:S(2)}) copy-start(f32[1,128]{1,0:T(1,128)} %bias.1) | copy-start | bytes 1540
  61.8 1.0 copy-start.1
  62.8 5.2 %copy-start.2 = (bf16[1024,512]{1,0:T(8,128)(2,1)S(1)}, bf16[1024,512]{1,0:T(8,128)(2,1)}, u32[]{:S(2)}) copy-start(bf16[1024,512]{1,0:T(8,128)(2,1)} %copy-done.1) | copy-start | bytes 3145732
  68.0 1.0 copy-start.5
  71.8 19.6 %all-to-all-start.3 = ((bf16[4,552,256]{2,1,0:T(8,128)(2,1)}), bf16[4,552,256]{2,1,0:T(8,128)(2,1)S(1)}, u32[]{:S(2)}, u32[]{:S(2)}) async-start(bf16[4,552,256]{2,1,0:T(8,128)(2,1)} %get-tuple-element.42), calls=%async_computation.3 | async-start | bytes 2260992 | tf_op jit(solution)/shard_map/all_to_all | solution.py:23
  75.3 20.4 %collective-permute-start.1 = (bf16[1024,256]{1,0:T(8,128)(2,1)}, bf16[1024,256]{1,0:T(8,128)(2,1)S(1)}, u32[]{:S(2)}, u32[]{:S(2)}) collective-permute-start(bf16[1024,256]{1,0:T(8,128)(2,1)} %get-tuple-element.33), channel_id=1, source_target_pairs={{0,1},{1,0},{2,3},{3,2},{4,5},{5,4},{6,7},{7,6},{8,9},{9,8},{10,11... | collective-permute-start | bytes 1572872 | tf_op jit(solution)/shard_map/ppermute | solution.py:27
  77.2 18.5 %collective-permute-start = (bf16[512,256]{1,0:T(8,128)(2,1)S(1)}, bf16[512,256]{1,0:T(8,128)(2,1)S(1)}, u32[]{:S(2)}, u32[]{:S(2)}) collective-permute-start(bf16[512,256]{1,0:T(8,128)(2,1)S(1)} %get-tuple-element.31.joined), channel_id=1, source_target_pairs={{0,1},{1,0},{2,3},{3,2},{4,5},{5,4},{6,7},{7,6},{8,9},{9,8},{10,11... | collective-permute-start | bytes 786440 | tf_op jit(solution)/shard_map/ppermute | solution.py:27
  92.3 36.0 %all-to-all-start.4 = ((bf16[8,104,256]{2,1,0:T(8,128)(2,1)}), bf16[8,104,256]{2,1,0:T(8,128)(2,1)S(1)}, u32[]{:S(2)}, u32[]{:S(2)}) async-start(bf16[8,104,256]{2,1,0:T(8,128)(2,1)} %regroup.1), calls=%async_computation.4 | async-start | bytes 851968 | tf_op jit(solution)/shard_map/all_to_all | solution.py:23
  97.7 11.8 %collective-permute-start.2 = (bf16[512,512]{1,0:T(8,128)(2,1)S(1)}, bf16[512,512]{1,0:T(8,128)(2,1)S(1)}, u32[]{:S(2)}, u32[]{:S(2)}) collective-permute-start(bf16[512,512]{1,0:T(8,128)(2,1)S(1)} %get-tuple-element.36), channel_id=1, source_target_pairs={{0,2},{1,15},{2,4},{3,1},{4,6},{5,3},{6,8},{7,5},{8,10},{9,7},{10,... | collective-permute-start | bytes 1572872 | tf_op jit(solution)/shard_map/ppermute | solution.py:36
  100.9 8.6 %collective-permute-start.3 = (bf16[512,128]{1,0:T(8,128)(2,1)S(1)}, bf16[512,128]{1,0:T(8,128)(2,1)S(1)}, u32[]{:S(2)}, u32[]{:S(2)}) collective-permute-start(bf16[512,128]{1,0:T(8,128)(2,1)S(1)} %get-tuple-element.37), channel_id=1, source_target_pairs={{0,4},{1,13},{2,6},{3,15},{4,8},{5,1},{6,10},{7,3},{8,12},{9,5},{1... | collective-permute-start | bytes 393224 | tf_op jit(solution)/shard_map/ppermute | solution.py:36
  110.2 14.5 %collective-permute-start.4 = (bf16[512,128]{1,0:T(8,128)(2,1)S(1)}, bf16[512,128]{1,0:T(8,128)(2,1)S(1)}, u32[]{:S(2)}, u32[]{:S(2)}) collective-permute-start(bf16[512,128]{1,0:T(8,128)(2,1)S(1)} %get-tuple-element.38), channel_id=1, source_target_pairs={{0,4},{1,13},{2,6},{3,15},{4,8},{5,1},{6,10},{7,3},{8,12},{9,5},{1... | collective-permute-start | bytes 393224 | tf_op jit(solution)/shard_map/ppermute | solution.py:36
  116.5 11.1 %collective-permute-start.5 = (bf16[512,128]{1,0:T(8,128)(2,1)S(1)}, bf16[512,128]{1,0:T(8,128)(2,1)S(1)}, u32[]{:S(2)}, u32[]{:S(2)}) collective-permute-start(bf16[512,128]{1,0:T(8,128)(2,1)S(1)} %get-tuple-element.39), channel_id=1, source_target_pairs={{0,5},{1,12},{2,7},{3,14},{4,9},{5,0},{6,11},{7,2},{8,13},{9,4},{1... | collective-permute-start | bytes 393224 | tf_op jit(solution)/shard_map/ppermute | solution.py:36
  122.8 4.8 %collective-permute-start.6 = (bf16[512,128]{1,0:T(8,128)(2,1)S(1)}, bf16[512,128]{1,0:T(8,128)(2,1)S(1)}, u32[]{:S(2)}, u32[]{:S(2)}) collective-permute-start(bf16[512,128]{1,0:T(8,128)(2,1)S(1)} %get-tuple-element.41), channel_id=1, source_target_pairs={{0,1},{1,0},{2,3},{3,2},{4,5},{5,4},{6,7},{7,6},{8,9},{9,8},{10,11... | collective-permute-start | bytes 393224 | tf_op jit(solution)/shard_map/ppermute | solution.py:27

commit v11 on v9

--- a/solution.py
+++ b/solution.py
@@ -11,7 +11,8 @@
 
 
 BLOCK = 128
-SP = ("sp_0", "sp_1")
+Z = ("z_far", "z_near")
+SP = (*Z, "x")
 DP = ("dp_0", "dp_1")
 
 
@@ -172,9 +173,9 @@
         bottom[at : at + step] = array[:, half + at : half + at + step].T
 
 
-def norm_terms_body(full_width, rows, sums, pre, grad, table, flipped, bias, gain, top, bottom, joined_out, out, held, come):
-    n_x, tall, _ = out.shape
-    n_z = (tall - PACKED) // rows
+def norm_terms_body(full_width, rows, n_x, sums, pre, grad, table, flipped, bias, gain, top, bottom, joined_out, out, held, come):
+    n_first, tall, _ = out.shape
+    n_far, n_near = (tall - PACKED) // rows, n_first // n_x
     later, chunk, _ = held.shape
     loads = [
         pltpu.make_async_copy(bottom.at[pl.ds(i * chunk, chunk)], held.at[i], come.at[i])
@@ -208,11 +209,11 @@
     gating_back = inv_std * (back - first - centred * second)
     joined_out[:, width:] = (gating_back * gelu_slope(pre_gating)).astype(bf16)
     mixing_term = packed(causal(mixing_grad)).astype(bf16)
-    for x in range(n_x):
-        out[x, n_z * rows :] = mixing_term
+    for peer in range(n_first):
+        out[peer, n_far * rows :] = mixing_term
     slab = n_x * rows
     ready = top.shape[0] // slab
-    for z in range(n_z):
+    for z in range(n_far * n_near):
         if z < ready:
             part = top[z * slab : (z + 1) * slab]
         else:
@@ -221,18 +222,19 @@
                 loads[at // chunk].wait()
             part = held[at // chunk, at % chunk : at % chunk + slab]
         term = nn(part, joined_out[...]).astype(bf16)
+        at = z // n_near * rows
         for x in range(n_x):
-            out[x, z * rows : (z + 1) * rows] = term[x * rows : (x + 1) * rows]
-
-
-def norm_terms(full_width, small, top, bottom, n_x, n_z):
+            out[z % n_near * n_x + x, at : at + rows] = term[x * rows : (x + 1) * rows]
+
+
+def norm_terms(full_width, small, top, bottom, n_x, n_near, n_far):
     width, tokens = 2 * top.shape[0], top.shape[1]
     both = 2 * small[2].shape[1]
-    rows = width // (n_x * n_z)
+    rows = width // (n_x * n_near * n_far)
     near, far = pl.BlockSpec(memory_space=pltpu.VMEM), pl.BlockSpec(memory_space=pl.ANY)
     return pl.pallas_call(
-        functools.partial(norm_terms_body, full_width, rows),
-        out_shape=(like((tokens, both), bf16), stored((n_x, n_z * rows + PACKED, both), bf16)),
+        functools.partial(norm_terms_body, full_width, rows, n_x),
+        out_shape=(like((tokens, both), bf16), stored((n_near * n_x, n_far * rows + PACKED, both), bf16)),
         in_specs=[near] * (len(small) + 1) + [far],
         out_specs=(near, pl.BlockSpec()),
         scratch_shapes=[
@@ -328,8 +330,9 @@
     tok_rows, width = hidden_in.shape
     shard_rows, local_width = content_weight.shape
     both = 2 * local_width
-    n_z, n_x = lax.axis_size("sp_0"), lax.axis_size("sp_1")
+    n_z, n_x = lax.axis_size(Z), lax.axis_size("x")
     n_sp, n_dp = n_z * n_x, lax.axis_size(DP)
+    n_near, n_far = lax.axis_size("z_near"), lax.axis_size("z_far")
     ring = lax.axis_size("dp_0")
     full_width = local_width * n_dp
     out_cols = width // n_dp
@@ -346,9 +349,9 @@
     shards = call(join_body, stored((n_z, shard_rows, both), bf16), cold=(0, 1))(
         content_weight, gating_weight
     )
-    along_z = exchange(shards, "sp_0")
+    along_z = exchange(shards, Z)
     spread = call(spread_body, like((n_x, n_z, shard_rows, both), bf16))(along_z)
-    weight = exchange(spread, "sp_1")
+    weight = exchange(spread, "x")
     single, pair = (tok_rows, out_cols), (tok_rows, 2 * out_cols)
     wide_pair, picked = (tok_rows, 4 * out_cols), (width // 2, both)
     square = like((BLOCK, BLOCK), bf16)
@@ -366,10 +369,10 @@
     )(hidden_in, weight, mixing_weight, gain, out_grad)
     sums = exchange(sums, DP)
     small = (sums, pre, out_grad, table, flipped, mixing_bias, gain)
-    joined, terms = norm_terms(full_width, small, top, bottom, n_x, n_z)
+    joined, terms = norm_terms(full_width, small, top, bottom, n_x, n_near, n_far)
 
     joined_far = swapped(joined)
-    along_x = exchange(terms, "sp_1")
+    along_x = exchange(terms, ("z_near", "x"))
 
     odd, two, four, own = call(
         input_terms_body,
@@ -385,8 +388,8 @@
     other = sent_apart(other, 2, True)
     sent = swapped(send)
 
-    regrouped = call(regroup_body, stored((n_z, shard_rows + PACKED, both), bf16))(along_x)
-    arrived = exchange(regrouped, "sp_0")
+    regrouped = call(regroup_body, stored((n_far, shard_rows + PACKED, both), bf16))(along_x)
+    arrived = exchange(regrouped, "z_far")
 
     input_grad = call(total_body, outside(single, bf16))(own, same, other, keep, sent)
 
@@ -402,7 +405,7 @@
 
 
 def solution(mesh):
-    split = Mesh(mesh.devices.reshape(8, 4, 8, 2), (*SP, *DP))
+    split = Mesh(mesh.devices.reshape(4, 2, 4, 8, 2), (*SP, *DP))
     in_specs = (
         P(SP, None),
         P(SP, DP),

time: 122 us -> 116 us (0.951)
  the two profiles are of different devices: /device:TPU:9 before, /device:TPU:1 now
where the time goes in v11:
time: 116 us; the launch traced here: 115 us
  starting transfers between devices  38.1 us (33%)
  blocking collectives  37.9 us (33%)
  waiting for transfers between devices  20.9 us (18%)
  Pallas kernels  14.6 us (13%)
  local copies, waits for them, and re-layouts  2.74 us (2%)
    all_to_all x2, blocking collectives, exchange(): return lax.all_to_all(array, axis, split_axis=0, concat_axis=0, tiled=True)  37.9 us
    all_to_all x3, starting transfers between devices, exchange(): return lax.all_to_all(array, axis, split_axis=0, concat_axis=0, tiled=True)  17.7 us
    ppermute x4, starting transfers between devices, sent_apart(): return lax.ppermute(array, DP, moves)  14.2 us
    pallas_call x10, Pallas kernels, run(): return made(*operands)  11.7 us
    all_to_all x3, waiting for transfers between devices, exchange(): return lax.all_to_all(array, axis, split_axis=0, concat_axis=0, tiled=True)  11.7 us
    ppermute x4, waiting for transfers between devices, sent_apart(): return lax.ppermute(array, DP, moves)  8.06 us
    ppermute x3, starting transfers between devices, swapped(): return lax.ppermute(array, 'dp_1', [(0, 1), (1, 0)])  6.25 us
    pallas_call x1, Pallas kernels, norm_terms(): pl.pallas_call(functools.partial(norm_terms_body, full_width, rows, n_x),...  2.82 us
  transfers between devices with their start and end apart: 10, of which 5 were waited for; matrix products, arithmetic and copies ran while one was open for 0% of the time, Pallas kernels for 7%

profile of v11, /device:TPU:1, one launch (start us, length us, event | category | flops | bytes accessed | tf_op | source)
XLA Modules:
  0.0 114.9 jit_solution(11201718897216218457)
XLA Ops:
  0.6 1.5 %shard_map.102 = bf16[8,64,256]{2,1,0:T(8,128)(2,1)} custom-call(bf16[64,128]{1,0:T(8,128)(2,1)} %content.1, bf16[64,128]{1,0:T(8,128)(2,1)} %gating.1), custom_call_target="tpu_custom_call" | custom-call | tf_op jit(solution)/shard_map/pallas_call | solution.py:108
  2.1 21.3 %all_to_all.25.arrived = bf16[8,64,256]{2,1,0:T(8,128)(2,1)S(1)} all-to-all(bf16[8,64,256]{2,1,0:T(8,128)(2,1)} %shard_map.102), channel_id=1, replica_groups=mesh['z_far'=4,'z_near'=2,'x'=4,'dp_0'=8,'dp_1'=2] {'z_far','z_near'}, dimensions={0} | all-to-all | bytes 524288 | tf_op jit(solution)/shard_map/all_to_all | solution.py:24
  23.4 0.0 copy-start.3
  23.4 0.1 shard_map.103
  23.5 0.0 copy-start
  23.5 0.0 copy-start.7
  23.5 16.5 %all_to_all.26.weight = bf16[4,8,64,256]{3,2,1,0:T(8,128)(2,1)S(1)} all-to-all(bf16[4,8,64,256]{3,2,1,0:T(8,128)(2,1)S(1)} %shard_map.103), channel_id=1, replica_groups=mesh['z_far'=4,'z_near'=2,'x'=4,'dp_0'=8,'dp_1'=2] {'x'}, dimensions={0} | all-to-all | bytes 2097152 | tf_op jit(solution)/shard_map/all_to_all | solution.py:24
  40.1 0.0 copy-done.3
  40.1 0.0 copy-done.6
  40.1 0.0 copy-done
  40.1 0.0 copy-done.7
  40.1 1.8 %shard_map.104 = (bf16[512,256]{1,0:T(8,128)(2,1)S(1)}, f32[16,4,512]{2,1,0:T(4,128)}) custom-call(bf16[512,2048]{1,0:T(8,128)(2,1)S(1)} %copy-done, bf16[4,8,64,256]{3,2,1,0:T(8,128)(2,1)S(1)} %all_to_all.26.weight, bf16[1,128,128]{2,1,0:T(8,128)(2,1)S(1)} %copy-done.6, f32[1,128]{1,0:T(1,128)S(1)} %bitcast.11, bf16[512,128]{1,0:T(8,128)(2,1)S(1)} %copy-done.3), custom_call_target="tpu_custom_call" | custom-call | tf_op jit(solution)/shard_map/pallas_call | solution.py:108
  41.9 0.7 copy-done.4
  42.6 10.6 %all-to-all-start.2 = ((f32[16,4,512]{2,1,0:T(4,128)}), f32[16,4,512]{2,1,0:T(4,128)S(1)}, u32[]{:S(2)}, u32[]{:S(2)}) async-start(f32[16,4,512]{2,1,0:T(4,128)} %get-tuple-element.25), calls=%async_computation.2 | async-start | bytes 262144 | tf_op jit(solution)/shard_map/all_to_all | solution.py:24
  53.2 1.6 %shard_map.106 = (bf16[1024,512]{1,0:T(8,128)(2,1)S(1)}, bf16[1024,512]{1,0:T(8,128)(2,1)}) custom-call(bf16[512,2048]{1,0:T(8,128)(2,1)S(1)} %copy-done), custom_call_target="tpu_custom_call" | custom-call | tf_op jit(solution)/shard_map/pallas_call | solution.py:108
  54.8 1.0 copy-done.1
  55.8 0.1 stack.44.where
  55.9 1.9 %shard_map.105 = (bf16[1024,256]{1,0:T(8,128)(2,1)}, bf16[1024,256]{1,0:T(8,128)(2,1)}, bf16[128,128]{1,0:T(8,128)(2,1)S(1)}, bf16[128,128]{1,0:T(8,128)(2,1)S(1)}) custom-call(s32[11]{0:T(128)S(1)} %stack.44.where, bf16[4,8,64,256]{3,2,1,0:T(8,128)(2,1)S(1)} %all_to_all.26.weight, bf16[1,128,128]{2,1,0:T(8,128)(2,1)} %mixing.3), custom_call_target="tpu_custom_call" | custom-call | tf_op jit(solution)/shard_map/pallas_call | solution.py:108
  57.7 4.3 %all-to-all-done.2.sums = f32[16,4,512]{2,1,0:T(4,128)S(1)} async-done(((f32[16,4,512]{2,1,0:T(4,128)}), f32[16,4,512]{2,1,0:T(4,128)S(1)}, u32[]{:S(2)}, u32[]{:S(2)}) %all-to-all-start.2) | async-done | bytes 131104 | tf_op jit(solution)/shard_map/all_to_all | solution.py:24
  62.1 0.0 copy-done.8
  62.1 0.0 copy-done.2
  62.1 0.9 copy-done.5
  63.0 2.8 %norm_terms.1 = (bf16[512,256]{1,0:T(8,128)(2,1)S(1)}, bf16[8,296,256]{2,1,0:T(8,128)(2,1)}) custom-call(f32[16,4,512]{2,1,0:T(4,128)S(1)} %all-to-all-done.2.sums, bf16[512,256]{1,0:T(8,128)(2,1)S(1)} %copy-done.5, bf16[512,128]{1,0:T(8,128)(2,1)S(1)} %copy-done.3, bf16[128,128]{1,0:T(8,128)(2,1)S(1)} %get-tuple-element.27.table, ...), custom_call_target="tpu_custom_call" | custom-call | tf_op jit(solution)/shard_map/norm_terms/pallas_call | solution.py:235
  65.9 0.0 copy-start.9
  65.9 3.7 %all-to-all-start.3 = ((bf16[8,296,256]{2,1,0:T(8,128)(2,1)}), bf16[8,296,256]{2,1,0:T(8,128)(2,1)S(1)}, u32[]{:S(2)}, u32[]{:S(2)}) async-start(bf16[8,296,256]{2,1,0:T(8,128)(2,1)} %get-tuple-element.42), calls=%async_computation.3 | async-start | bytes 2424832 | tf_op jit(solution)/shard_map/all_to_all | solution.py:24
  69.6 0.0 copy-done.9
  69.6 1.9 %collective-permute-start.1 = (bf16[1024,256]{1,0:T(8,128)(2,1)S(1)}, bf16[1024,256]{1,0:T(8,128)(2,1)S(1)}, u32[]{:S(2)}, u32[]{:S(2)}) collective-permute-start(bf16[1024,256]{1,0:T(8,128)(2,1)S(1)} %copy-done.9), channel_id=1, source_target_pairs={{0,1},{1,0},{2,3},{3,2},{4,5},{5,4},{6,7},{7,6},{8,9},{9,8},{10,11... | collective-permute-start | bytes 1572872 | tf_op jit(solution)/shard_map/ppermute | solution.py:28
  71.5 2.4 %collective-permute-start = (bf16[512,256]{1,0:T(8,128)(2,1)S(1)}, bf16[512,256]{1,0:T(8,128)(2,1)S(1)}, u32[]{:S(2)}, u32[]{:S(2)}) collective-permute-start(bf16[512,256]{1,0:T(8,128)(2,1)S(1)} %get-tuple-element.31.joined), channel_id=1, source_target_pairs={{0,1},{1,0},{2,3},{3,2},{4,5},{5,4},{6,7},{7,6},{8,9},{9,8},{10,11... | collective-permute-start | bytes 786440 | tf_op jit(solution)/shard_map/ppermute | solution.py:28
  73.9 1.1 collective-permute-done.joined_far
  75.1 0.0 collective-permute-done.1.far
  75.1 1.9 %shard_map.107 = (bf16[512,512]{1,0:T(8,128)(2,1)S(1)}, f32[512,256]{1,0:T(8,128)S(1)}, bf16[512,128]{1,0:T(8,128)(2,1)S(1)}, f32[512,128]{1,0:T(8,128)S(1)}) custom-call(bf16[512,256]{1,0:T(8,128)(2,1)S(1)} %get-tuple-element.31.joined, bf16[512,256]{1,0:T(8,128)(2,1)S(1)} %collective-permute-done.joined_far, bf16[1024,256]{1,0:T(8,128)(2,1)} %get-tuple-element.32.mine, ...), custom_call_target="tpu_custom_call" | custom-call | tf_op jit(solution)/shard_map/pallas_call | solution.py:108
  77.0 2.0 %collective-permute-start.2 = (bf16[512,512]{1,0:T(8,128)(2,1)S(1)}, bf16[512,512]{1,0:T(8,128)(2,1)S(1)}, u32[]{:S(2)}, u32[]{:S(2)}) collective-permute-start(bf16[512,512]{1,0:T(8,128)(2,1)S(1)} %get-tuple-element.36), channel_id=1, source_target_pairs={{0,2},{1,15},{2,4},{3,1},{4,6},{5,3},{6,8},{7,5},{8,10},{9,7},{10,... | collective-permute-start | bytes 1572872 | tf_op jit(solution)/shard_map/ppermute | solution.py:37
  79.0 7.3 %all-to-all-done.3.arrived = bf16[8,296,256]{2,1,0:T(8,128)(2,1)S(1)} async-done(((bf16[8,296,256]{2,1,0:T(8,128)(2,1)}), bf16[8,296,256]{2,1,0:T(8,128)(2,1)S(1)}, u32[]{:S(2)}, u32[]{:S(2)}) %all-to-all-start.3) | async-done | bytes 1212448 | tf_op jit(solution)/shard_map/all_to_all | solution.py:24
  86.3 0.8 shard_map.110
  87.1 3.4 %all-to-all-start.4 = ((bf16[4,104,256]{2,1,0:T(8,128)(2,1)}), bf16[4,104,256]{2,1,0:T(8,128)(2,1)S(1)}, u32[]{:S(2)}, u32[]{:S(2)}) async-start(bf16[4,104,256]{2,1,0:T(8,128)(2,1)} %shard_map.110), calls=%async_computation.4 | async-start | bytes 425984 | tf_op jit(solution)/shard_map/all_to_all | solution.py:24
  90.5 2.4 %collective-permute-start.3 = (bf16[512,128]{1,0:T(8,128)(2,1)S(1)}, bf16[512,128]{1,0:T(8,128)(2,1)S(1)}, u32[]{:S(2)}, u32[]{:S(2)}) collective-permute-start(bf16[512,128]{1,0:T(8,128)(2,1)S(1)} %get-tuple-element.37), channel_id=1, source_target_pairs={{0,4},{1,13},{2,6},{3,15},{4,8},{5,1},{6,10},{7,3},{8,12},{9,5},{1... | collective-permute-start | bytes 393224 | tf_op jit(solution)/shard_map/ppermute | solution.py:37
  92.9 5.9 %collective-permute-done.3.four = bf16[512,128]{1,0:T(8,128)(2,1)S(1)} collective-permute-done((bf16[512,128]{1,0:T(8,128)(2,1)S(1)}, bf16[512,128]{1,0:T(8,128)(2,1)S(1)}, u32[]{:S(2)}, u32[]{:S(2)}) %collective-permute-start.3) | collective-permute-done | bytes 131104 | tf_op jit(solution)/shard_map/ppermute | solution.py:37
  98.8 0.0 collective-permute-done.2.odd
  98.8 0.7 shard_map.108
  99.5 3.7 %collective-permute-start.4 = (bf16[512,128]{1,0:T(8,128)(2,1)S(1)}, bf16[512,128]{1,0:T(8,128)(2,1)S(1)}, u32[]{:S(2)}, u32[]{:S(2)}) collective-permute-start(bf16[512,128]{1,0:T(8,128)(2,1)S(1)} %get-tuple-element.38), channel_id=1, source_target_pairs={{0,4},{1,13},{2,6},{3,15},{4,8},{5,1},{6,10},{7,3},{8,12},{9,5},{1... | collective-permute-start | bytes 393224 | tf_op jit(solution)/shard_map/ppermute | solution.py:37
  103.1 6.2 %collective-permute-start.5 = (bf16[512,128]{1,0:T(8,128)(2,1)S(1)}, bf16[512,128]{1,0:T(8,128)(2,1)S(1)}, u32[]{:S(2)}, u32[]{:S(2)}) collective-permute-start(bf16[512,128]{1,0:T(8,128)(2,1)S(1)} %get-tuple-element.39), channel_id=1, source_target_pairs={{0,5},{1,12},{2,7},{3,14},{4,9},{5,0},{6,11},{7,2},{8,13},{9,4},{1... | collective-permute-start | bytes 393224 | tf_op jit(solution)/shard_map/ppermute | solution.py:37
  109.3 1.9 %collective-permute-start.6 = (bf16[512,128]{1,0:T(8,128)(2,1)S(1)}, bf16[512,128]{1,0:T(8,128)(2,1)S(1)}, u32[]{:S(2)}, u32[]{:S(2)}) collective-permute-start(bf16[512,128]{1,0:T(8,128)(2,1)S(1)} %get-tuple-element.41), channel_id=1, source_target_pairs={{0,1},{1,0},{2,3},{3,2},{4,5},{5,4},{6,7},{7,6},{8,9},{9,8},{10,11... | collective-permute-start | bytes 393224 | tf_op jit(solution)/shard_map/ppermute | solution.py:28
  111.2 0.0 collective-permute-done.4.same
  111.2 2.2 %collective-permute-done.5.other = bf16[512,128]{1,0:T(8,128)(2,1)S(1)} collective-permute-done((bf16[512,128]{1,0:T(8,128)(2,1)S(1)}, bf16[512,128]{1,0:T(8,128)(2,1)S(1)}, u32[]{:S(2)}, u32[]{:S(2)}) %collective-permute-start.5) | collective-permute-done | bytes 131104 | tf_op jit(solution)/shard_map/ppermute | solution.py:37
  113.4 0.0 collective-permute-done.6.sent
  113.5 0.7 shard_map.109
  114.2 0.0 all-to-all-done.4.arrived
  114.2 0.7 shard_map.111
  (6 shorter events, 0.0 us)
Async XLA Ops:
  23.4 16.6 %copy-start.3 = (bf16[512,128]{1,0:T(8,128)(2,1)S(1)}, bf16[512,128]{1,0:T(8,128)(2,1)}, u32[]{:S(2)}) copy-start(bf16[512,128]{1,0:T(8,128)(2,1)} %grad.3) | copy-start | bytes 393220
  23.4 16.6 %copy-start.6 = (bf16[1,128,128]{2,1,0:T(8,128)(2,1)S(1)}, bf16[1,128,128]{2,1,0:T(8,128)(2,1)}, u32[]{:S(2)}) copy-start(bf16[1,128,128]{2,1,0:T(8,128)(2,1)} %mixing.3) | copy-start | bytes 98308
  23.5 16.6 %copy-start = (bf16[512,2048]{1,0:T(8,128)(2,1)S(1)}, bf16[512,2048]{1,0:T(8,128)(2,1)}, u32[]{:S(2)}) copy-start(bf16[512,2048]{1,0:T(8,128)(2,1)} %array.1) | copy-start | bytes 6291460
  23.5 16.5 %copy-start.7 = (f32[128]{0:T(128)S(1)}, f32[128]{0:T(128)}, u32[]{:S(2)}) copy-start(f32[128]{0:T(128)} %param.10) | copy-start | bytes 1540
  41.9 0.7 copy-start.4
  42.6 19.5 %all-to-all-start.2 = ((f32[16,4,512]{2,1,0:T(4,128)}), f32[16,4,512]{2,1,0:T(4,128)S(1)}, u32[]{:S(2)}, u32[]{:S(2)}) async-start(f32[16,4,512]{2,1,0:T(4,128)} %get-tuple-element.25), calls=%async_computation.2 | async-start | bytes 262144 | tf_op jit(solution)/shard_map/all_to_all | solution.py:24
  53.2 8.9 %copy-start.8 = (f32[1,128]{1,0:T(1,128)S(1)}, f32[1,128]{1,0:T(1,128)}, u32[]{:S(2)}) copy-start(f32[1,128]{1,0:T(1,128)} %bias.1) | copy-start | bytes 1540
  54.8 1.0 copy-start.1
  55.8 6.3 %copy-start.2 = (bf16[1024,512]{1,0:T(8,128)(2,1)S(1)}, bf16[1024,512]{1,0:T(8,128)(2,1)}, u32[]{:S(2)}) copy-start(bf16[1024,512]{1,0:T(8,128)(2,1)} %copy-done.1) | copy-start | bytes 3145732
  62.1 1.0 copy-start.5
  65.9 3.7 %copy-start.9 = (bf16[1024,256]{1,0:T(8,128)(2,1)S(1)}, bf16[1024,256]{1,0:T(8,128)(2,1)}, u32[]{:S(2)}) copy-start(bf16[1024,256]{1,0:T(8,128)(2,1)} %get-tuple-element.33) | copy-start | bytes 1572868
  65.9 20.4 %all-to-all-start.3 = ((bf16[8,296,256]{2,1,0:T(8,128)(2,1)}), bf16[8,296,256]{2,1,0:T(8,128)(2,1)S(1)}, u32[]{:S(2)}, u32[]{:S(2)}) async-start(bf16[8,296,256]{2,1,0:T(8,128)(2,1)} %get-tuple-element.42), calls=%async_computation.3 | async-start | bytes 2424832 | tf_op jit(solution)/shard_map/all_to_all | solution.py:24
  69.6 5.5 %collective-permute-start.1 = (bf16[1024,256]{1,0:T(8,128)(2,1)S(1)}, bf16[1024,256]{1,0:T(8,128)(2,1)S(1)}, u32[]{:S(2)}, u32[]{:S(2)}) collective-permute-start(bf16[1024,256]{1,0:T(8,128)(2,1)S(1)} %copy-done.9), channel_id=1, source_target_pairs={{0,1},{1,0},{2,3},{3,2},{4,5},{5,4},{6,7},{7,6},{8,9},{9,8},{10,11... | collective-permute-start | bytes 1572872 | tf_op jit(solution)/shard_map/ppermute | solution.py:28
  71.5 3.6 %collective-permute-start = (bf16[512,256]{1,0:T(8,128)(2,1)S(1)}, bf16[512,256]{1,0:T(8,128)(2,1)S(1)}, u32[]{:S(2)}, u32[]{:S(2)}) collective-permute-start(bf16[512,256]{1,0:T(8,128)(2,1)S(1)} %get-tuple-element.31.joined), channel_id=1, source_target_pairs={{0,1},{1,0},{2,3},{3,2},{4,5},{5,4},{6,7},{7,6},{8,9},{9,8},{10,11... | collective-permute-start | bytes 786440 | tf_op jit(solution)/shard_map/ppermute | solution.py:28
  77.0 21.8 %collective-permute-start.2 = (bf16[512,512]{1,0:T(8,128)(2,1)S(1)}, bf16[512,512]{1,0:T(8,128)(2,1)S(1)}, u32[]{:S(2)}, u32[]{:S(2)}) collective-permute-start(bf16[512,512]{1,0:T(8,128)(2,1)S(1)} %get-tuple-element.36), channel_id=1, source_target_pairs={{0,2},{1,15},{2,4},{3,1},{4,6},{5,3},{6,8},{7,5},{8,10},{9,7},{10,... | collective-permute-start | bytes 1572872 | tf_op jit(solution)/shard_map/ppermute | solution.py:37
  87.1 27.0 %all-to-all-start.4 = ((bf16[4,104,256]{2,1,0:T(8,128)(2,1)}), bf16[4,104,256]{2,1,0:T(8,128)(2,1)S(1)}, u32[]{:S(2)}, u32[]{:S(2)}) async-start(bf16[4,104,256]{2,1,0:T(8,128)(2,1)} %shard_map.110), calls=%async_computation.4 | async-start | bytes 425984 | tf_op jit(solution)/shard_map/all_to_all | solution.py:24
  90.5 8.2 %collective-permute-start.3 = (bf16[512,128]{1,0:T(8,128)(2,1)S(1)}, bf16[512,128]{1,0:T(8,128)(2,1)S(1)}, u32[]{:S(2)}, u32[]{:S(2)}) collective-permute-start(bf16[512,128]{1,0:T(8,128)(2,1)S(1)} %get-tuple-element.37), channel_id=1, source_target_pairs={{0,4},{1,13},{2,6},{3,15},{4,8},{5,1},{6,10},{7,3},{8,12},{9,5},{1... | collective-permute-start | bytes 393224 | tf_op jit(solution)/shard_map/ppermute | solution.py:37
  99.5 11.8 %collective-permute-start.4 = (bf16[512,128]{1,0:T(8,128)(2,1)S(1)}, bf16[512,128]{1,0:T(8,128)(2,1)S(1)}, u32[]{:S(2)}, u32[]{:S(2)}) collective-permute-start(bf16[512,128]{1,0:T(8,128)(2,1)S(1)} %get-tuple-element.38), channel_id=1, source_target_pairs={{0,4},{1,13},{2,6},{3,15},{4,8},{5,1},{6,10},{7,3},{8,12},{9,5},{1... | collective-permute-start | bytes 393224 | tf_op jit(solution)/shard_map/ppermute | solution.py:37
  103.1 10.3 %collective-permute-start.5 = (bf16[512,128]{1,0:T(8,128)(2,1)S(1)}, bf16[512,128]{1,0:T(8,128)(2,1)S(1)}, u32[]{:S(2)}, u32[]{:S(2)}) collective-permute-start(bf16[512,128]{1,0:T(8,128)(2,1)S(1)} %get-tuple-element.39), channel_id=1, source_target_pairs={{0,5},{1,12},{2,7},{3,14},{4,9},{5,0},{6,11},{7,2},{8,13},{9,4},{1... | collective-permute-start | bytes 393224 | tf_op jit(solution)/shard_map/ppermute | solution.py:37
  109.3 4.1 %collective-permute-start.6 = (bf16[512,128]{1,0:T(8,128)(2,1)S(1)}, bf16[512,128]{1,0:T(8,128)(2,1)S(1)}, u32[]{:S(2)}, u32[]{:S(2)}) collective-permute-start(bf16[512,128]{1,0:T(8,128)(2,1)S(1)} %get-tuple-element.41), channel_id=1, source_target_pairs={{0,1},{1,0},{2,3},{3,2},{4,5},{5,4},{6,7},{7,6},{8,9},{9,8},{10,11... | collective-permute-start | bytes 393224 | tf_op jit(solution)/shard_map/ppermute | solution.py:28

commit v12 on v11

--- a/solution.py
+++ b/solution.py
@@ -122,12 +122,15 @@
     return jax.ShapeDtypeStruct(shape, dtype)
 
 
-def project_body(hidden, weight, mixing, gain, grad, pre_out, sums_out):
-    n_x, n_z, rows, both = weight.shape
+def project_body(n_x, hidden, weight, mixing, gain, grad, pre_out, sums_out):
+    n_first, n_far, rows, both = weight.shape
     slab = n_x * rows
+    n_near = n_first // n_x
     pre = None
-    for z in range(n_z):
-        term = nn(hidden[:, z * slab : (z + 1) * slab], weight[:, z].reshape(slab, both))
+    for z in range(n_far * n_near):
+        near = z % n_near * n_x
+        block = weight[near : near + n_x, z // n_near].reshape(slab, both)
+        term = nn(hidden[:, z * slab : (z + 1) * slab], block)
         pre = term if pre is None else pre + term
     pre = pre.astype(bf16)
     pre_out[...] = pre
@@ -249,20 +252,24 @@
     )
 
 
-def pick_body(where, weight, mixing, mine_out, theirs_out, table_out, flipped_out):
+def pick_body(n_x, where, weight, mixing, mine_out, theirs_out, table_out, flipped_out):
     table = causal(mixing[0].astype(f32))
     table_out[...] = table.astype(bf16)
     flipped_out[...] = table.T.astype(bf16)
-    n_x, _, rows, both = weight.shape
+    n_first, _, rows, both = weight.shape
+    n_near = n_first // n_x
     half = n_x // 2
     for out, base, core in ((mine_out, 0, where[10]), (theirs_out, 5, 1 - where[10])):
         at = 0
         for step in (3, 1, 2):
-            block = weight[:, pl.ds(where[base + step], 1)].reshape(n_x * rows, both)
+            z = where[base + step]
+            block = weight[pl.ds(z % n_near * n_x, n_x), pl.ds(z // n_near, 1)]
+            block = block.reshape(n_x * rows, both)
             out[at : at + n_x * rows] = block
             at += n_x * rows
         for step in (4, 0):
-            block = weight[pl.ds(core * half, half), pl.ds(where[base + step], 1)]
+            z = where[base + step]
+            block = weight[pl.ds(z % n_near * n_x + core * half, half), pl.ds(z // n_near, 1)]
             out[at : at + half * rows] = block.reshape(half * rows, both)
             at += half * rows
 
@@ -346,17 +353,17 @@
 
     half = (width // 2, tok_rows)
     top, bottom = call(flip_body, (like(half, bf16), stored(half, bf16)))(hidden_in)
-    shards = call(join_body, stored((n_z, shard_rows, both), bf16), cold=(0, 1))(
+    shards = call(join_body, stored((n_far, shard_rows, both), bf16), cold=(0, 1))(
         content_weight, gating_weight
     )
-    along_z = exchange(shards, Z)
-    spread = call(spread_body, like((n_x, n_z, shard_rows, both), bf16))(along_z)
-    weight = exchange(spread, "x")
+    along_z = exchange(shards, "z_far")
+    spread = call(spread_body, like((n_near * n_x, n_far, shard_rows, both), bf16))(along_z)
+    weight = exchange(spread, ("z_near", "x"))
     single, pair = (tok_rows, out_cols), (tok_rows, 2 * out_cols)
     wide_pair, picked = (tok_rows, 4 * out_cols), (width // 2, both)
     square = like((BLOCK, BLOCK), bf16)
     mine, theirs, table, flipped = call(
-        pick_body,
+        functools.partial(pick_body, n_x),
         (stored(picked, bf16), stored(picked, bf16), square, square),
         scalars=True,
         cold=(2,),
@@ -365,7 +372,7 @@
 
     wide = (tok_rows, both)
     pre, sums = call(
-        project_body, (like(wide, bf16), stored((n_dp, 4, tok_rows), f32))
+        functools.partial(project_body, n_x), (like(wide, bf16), stored((n_dp, 4, tok_rows), f32))
     )(hidden_in, weight, mixing_weight, gain, out_grad)
     sums = exchange(sums, DP)
     small = (sums, pre, out_grad, table, flipped, mixing_bias, gain)

time: 116 us -> 114 us (0.983)
  blocking collectives: 37.9 us -> 36.2 us
    all_to_all x2, blocking collectives: 37.9 us -> 36.2 us  [exchange(): return lax.all_to_all(array, axis, split_axis=0, concat_axis=0, tiled=True)]
where the time goes in v12:
time: 114 us; the launch traced here: 113 us
  starting transfers between devices  38.2 us (34%)
  blocking collectives  36.2 us (32%)
  waiting for transfers between devices  20.9 us (18%)
  Pallas kernels  14.5 us (13%)
  local copies, waits for them, and re-layouts  2.74 us (2%)
    all_to_all x2, blocking collectives, exchange(): return lax.all_to_all(array, axis, split_axis=0, concat_axis=0, tiled=True)  36.2 us
    all_to_all x3, starting transfers between devices, exchange(): return lax.all_to_all(array, axis, split_axis=0, concat_axis=0, tiled=True)  17.8 us
    ppermute x4, starting transfers between devices, sent_apart(): return lax.ppermute(array, DP, moves)  14.2 us
    pallas_call x10, Pallas kernels, run(): return made(*operands)  11.7 us
    all_to_all x3, waiting for transfers between devices, exchange(): return lax.all_to_all(array, axis, split_axis=0, concat_axis=0, tiled=True)  11.7 us
    ppermute x4, waiting for transfers between devices, sent_apart(): return lax.ppermute(array, DP, moves)  8.07 us
    ppermute x3, starting transfers between devices, swapped(): return lax.ppermute(array, 'dp_1', [(0, 1), (1, 0)])  6.25 us
    pallas_call x1, Pallas kernels, norm_terms(): pl.pallas_call(functools.partial(norm_terms_body, full_width, rows, n_x),...  2.82 us
  transfers between devices with their start and end apart: 10, of which 5 were waited for; matrix products, arithmetic and copies ran while one was open for 0% of the time, Pallas kernels for 7%

profile of v12, /device:TPU:1, one launch (start us, length us, event | category | flops | bytes accessed | tf_op | source)
XLA Modules:
  0.0 113.4 jit_solution(3807130656101653164)
XLA Ops:
  0.6 1.4 %shard_map.102 = bf16[4,64,256]{2,1,0:T(8,128)(2,1)} custom-call(bf16[64,128]{1,0:T(8,128)(2,1)} %content.1, bf16[64,128]{1,0:T(8,128)(2,1)} %gating.1), custom_call_target="tpu_custom_call" | custom-call | tf_op jit(solution)/shard_map/pallas_call | solution.py:108
  2.0 18.4 %all_to_all.25.arrived = bf16[4,64,256]{2,1,0:T(8,128)(2,1)S(1)} all-to-all(bf16[4,64,256]{2,1,0:T(8,128)(2,1)} %shard_map.102), channel_id=1, replica_groups=mesh['z_far'=4,'z_near'=2,'x'=4,'dp_0'=8,'dp_1'=2] {'z_far'}, dimensions={0} | all-to-all | bytes 262144 | tf_op jit(solution)/shard_map/all_to_all | solution.py:24
  20.4 0.0 copy-start.3
  20.4 0.1 shard_map.103
  20.5 0.0 copy-start
  20.5 0.0 copy-start.7
  20.5 17.9 %all_to_all.26.weight = bf16[8,4,64,256]{3,2,1,0:T(8,128)(2,1)S(1)} all-to-all(bf16[8,4,64,256]{3,2,1,0:T(8,128)(2,1)S(1)} %shard_map.103), channel_id=1, replica_groups=mesh['z_far'=4,'z_near'=2,'x'=4,'dp_0'=8,'dp_1'=2] {'z_near','x'}, dimensions={0} | all-to-all | bytes 2097152 | tf_op jit(solution)/shard_map/all_to_all | solution.py:24
  38.4 0.0 copy-done.3
  38.4 0.0 copy-done.6
  38.4 0.0 copy-done
  38.4 0.0 copy-done.7
  38.4 1.8 %shard_map.104 = (bf16[512,256]{1,0:T(8,128)(2,1)S(1)}, f32[16,4,512]{2,1,0:T(4,128)}) custom-call(bf16[512,2048]{1,0:T(8,128)(2,1)S(1)} %copy-done, bf16[8,4,64,256]{3,2,1,0:T(8,128)(2,1)S(1)} %all_to_all.26.weight, bf16[1,128,128]{2,1,0:T(8,128)(2,1)S(1)} %copy-done.6, f32[1,128]{1,0:T(1,128)S(1)} %bitcast.11, bf16[512,128]{1,0:T(8,128)(2,1)S(1)} %copy-done.3), custom_call_target="tpu_custom_call" | custom-call | tf_op jit(solution)/shard_map/pallas_call | solution.py:108
  40.2 0.7 copy-done.4
  40.9 10.7 %all-to-all-start.2 = ((f32[16,4,512]{2,1,0:T(4,128)}), f32[16,4,512]{2,1,0:T(4,128)S(1)}, u32[]{:S(2)}, u32[]{:S(2)}) async-start(f32[16,4,512]{2,1,0:T(4,128)} %get-tuple-element.25), calls=%async_computation.2 | async-start | bytes 262144 | tf_op jit(solution)/shard_map/all_to_all | solution.py:24
  51.6 1.6 %shard_map.106 = (bf16[1024,512]{1,0:T(8,128)(2,1)S(1)}, bf16[1024,512]{1,0:T(8,128)(2,1)}) custom-call(bf16[512,2048]{1,0:T(8,128)(2,1)S(1)} %copy-done), custom_call_target="tpu_custom_call" | custom-call | tf_op jit(solution)/shard_map/pallas_call | solution.py:108
  53.2 1.0 copy-done.1
  54.2 0.1 stack.44.where
  54.3 1.9 %shard_map.105 = (bf16[1024,256]{1,0:T(8,128)(2,1)}, bf16[1024,256]{1,0:T(8,128)(2,1)}, bf16[128,128]{1,0:T(8,128)(2,1)S(1)}, bf16[128,128]{1,0:T(8,128)(2,1)S(1)}) custom-call(s32[11]{0:T(128)S(1)} %stack.44.where, bf16[8,4,64,256]{3,2,1,0:T(8,128)(2,1)S(1)} %all_to_all.26.weight, bf16[1,128,128]{2,1,0:T(8,128)(2,1)} %mixing.3), custom_call_target="tpu_custom_call" | custom-call | tf_op jit(solution)/shard_map/pallas_call | solution.py:108
  56.2 4.3 %all-to-all-done.2.sums = f32[16,4,512]{2,1,0:T(4,128)S(1)} async-done(((f32[16,4,512]{2,1,0:T(4,128)}), f32[16,4,512]{2,1,0:T(4,128)S(1)}, u32[]{:S(2)}, u32[]{:S(2)}) %all-to-all-start.2) | async-done | bytes 131104 | tf_op jit(solution)/shard_map/all_to_all | solution.py:24
  60.5 0.0 copy-done.8
  60.5 0.0 copy-done.2
  60.5 0.9 copy-done.5
  61.5 2.8 %norm_terms.1 = (bf16[512,256]{1,0:T(8,128)(2,1)S(1)}, bf16[8,296,256]{2,1,0:T(8,128)(2,1)}) custom-call(f32[16,4,512]{2,1,0:T(4,128)S(1)} %all-to-all-done.2.sums, bf16[512,256]{1,0:T(8,128)(2,1)S(1)} %copy-done.5, bf16[512,128]{1,0:T(8,128)(2,1)S(1)} %copy-done.3, bf16[128,128]{1,0:T(8,128)(2,1)S(1)} %get-tuple-element.27.table, ...), custom_call_target="tpu_custom_call" | custom-call | tf_op jit(solution)/shard_map/norm_terms/pallas_call | solution.py:238
  64.3 0.0 copy-start.9
  64.3 3.7 %all-to-all-start.3 = ((bf16[8,296,256]{2,1,0:T(8,128)(2,1)}), bf16[8,296,256]{2,1,0:T(8,128)(2,1)S(1)}, u32[]{:S(2)}, u32[]{:S(2)}) async-start(bf16[8,296,256]{2,1,0:T(8,128)(2,1)} %get-tuple-element.42), calls=%async_computation.3 | async-start | bytes 2424832 | tf_op jit(solution)/shard_map/all_to_all | solution.py:24
  68.0 0.0 copy-done.9
  68.0 1.9 %collective-permute-start.1 = (bf16[1024,256]{1,0:T(8,128)(2,1)S(1)}, bf16[1024,256]{1,0:T(8,128)(2,1)S(1)}, u32[]{:S(2)}, u32[]{:S(2)}) collective-permute-start(bf16[1024,256]{1,0:T(8,128)(2,1)S(1)} %copy-done.9), channel_id=1, source_target_pairs={{0,1},{1,0},{2,3},{3,2},{4,5},{5,4},{6,7},{7,6},{8,9},{9,8},{10,11... | collective-permute-start | bytes 1572872 | tf_op jit(solution)/shard_map/ppermute | solution.py:28
  70.0 2.4 %collective-permute-start = (bf16[512,256]{1,0:T(8,128)(2,1)S(1)}, bf16[512,256]{1,0:T(8,128)(2,1)S(1)}, u32[]{:S(2)}, u32[]{:S(2)}) collective-permute-start(bf16[512,256]{1,0:T(8,128)(2,1)S(1)} %get-tuple-element.31.joined), channel_id=1, source_target_pairs={{0,1},{1,0},{2,3},{3,2},{4,5},{5,4},{6,7},{7,6},{8,9},{9,8},{10,11... | collective-permute-start | bytes 786440 | tf_op jit(solution)/shard_map/ppermute | solution.py:28
  72.4 1.1 %collective-permute-done.joined_far = bf16[512,256]{1,0:T(8,128)(2,1)S(1)} collective-permute-done((bf16[512,256]{1,0:T(8,128)(2,1)S(1)}, bf16[512,256]{1,0:T(8,128)(2,1)S(1)}, u32[]{:S(2)}, u32[]{:S(2)}) %collective-permute-start) | collective-permute-done | bytes 262176 | tf_op jit(solution)/shard_map/ppermute | solution.py:28
  73.5 0.0 collective-permute-done.1.far
  73.5 1.9 %shard_map.107 = (bf16[512,512]{1,0:T(8,128)(2,1)S(1)}, f32[512,256]{1,0:T(8,128)S(1)}, bf16[512,128]{1,0:T(8,128)(2,1)S(1)}, f32[512,128]{1,0:T(8,128)S(1)}) custom-call(bf16[512,256]{1,0:T(8,128)(2,1)S(1)} %get-tuple-element.31.joined, bf16[512,256]{1,0:T(8,128)(2,1)S(1)} %collective-permute-done.joined_far, bf16[1024,256]{1,0:T(8,128)(2,1)} %get-tuple-element.32.mine, ...), custom_call_target="tpu_custom_call" | custom-call | tf_op jit(solution)/shard_map/pallas_call | solution.py:108
  75.4 2.0 %collective-permute-start.2 = (bf16[512,512]{1,0:T(8,128)(2,1)S(1)}, bf16[512,512]{1,0:T(8,128)(2,1)S(1)}, u32[]{:S(2)}, u32[]{:S(2)}) collective-permute-start(bf16[512,512]{1,0:T(8,128)(2,1)S(1)} %get-tuple-element.36), channel_id=1, source_target_pairs={{0,2},{1,15},{2,4},{3,1},{4,6},{5,3},{6,8},{7,5},{8,10},{9,7},{10,... | collective-permute-start | bytes 1572872 | tf_op jit(solution)/shard_map/ppermute | solution.py:37
  77.4 7.3 %all-to-all-done.3.arrived = bf16[8,296,256]{2,1,0:T(8,128)(2,1)S(1)} async-done(((bf16[8,296,256]{2,1,0:T(8,128)(2,1)}), bf16[8,296,256]{2,1,0:T(8,128)(2,1)S(1)}, u32[]{:S(2)}, u32[]{:S(2)}) %all-to-all-start.3) | async-done | bytes 1212448 | tf_op jit(solution)/shard_map/all_to_all | solution.py:24
  84.7 0.8 shard_map.110
  85.6 3.4 %all-to-all-start.4 = ((bf16[4,104,256]{2,1,0:T(8,128)(2,1)}), bf16[4,104,256]{2,1,0:T(8,128)(2,1)S(1)}, u32[]{:S(2)}, u32[]{:S(2)}) async-start(bf16[4,104,256]{2,1,0:T(8,128)(2,1)} %shard_map.110), calls=%async_computation.4 | async-start | bytes 425984 | tf_op jit(solution)/shard_map/all_to_all | solution.py:24
  89.0 2.4 %collective-permute-start.3 = (bf16[512,128]{1,0:T(8,128)(2,1)S(1)}, bf16[512,128]{1,0:T(8,128)(2,1)S(1)}, u32[]{:S(2)}, u32[]{:S(2)}) collective-permute-start(bf16[512,128]{1,0:T(8,128)(2,1)S(1)} %get-tuple-element.37), channel_id=1, source_target_pairs={{0,4},{1,13},{2,6},{3,15},{4,8},{5,1},{6,10},{7,3},{8,12},{9,5},{1... | collective-permute-start | bytes 393224 | tf_op jit(solution)/shard_map/ppermute | solution.py:37
  91.3 5.9 %collective-permute-done.3.four = bf16[512,128]{1,0:T(8,128)(2,1)S(1)} collective-permute-done((bf16[512,128]{1,0:T(8,128)(2,1)S(1)}, bf16[512,128]{1,0:T(8,128)(2,1)S(1)}, u32[]{:S(2)}, u32[]{:S(2)}) %collective-permute-start.3) | collective-permute-done | bytes 131104 | tf_op jit(solution)/shard_map/ppermute | solution.py:37
  97.2 0.0 collective-permute-done.2.odd
  97.2 0.7 shard_map.108
  97.9 3.7 %collective-permute-start.4 = (bf16[512,128]{1,0:T(8,128)(2,1)S(1)}, bf16[512,128]{1,0:T(8,128)(2,1)S(1)}, u32[]{:S(2)}, u32[]{:S(2)}) collective-permute-start(bf16[512,128]{1,0:T(8,128)(2,1)S(1)} %get-tuple-element.38), channel_id=1, source_target_pairs={{0,4},{1,13},{2,6},{3,15},{4,8},{5,1},{6,10},{7,3},{8,12},{9,5},{1... | collective-permute-start | bytes 393224 | tf_op jit(solution)/shard_map/ppermute | solution.py:37
  101.5 6.2 %collective-permute-start.5 = (bf16[512,128]{1,0:T(8,128)(2,1)S(1)}, bf16[512,128]{1,0:T(8,128)(2,1)S(1)}, u32[]{:S(2)}, u32[]{:S(2)}) collective-permute-start(bf16[512,128]{1,0:T(8,128)(2,1)S(1)} %get-tuple-element.39), channel_id=1, source_target_pairs={{0,5},{1,12},{2,7},{3,14},{4,9},{5,0},{6,11},{7,2},{8,13},{9,4},{1... | collective-permute-start | bytes 393224 | tf_op jit(solution)/shard_map/ppermute | solution.py:37
  107.7 1.9 %collective-permute-start.6 = (bf16[512,128]{1,0:T(8,128)(2,1)S(1)}, bf16[512,128]{1,0:T(8,128)(2,1)S(1)}, u32[]{:S(2)}, u32[]{:S(2)}) collective-permute-start(bf16[512,128]{1,0:T(8,128)(2,1)S(1)} %get-tuple-element.41), channel_id=1, source_target_pairs={{0,1},{1,0},{2,3},{3,2},{4,5},{5,4},{6,7},{7,6},{8,9},{9,8},{10,11... | collective-permute-start | bytes 393224 | tf_op jit(solution)/shard_map/ppermute | solution.py:28
  109.7 0.0 collective-permute-done.4.same
  109.7 2.2 %collective-permute-done.5.other = bf16[512,128]{1,0:T(8,128)(2,1)S(1)} collective-permute-done((bf16[512,128]{1,0:T(8,128)(2,1)S(1)}, bf16[512,128]{1,0:T(8,128)(2,1)S(1)}, u32[]{:S(2)}, u32[]{:S(2)}) %collective-permute-start.5) | collective-permute-done | bytes 131104 | tf_op jit(solution)/shard_map/ppermute | solution.py:37
  111.9 0.0 collective-permute-done.6.sent
  111.9 0.7 shard_map.109
  112.6 0.0 all-to-all-done.4.arrived
  112.6 0.7 shard_map.111
  (6 shorter events, 0.0 us)
Async XLA Ops:
  20.4 18.0 %copy-start.3 = (bf16[512,128]{1,0:T(8,128)(2,1)S(1)}, bf16[512,128]{1,0:T(8,128)(2,1)}, u32[]{:S(2)}) copy-start(bf16[512,128]{1,0:T(8,128)(2,1)} %grad.3) | copy-start | bytes 393220
  20.4 18.0 %copy-start.6 = (bf16[1,128,128]{2,1,0:T(8,128)(2,1)S(1)}, bf16[1,128,128]{2,1,0:T(8,128)(2,1)}, u32[]{:S(2)}) copy-start(bf16[1,128,128]{2,1,0:T(8,128)(2,1)} %mixing.3) | copy-start | bytes 98308
  20.5 17.9 %copy-start = (bf16[512,2048]{1,0:T(8,128)(2,1)S(1)}, bf16[512,2048]{1,0:T(8,128)(2,1)}, u32[]{:S(2)}) copy-start(bf16[512,2048]{1,0:T(8,128)(2,1)} %array.1) | copy-start | bytes 6291460
  20.5 17.9 %copy-start.7 = (f32[128]{0:T(128)S(1)}, f32[128]{0:T(128)}, u32[]{:S(2)}) copy-start(f32[128]{0:T(128)} %param.10) | copy-start | bytes 1540
  40.2 0.7 copy-start.4
  40.9 19.6 %all-to-all-start.2 = ((f32[16,4,512]{2,1,0:T(4,128)}), f32[16,4,512]{2,1,0:T(4,128)S(1)}, u32[]{:S(2)}, u32[]{:S(2)}) async-start(f32[16,4,512]{2,1,0:T(4,128)} %get-tuple-element.25), calls=%async_computation.2 | async-start | bytes 262144 | tf_op jit(solution)/shard_map/all_to_all | solution.py:24
  51.6 8.9 %copy-start.8 = (f32[1,128]{1,0:T(1,128)S(1)}, f32[1,128]{1,0:T(1,128)}, u32[]{:S(2)}) copy-start(f32[1,128]{1,0:T(1,128)} %bias.1) | copy-start | bytes 1540
  53.2 1.0 copy-start.1
  54.2 6.3 %copy-start.2 = (bf16[1024,512]{1,0:T(8,128)(2,1)S(1)}, bf16[1024,512]{1,0:T(8,128)(2,1)}, u32[]{:S(2)}) copy-start(bf16[1024,512]{1,0:T(8,128)(2,1)} %copy-done.1) | copy-start | bytes 3145732
  60.5 1.0 copy-start.5
  64.3 3.7 %copy-start.9 = (bf16[1024,256]{1,0:T(8,128)(2,1)S(1)}, bf16[1024,256]{1,0:T(8,128)(2,1)}, u32[]{:S(2)}) copy-start(bf16[1024,256]{1,0:T(8,128)(2,1)} %get-tuple-element.33) | copy-start | bytes 1572868
  64.3 20.4 %all-to-all-start.3 = ((bf16[8,296,256]{2,1,0:T(8,128)(2,1)}), bf16[8,296,256]{2,1,0:T(8,128)(2,1)S(1)}, u32[]{:S(2)}, u32[]{:S(2)}) async-start(bf16[8,296,256]{2,1,0:T(8,128)(2,1)} %get-tuple-element.42), calls=%async_computation.3 | async-start | bytes 2424832 | tf_op jit(solution)/shard_map/all_to_all | solution.py:24
  68.0 5.5 %collective-permute-start.1 = (bf16[1024,256]{1,0:T(8,128)(2,1)S(1)}, bf16[1024,256]{1,0:T(8,128)(2,1)S(1)}, u32[]{:S(2)}, u32[]{:S(2)}) collective-permute-start(bf16[1024,256]{1,0:T(8,128)(2,1)S(1)} %copy-done.9), channel_id=1, source_target_pairs={{0,1},{1,0},{2,3},{3,2},{4,5},{5,4},{6,7},{7,6},{8,9},{9,8},{10,11... | collective-permute-start | bytes 1572872 | tf_op jit(solution)/shard_map/ppermute | solution.py:28
  70.0 3.6 %collective-permute-start = (bf16[512,256]{1,0:T(8,128)(2,1)S(1)}, bf16[512,256]{1,0:T(8,128)(2,1)S(1)}, u32[]{:S(2)}, u32[]{:S(2)}) collective-permute-start(bf16[512,256]{1,0:T(8,128)(2,1)S(1)} %get-tuple-element.31.joined), channel_id=1, source_target_pairs={{0,1},{1,0},{2,3},{3,2},{4,5},{5,4},{6,7},{7,6},{8,9},{9,8},{10,11... | collective-permute-start | bytes 786440 | tf_op jit(solution)/shard_map/ppermute | solution.py:28
  75.4 21.8 %collective-permute-start.2 = (bf16[512,512]{1,0:T(8,128)(2,1)S(1)}, bf16[512,512]{1,0:T(8,128)(2,1)S(1)}, u32[]{:S(2)}, u32[]{:S(2)}) collective-permute-start(bf16[512,512]{1,0:T(8,128)(2,1)S(1)} %get-tuple-element.36), channel_id=1, source_target_pairs={{0,2},{1,15},{2,4},{3,1},{4,6},{5,3},{6,8},{7,5},{8,10},{9,7},{10,... | collective-permute-start | bytes 1572872 | tf_op jit(solution)/shard_map/ppermute | solution.py:37
  85.6 27.1 %all-to-all-start.4 = ((bf16[4,104,256]{2,1,0:T(8,128)(2,1)}), bf16[4,104,256]{2,1,0:T(8,128)(2,1)S(1)}, u32[]{:S(2)}, u32[]{:S(2)}) async-start(bf16[4,104,256]{2,1,0:T(8,128)(2,1)} %shard_map.110), calls=%async_computation.4 | async-start | bytes 425984 | tf_op jit(solution)/shard_map/all_to_all | solution.py:24
  89.0 8.2 %collective-permute-start.3 = (bf16[512,128]{1,0:T(8,128)(2,1)S(1)}, bf16[512,128]{1,0:T(8,128)(2,1)S(1)}, u32[]{:S(2)}, u32[]{:S(2)}) collective-permute-start(bf16[512,128]{1,0:T(8,128)(2,1)S(1)} %get-tuple-element.37), channel_id=1, source_target_pairs={{0,4},{1,13},{2,6},{3,15},{4,8},{5,1},{6,10},{7,3},{8,12},{9,5},{1... | collective-permute-start | bytes 393224 | tf_op jit(solution)/shard_map/ppermute | solution.py:37
  97.9 11.8 %collective-permute-start.4 = (bf16[512,128]{1,0:T(8,128)(2,1)S(1)}, bf16[512,128]{1,0:T(8,128)(2,1)S(1)}, u32[]{:S(2)}, u32[]{:S(2)}) collective-permute-start(bf16[512,128]{1,0:T(8,128)(2,1)S(1)} %get-tuple-element.38), channel_id=1, source_target_pairs={{0,4},{1,13},{2,6},{3,15},{4,8},{5,1},{6,10},{7,3},{8,12},{9,5},{1... | collective-permute-start | bytes 393224 | tf_op jit(solution)/shard_map/ppermute | solution.py:37
  101.5 10.3 %collective-permute-start.5 = (bf16[512,128]{1,0:T(8,128)(2,1)S(1)}, bf16[512,128]{1,0:T(8,128)(2,1)S(1)}, u32[]{:S(2)}, u32[]{:S(2)}) collective-permute-start(bf16[512,128]{1,0:T(8,128)(2,1)S(1)} %get-tuple-element.39), channel_id=1, source_target_pairs={{0,5},{1,12},{2,7},{3,14},{4,9},{5,0},{6,11},{7,2},{8,13},{9,4},{1... | collective-permute-start | bytes 393224 | tf_op jit(solution)/shard_map/ppermute | solution.py:37
  107.7 4.2 %collective-permute-start.6 = (bf16[512,128]{1,0:T(8,128)(2,1)S(1)}, bf16[512,128]{1,0:T(8,128)(2,1)S(1)}, u32[]{:S(2)}, u32[]{:S(2)}) collective-permute-start(bf16[512,128]{1,0:T(8,128)(2,1)S(1)} %get-tuple-element.41), channel_id=1, source_target_pairs={{0,1},{1,0},{2,3},{3,2},{4,5},{5,4},{6,7},{7,6},{8,9},{9,8},{10,11... | collective-permute-start | bytes 393224 | tf_op jit(solution)/shard_map/ppermute | solution.py:28
